TPU v7x, 256 devices: a whole 4x4x8 slice. The times are simulated.
256 devices in a mesh: st: 64 (over z, y, core), tp: 4 (over x).
Axes of the slice: x: 4, y: 4, z: 8, core: 2. Of those that a mesh axis runs over, the one named last changes fastest.
Arguments:
- tokens: bfloat16 [65536, 2048], P('st', 'tp'), may hold values from -6 to 6
- token_gain: float32 [2048], replicated, may hold values from 0.1 to 1.9
- inner_weight: bfloat16 [2048, 2048], P(None, 'tp'), may hold values from -0.125 to 0.125
- gating_weight: bfloat16 [2048, 2048], P(None, 'tp'), may hold values from -0.125 to 0.125
- filter_taps: float32 [31, 2048], P(None, 'tp'), may hold values from -2.4 to 2.4
- channel_gain: float32 [2048], P('tp'), may hold values from 0.1 to 1.9
- retrieval_gate: float32 [2048], P('tp'), may hold values from -2 to 2
- passage_store: bfloat16 [1024, 64, 2048], P('st'), may hold values from -6 to 6
- passage_gain: float32 [2048], replicated, may hold values from 0.1 to 1.9
- keys_weight: bfloat16 [2048, 1024], P(None, 'tp'), may hold values from -0.125 to 0.125
- values_weight: bfloat16 [2048, 1024], P(None, 'tp'), may hold values from -0.125 to 0.125
- owners: int32 [1024, 2], P('st'), may hold values from 0 to 63, all different within a row; in each aligned block of 16 rows (0 to 15, 16 to 31, ...) no two rows name the same one
- local_slots: int32 [1024, 2], P('st'), may hold values from 0 to 15
Outputs:
- mixed: bfloat16 [65536, 2048], P('st', 'tp')
Inputs may be any that keep to these rules, and one draw needn't show every extreme that they name: In the rows of one index of st no owner is named by more than 1 row, a bound that some block reaches; a row names 2 different owners, and every owner is named somewhere.
All inputs are finite; a program needn't handle non-finite values.
Results may differ from a plain program's by a relative error of at most 0.0059.
Values may be sent and summed in bfloat16 or wider, within the bound.
No kernel may reach another device: no remote copies, remote signals or barrier semaphores. Data moves between devices by JAX's collectives and lax.ppermute only.
A program may use at most 128 MiB of HBM per device.

v0:
```python
import math

import jax
import jax.numpy as jnp
from jax import lax
from jax.sharding import PartitionSpec as P

HEAD = 256
CONV = 31
LENGTH = 512
BLOCK = 64
PB = 2
PROWS = 64


EPSILON = 1e-06
EPSILON_NORM = 1e-05


def from_everyone(value, axis):
    copies = jnp.broadcast_to(value, (lax.axis_size(axis), *value.shape))
    return lax.all_to_all(copies, axis, split_axis=0, concat_axis=0, tiled=True)


def of_everyone(value, axis):
    return from_everyone(value, axis).sum(axis=0)


def packed_total(arrays, axis):
    ravelled, at, finished = (jnp.concatenate([a.reshape(-1) for a in arrays]), 0, [])
    subtotal = of_everyone(ravelled, axis)
    for a in arrays:
        finished.append(subtotal[at : at + a.size].reshape(a.shape))
        at += a.size
    return tuple(finished)


def project_passages(rows, passage_gain, keys_weight, values_weight):
    flat_rows = rows.reshape(-1, rows.shape[-1]).astype(jnp.float32)
    inverse = lax.rsqrt(jnp.mean(flat_rows * flat_rows, axis=1, keepdims=True) + EPSILON)
    normed = (flat_rows * inverse * passage_gain).astype(jnp.bfloat16)
    key_rows = jnp.dot(normed, keys_weight, preferred_element_type=jnp.float32).astype(jnp.bfloat16)
    value_rows = jnp.dot(normed, values_weight, preferred_element_type=jnp.float32).astype(
        jnp.bfloat16
    )
    return (key_rows, value_rows)


def body(
    tokens,
    token_gain,
    inner_weight,
    gating_weight,
    filter_taps,
    channel_gain,
    retrieval_gate,
    passage_store,
    passage_gain,
    keys_weight,
    values_weight,
    owners,
    local_slots,
):
    tok_rows = tokens.shape[0]
    model_width = inner_weight.shape[0]
    local_width = inner_weight.shape[1]
    wide_piece = lax.all_gather(tokens, "tp", axis=1, tiled=True).astype(jnp.float32)
    scaled = (wide_piece * token_gain).astype(jnp.bfloat16)
    inner_sum = jnp.dot(scaled, inner_weight, preferred_element_type=jnp.float32)
    gating_sum = jnp.dot(scaled, gating_weight, preferred_element_type=jnp.float32)
    squares = jnp.sum(wide_piece * wide_piece, axis=1)
    inner_proj, gating, squares = (inner_sum, gating_sum, squares)
    inverse = lax.rsqrt(squares / model_width + EPSILON)[:, None]
    gated = (inner_proj * inverse * jax.nn.sigmoid(gating * inverse)).astype(jnp.bfloat16)
    sequences = gated.reshape(-1, LENGTH, local_width)
    padded = jnp.pad(sequences, ((0, 0), (CONV - 1, 0), (0, 0)))
    convolved = jnp.zeros(sequences.shape, jnp.float32)
    for offset in range(CONV):
        convolved = (
            convolved
            + padded[:, offset : offset + LENGTH].astype(jnp.float32) * filter_taps[offset]
        )
    convolved = convolved.reshape(tok_rows, local_width)
    totals, square_totals = packed_total(
        (jnp.sum(convolved, axis=1), jnp.sum(convolved * convolved, axis=1)), "tp"
    )
    average = (totals / model_width)[:, None]
    variance = (square_totals / model_width)[:, None] - average * average
    conv_out = jax.nn.silu(
        (convolved - average) * lax.rsqrt(variance + EPSILON_NORM) * channel_gain
    )
    queries = conv_out.astype(jnp.bfloat16)
    store_devices = lax.axis_size("st")
    request_owner = owners.reshape(-1)
    request_slot = local_slots.reshape(-1)
    request_count = request_owner.shape[0]
    capacity = max(1, 2 * request_count // store_devices)
    matches = (
        request_owner[:, None] == jnp.arange(store_devices, dtype=jnp.int32)[None, :]
    ).astype(jnp.int32)
    before = jnp.cumsum(matches, axis=0) - matches
    ranking = jnp.sum(before * matches, axis=1)
    placed = (ranking[:, None, None] == jnp.arange(capacity, dtype=jnp.int32)[None, None, :]) & (
        matches[:, :, None] == 1
    )
    wanted = jnp.sum(jnp.where(placed, request_slot[:, None, None] + 1, 0), axis=0) - 1
    asked_slots = lax.all_to_all(wanted, "st", split_axis=0, concat_axis=0, tiled=True)
    picked = passage_store[jnp.maximum(asked_slots, 0).reshape(-1)]
    flat_index = request_owner * capacity + ranking
    owner_keys, owner_values = project_passages(picked, passage_gain, keys_weight, values_weight)
    head_width = owner_keys.shape[-1]
    arrived_keys, arrived_values = (
        lax.all_to_all(
            owner_keys.reshape(store_devices, capacity, PROWS, head_width),
            "st",
            split_axis=0,
            concat_axis=0,
            tiled=True,
        ),
        lax.all_to_all(
            owner_values.reshape(store_devices, capacity, PROWS, head_width),
            "st",
            split_axis=0,
            concat_axis=0,
            tiled=True,
        ),
    )
    key_rows = arrived_keys.reshape(store_devices * capacity, PROWS, head_width)[flat_index]
    value_rows = arrived_values.reshape(store_devices * capacity, PROWS, head_width)[flat_index]
    blocks = tok_rows // BLOCK
    key_heads = keys_weight.shape[1] // HEAD
    group_size = local_width // (key_heads * HEAD)
    query_blocks = queries.reshape(blocks, BLOCK, key_heads, group_size, HEAD)
    block_keys = key_rows.reshape(blocks, PB * PROWS, key_heads, HEAD)
    block_values = value_rows.reshape(blocks, PB * PROWS, key_heads, HEAD)
    scores = jnp.einsum(
        "btkgd,bskd->bkgts", query_blocks, block_keys, preferred_element_type=jnp.float32
    ) / math.sqrt(HEAD)
    attention_weights = jax.nn.softmax(scores, axis=-1).astype(jnp.bfloat16)
    attended = jnp.einsum(
        "bkgts,bskd->btkgd", attention_weights, block_values, preferred_element_type=jnp.float32
    ).reshape(tok_rows, local_width)
    return (conv_out + jax.nn.sigmoid(retrieval_gate) * attended).astype(jnp.bfloat16)


def solution(mesh):
    placed = (
        P("st", "tp"),
        P(),
        P(None, "tp"),
        P(None, "tp"),
        P(None, "tp"),
        P("tp"),
        P("tp"),
        P("st", None, None),
        P(),
        P(None, "tp"),
        P(None, "tp"),
        P("st", None),
        P("st", None),
    )
    return jax.shard_map(body, mesh=mesh, in_specs=placed, out_specs=P("st", "tp"), check_vma=False)
```

profile of v0, /device:TPU:2, one launch (start us, length us, event | category | flops | bytes accessed | tf_op | source)
XLA Modules:
  0.0 211.6 jit_solution(8918889044891661108)
XLA Ops:
  9.5 12.1 %all-to-all-start.1 = ((s32[64,1,1]{2,1,0:T(1,128)}), s32[64,1,1]{2,1,0:T(1,128)S(1)}, u32[]{:S(2)}, u32[]{:S(2)}) async-start(s32[64,1,1]{2,1,0:T(1,128)} %copy.59), calls=%async_computation.1 | async-start | bytes 65536 | tf_op jit(solution)/shard_map/all_to_all | solution.py:107
  22.4 8.8 %all-to-all-done.1 = s32[64,1,1]{2,1,0:T(1,128)S(1)} async-done(((s32[64,1,1]{2,1,0:T(1,128)}), s32[64,1,1]{2,1,0:T(1,128)S(1)}, u32[]{:S(2)}, u32[]{:S(2)}) %all-to-all-start.1) | async-done | bytes 288 | tf_op jit(solution)/shard_map/all_to_all | solution.py:107
  32.4 10.1 %gather_fusion = bf16[64,64,2048]{2,1,0:T(8,128)(2,1)} fusion(bf16[16,64,2048]{2,1,0:T(8,128)(2,1)} %param.20, s32[1024]{0:T(1024)S(1)} %pad_clamp_fusion.1), kind=kCustom, calls=%fused_computation | custom fusion | bytes 33554688 | tf_op jit(solution)/shard_map/gather | solution.py:108
  42.5 7.3 %multiply_reduce_fusion = f32[64,64]{1,0:T(8,128)S(1)} fusion(bf16[64,64,2048]{2,1,0:T(8,128)(2,1)} %gather_fusion), kind=kLoop, calls=%fused_computation.6 | loop fusion | flops 25161728 | bytes 16793600 | tf_op jit(solution)/shard_map/reduce_sum | solution.py:40
  49.9 10.2 %fusion.1 = bf16[4096,2048]{1,0:T(8,128)(2,1)S(1)} fusion(f32[2048]{0:T(1024)S(1)} %copy-done.5, f32[4096]{0:T(1024)S(1)} %rsqrt.28, bf16[64,64,2048]{2,1,0:T(8,128)(2,1)} %gather_fusion), kind=kLoop, calls=%fused_computation.5 | loop fusion | flops 33554432 | bytes 33579008 | tf_op jit(solution)/shard_map/convert_element_type | solution.py:41
  60.1 6.4 %convolution_convert_fusion.1 = bf16[4096,256]{1,0:T(8,128)(2,1)} fusion(bf16[4096,2048]{1,0:T(8,128)(2,1)S(1)} %fusion.1, bf16[2048,256]{1,0:T(8,128)(2,1)S(1)} %copy-done.9), kind=kOutput, calls=%fused_computation.12 | convolution fusion | flops 4296015872 | bytes 19922944 | tf_op jit(solution)/shard_map/dot_general | solution.py:43
  66.5 5.9 %all-to-all-start.2 = ((bf16[64,1,64,256]{3,2,1,0:T(8,128)(2,1)}), bf16[64,1,64,256]{3,2,1,0:T(8,128)(2,1)}, u32[]{:S(2)}, u32[]{:S(2)}) async-start(bf16[64,1,64,256]{3,2,1,0:T(8,128)(2,1)} %bitcast.102), calls=%async_computation.2 | async-start | bytes 4194304 | tf_op jit(solution)/shard_map/all_to_all | solution.py:120
  72.5 11.9 %convolution_convert_fusion = bf16[4096,256]{1,0:T(8,128)(2,1)} fusion(bf16[4096,2048]{1,0:T(8,128)(2,1)} %copy-done.2, bf16[2048,256]{1,0:T(8,128)(2,1)} %param.22), kind=kOutput, calls=%fused_computation.11 | convolution fusion | flops 4296015872 | bytes 19922944 | tf_op jit(solution)/shard_map/dot_general | solution.py:42
  84.3 39.0 %all-to-all-done.2 = bf16[64,1,64,256]{3,2,1,0:T(8,128)(2,1)} async-done(((bf16[64,1,64,256]{3,2,1,0:T(8,128)(2,1)}), bf16[64,1,64,256]{3,2,1,0:T(8,128)(2,1)}, u32[]{:S(2)}, u32[]{:S(2)}) %all-to-all-start.2) | async-done | bytes 2097184 | tf_op jit(solution)/shard_map/all_to_all | solution.py:120
  123.4 6.0 %all-to-all-start.3 = ((bf16[64,1,64,256]{3,2,1,0:T(8,128)(2,1)}), bf16[64,1,64,256]{3,2,1,0:T(8,128)(2,1)}, u32[]{:S(2)}, u32[]{:S(2)}) async-start(bf16[64,1,64,256]{3,2,1,0:T(8,128)(2,1)} %bitcast.101), calls=%async_computation.3 | async-start | bytes 4194304 | tf_op jit(solution)/shard_map/all_to_all | solution.py:113
  129.5 3.2 %fusion.3 = f32[1024]{0:T(1024)S(1)} fusion(bf16[1024,2048]{1,0:T(8,128)(2,1)} %all-gather.2.cloned.1.call-done), kind=kLoop, calls=%fused_computation.10 | loop fusion | flops 6290432 | bytes 4198400 | tf_op jit(solution)/shard_map/reduce_sum | solution.py:71
  132.9 2.3 %fusion.4 = f32[1024,512]{1,0:T(8,128)S(1)} fusion(bf16[2048,512]{1,0:T(8,128)(2,1)S(1)} %copy-done, bf16[1024,2048]{1,0:T(8,128)(2,1)S(1)} %copy-done.3, f32[2048]{0:T(1024)S(1)} %copy-done.10), kind=kOutput, calls=%fused_computation.13 | convolution fusion | flops 2153775104 | bytes 8396800 | tf_op jit(solution)/shard_map/dot_general | solution.py:70
  135.2 2.6 %multiply_convert_fusion.1 = bf16[1024,512]{1,0:T(8,128)(2,1)S(1)} fusion(f32[1024,512]{1,0:T(8,128)S(1)} %fusion.4, bf16[2048,512]{1,0:T(8,128)(2,1)S(1)} %copy-done.8, bf16[1024,2048]{1,0:T(8,128)(2,1)S(1)} %copy-done.3, f32[2048]{0:T(1024)S(1)} %copy-done.10, f32[1024]{0:T(1024)S(1)} %add_rsqrt_fusion.3), kind=kOutput, calls=%fused_computation.25 | convolution fusion | flops 2157445120 | bytes 9449472 | tf_op jit(solution)/shard_map/dot_general | solution.py:69
  137.8 9.8 %fusion.25 = (f32[2,512]{1,0:T(2,128)S(1)}, f32[2,512]{1,0:T(2,128)S(1)}, f32[2,512,512]{2,1,0:T(8,128)}) fusion(f32[512]{0:T(512)S(1)} %bitcast.120, bf16[2,512,512]{2,1,0:T(8,128)(2,1)S(1)} %bitcast.105, f32[512]{0:T(512)S(1)} %bitcast.121, f32[512]{0:T(512)S(1)} %bitcast.123, f32[512]{0:T(512)S(1)} %bitcast.124, f32[512]{0:T(512)S(1)} %bitcast.125, ...), kind=kLoop, calls=%fused_computation.67 | loop fusion | flops 49805312 | bytes 3217408 | tf_op jit(solution)/shard_map/reduce_sum | solution.py:85
  147.7 32.6 %all-to-all-done.3 = bf16[64,1,64,256]{3,2,1,0:T(8,128)(2,1)} async-done(((bf16[64,1,64,256]{3,2,1,0:T(8,128)(2,1)}), bf16[64,1,64,256]{3,2,1,0:T(8,128)(2,1)}, u32[]{:S(2)}, u32[]{:S(2)}) %all-to-all-start.3) | async-done | bytes 2097184 | tf_op jit(solution)/shard_map/all_to_all | solution.py:113
  180.9 4.8 %all-to-all-start = ((f32[4,1,2048]{2,1,0:T(1,128)}), f32[4,1,2048]{2,1,0:T(1,128)S(1)}, u32[]{:S(2)}, u32[]{:S(2)}) async-start(f32[4,1,2048]{2,1,0:T(1,128)} %broadcast_in_dim.10), calls=%async_computation | async-start | bytes 65536 | tf_op jit(solution)/shard_map/all_to_all | solution.py:22
  185.7 2.2 %gather_fusion.1 = bf16[32,64,256]{2,1,0:T(8,128)(2,1)S(1)} fusion(bf16[64,64,256]{2,1,0:T(8,128)(2,1)} %bitcast.37, s32[1024]{0:T(1024)S(1)} %pad_clamp_fusion), kind=kCustom, calls=%fused_computation.1 | custom fusion | bytes 2097280 | tf_op jit(solution)/shard_map/gather | solution.py:129
  187.9 3.2 %gather_fusion.2 = bf16[32,64,256]{2,1,0:T(8,128)(2,1)} fusion(bf16[64,64,256]{2,1,0:T(8,128)(2,1)} %bitcast.45, s32[1024]{0:T(1024)S(1)} %pad_clamp_fusion), kind=kCustom, calls=%fused_computation.2 | custom fusion | bytes 2097280 | tf_op jit(solution)/shard_map/gather | solution.py:128
  191.1 3.5 %reshape.340 = f32[16,64,2,256]{3,2,1,0:T(2,128)} reshape(f32[2,512,512]{2,1,0:T(8,128)} %get-tuple-element.7) | data formatting | bytes 4194304 | tf_op jit(solution)/shard_map/reshape | solution.py:83
  194.9 2.9 %fusion.28 = (f32[16,2,64]{2,1,0:T(2,128)S(1)}, f32[16,1,2,64,128]{4,3,2,0,1:T(8,128)S(1)}) fusion(bf16[16,128,256,1]{2,1,3,0:T(8,128)(2,1)} %bitcast.104, f32[16,64,2,256]{3,2,1,0:T(2,128)} %reshape.340, f32[2,256]{1,0:T(2,128)S(1)} %mul.535, f32[16,64]{1,0:T(8,128)S(1)} %add_rsqrt_fusion.1, f32[16,64]{1,0:T(8,128)S(1)} %div.59), kind=kOutput, calls=%fused_computation.70 | convolution fusion | flops 138934272 | bytes 4212736 | tf_op jit(solution)/shard_map/btkgd,bskd->bkgts/dot_general | solution.py:136
  198.4 1.3 convolution_bitcast_fusion
  199.8 1.6 copy.64
  201.6 1.4 copy-done.1
  203.0 1.8 add_convert_fusion
  (60 shorter events, 7.1 us)
Async XLA Ops:
  6.5 126.2 %copy-start = (bf16[2048,512]{1,0:T(8,128)(2,1)S(1)}, bf16[2048,512]{1,0:T(8,128)(2,1)}, u32[]{:S(2)}) copy-start(bf16[2048,512]{1,0:T(8,128)(2,1)} %param.16) | copy-start | bytes 6291460
  9.5 21.7 %all-to-all-start.1 = ((s32[64,1,1]{2,1,0:T(1,128)}), s32[64,1,1]{2,1,0:T(1,128)S(1)}, u32[]{:S(2)}, u32[]{:S(2)}) async-start(s32[64,1,1]{2,1,0:T(1,128)} %copy.59), calls=%async_computation.1 | async-start | bytes 65536 | tf_op jit(solution)/shard_map/all_to_all | solution.py:107
  21.7 107.8 %all-gather.2.cloned.1.call-start = ((), (), s32[]{:S(2)}) async-start(), calls=%async_computation.4 | async-start | bytes 5242880 | tf_op jit(solution)/shard_map/all_gather | solution.py:67
  42.5 7.4 %copy-start.5 = (f32[2048]{0:T(1024)S(1)}, f32[2048]{0:T(1024)}, u32[]{:S(2)}) copy-start(f32[2048]{0:T(1024)} %param.21) | copy-start | bytes 24580
  49.9 10.2 %copy-start.9 = (bf16[2048,256]{1,0:T(8,128)(2,1)S(1)}, bf16[2048,256]{1,0:T(8,128)(2,1)}, u32[]{:S(2)}) copy-start(bf16[2048,256]{1,0:T(8,128)(2,1)} %param.23) | copy-start | bytes 3145732
  60.1 6.4 %copy-start.2 = (bf16[4096,2048]{1,0:T(8,128)(2,1)}, bf16[4096,2048]{1,0:T(8,128)(2,1)S(1)}, u32[]{:S(2)}) copy-start(bf16[4096,2048]{1,0:T(8,128)(2,1)S(1)} %fusion.1) | copy-start | bytes 50331652
  66.5 6.0 %copy-start.7 = (f32[512]{0:T(512)S(1)}, f32[512]{0:T(512)}, u32[]{:S(2)}) copy-start(f32[512]{0:T(512)} %param.19) | copy-start | bytes 6148
  66.5 56.9 %all-to-all-start.2 = ((bf16[64,1,64,256]{3,2,1,0:T(8,128)(2,1)}), bf16[64,1,64,256]{3,2,1,0:T(8,128)(2,1)}, u32[]{:S(2)}, u32[]{:S(2)}) async-start(bf16[64,1,64,256]{3,2,1,0:T(8,128)(2,1)} %bitcast.102), calls=%async_computation.2 | async-start | bytes 4194304 | tf_op jit(solution)/shard_map/all_to_all | solution.py:120
  123.4 6.0 %copy-start.4 = (f32[31,512]{1,0:T(8,128)S(1)}, f32[31,512]{1,0:T(8,128)}, u32[]{:S(2)}) copy-start(f32[31,512]{1,0:T(8,128)} %param.17) | copy-start | bytes 190468
  123.4 56.9 %all-to-all-start.3 = ((bf16[64,1,64,256]{3,2,1,0:T(8,128)(2,1)}), bf16[64,1,64,256]{3,2,1,0:T(8,128)(2,1)}, u32[]{:S(2)}, u32[]{:S(2)}) async-start(bf16[64,1,64,256]{3,2,1,0:T(8,128)(2,1)} %bitcast.101), calls=%async_computation.3 | async-start | bytes 4194304 | tf_op jit(solution)/shard_map/all_to_all | solution.py:113
  129.4 3.3 %copy-start.10 = (f32[2048]{0:T(1024)S(1)}, f32[2048]{0:T(1024)}, u32[]{:S(2)}) copy-start(f32[2048]{0:T(1024)} %param.14) | copy-start | bytes 24580
  129.4 3.5 %copy-start.3 = (bf16[1024,2048]{1,0:T(8,128)(2,1)S(1)}, bf16[1024,2048]{1,0:T(8,128)(2,1)}, u32[]{:S(2)}) copy-start(bf16[1024,2048]{1,0:T(8,128)(2,1)} %all-gather.2.cloned.1.call-done) | copy-start | bytes 12582916
  132.9 2.3 %copy-start.8 = (bf16[2048,512]{1,0:T(8,128)(2,1)S(1)}, bf16[2048,512]{1,0:T(8,128)(2,1)}, u32[]{:S(2)}) copy-start(bf16[2048,512]{1,0:T(8,128)(2,1)} %param.15) | copy-start | bytes 6291460
  137.8 47.9 %copy-start.6 = (f32[512]{0:T(512)S(1)}, f32[512]{0:T(512)}, u32[]{:S(2)}) copy-start(f32[512]{0:T(512)} %param.18) | copy-start | bytes 6148
  180.9 13.8 %all-to-all-start = ((f32[4,1,2048]{2,1,0:T(1,128)}), f32[4,1,2048]{2,1,0:T(1,128)S(1)}, u32[]{:S(2)}, u32[]{:S(2)}) async-start(f32[4,1,2048]{2,1,0:T(1,128)} %broadcast_in_dim.10), calls=%async_computation | async-start | bytes 65536 | tf_op jit(solution)/shard_map/all_to_all | solution.py:22
  201.4 1.6 copy-start.1
Sparse Core Ops, SparseCore 0:
  24.3 51.2 all-gather.1
where the time goes:
time: 212 us
  waiting for transfers between devices  81.1 us (38%)
  other arithmetic  35.6 us (17%)
  starting transfers between devices  28.8 us (14%)
  matrix products  27.4 us (13%)
  local copies, waits for them, and re-layouts  25.1 us (12%)
  between operations  13.7 us (6%)
    all_to_all x1, waiting for transfers between devices, body(): lax.all_to_all(owner_values.reshape(store_devices, capacity, PROWS, head_...  39 us
    all_to_all x1, waiting for transfers between devices, body(): lax.all_to_all(owner_keys.reshape(store_devices, capacity, PROWS, head_wi...  32.6 us
    all_to_all x1, starting transfers between devices, body(): lax.all_to_all(wanted, 'st', split_axis=0, concat_axis=0, tiled=True)  12.1 us
    dot_general x1, matrix products, project_passages(): jnp.dot(normed, keys_weight, preferred_element_type=jnp.float32)  11.9 us
    convert_element_type x1, other arithmetic, project_passages(): normed = (flat_rows * inverse * passage_gain).astype(jnp.bfloat16)  10.2 us
    gather x1, local copies, waits for them, and re-layouts, body(): picked = passage_store[jnp.maximum(asked_slots, 0).reshape(-1)]  10.1 us
    reduce_sum x1, other arithmetic, body(): jnp.sum(convolved, axis=1)  9.82 us
    all_to_all x1, waiting for transfers between devices, body(): lax.all_to_all(wanted, 'st', split_axis=0, concat_axis=0, tiled=True)  8.82 us
  transfers between devices with their start and end apart: 5, of which 3 were waited for; matrix products, arithmetic and copies ran while one was open for 35% of the time, Pallas kernels for 0%

commit v1 on v0

v1 whole, which is shorter than its diff:
```python
import math

import jax
import jax.numpy as jnp
from jax import lax
from jax.experimental import pallas as pl
from jax.experimental.pallas import tpu as pltpu
from jax.sharding import Mesh
from jax.sharding import PartitionSpec as P

D = 2048
HEAD = 256
CONV = 31
LENGTH = 512
BLOCK = 64
PB = 2
PROWS = 64
EPSILON = 1e-06
EPSILON_NORM = 1e-05
ST = ("z", "y", "c")
LEAD = 32
ROWS_CHUNK = 64


def ring(size, step):
    return [(i, (i + step) % size) for i in range(size)]


def whole(shape):
    return pl.BlockSpec(shape, lambda *_: (0,) * len(shape))


def project_kernel(rows_ref, gain_ref, keys_ref, values_ref, out_ref):
    rows = rows_ref[...].astype(jnp.float32)
    inverse = lax.rsqrt(jnp.mean(rows * rows, axis=1, keepdims=True) + EPSILON)
    normed = (rows * inverse * gain_ref[...]).astype(jnp.bfloat16)
    out_ref[:, :HEAD] = jnp.dot(normed, keys_ref[...], preferred_element_type=jnp.float32).astype(
        jnp.bfloat16
    )
    out_ref[:, HEAD:] = jnp.dot(
        normed, values_ref[...], preferred_element_type=jnp.float32
    ).astype(jnp.bfloat16)


def project_passages(store, gain, keys_weight, values_weight):
    rows = store.reshape(-1, D)
    count = rows.shape[0]
    tile = 256
    return pl.pallas_call(
        project_kernel,
        grid=(count // tile,),
        in_specs=[
            pl.BlockSpec((tile, D), lambda i: (i, 0)),
            whole((1, D)),
            whole((D, HEAD)),
            whole((D, HEAD)),
        ],
        out_specs=pl.BlockSpec((tile, 2 * HEAD), lambda i: (i, 0)),
        out_shape=jax.ShapeDtypeStruct((count, 2 * HEAD), jnp.bfloat16),
        cost_estimate=pl.CostEstimate(
            flops=4 * count * D * HEAD, transcendentals=0, bytes_accessed=7 << 20
        ),
        name="project_passages",
    )(rows, gain.reshape(1, D), keys_weight, values_weight)


def token_kernel(
    me_ref,
    own_ref,
    left_ref,
    right_ref,
    far0_ref,
    far1_ref,
    gain_ref,
    inner_ref,
    gating_ref,
    taps_ref,
    out_ref,
    stats_ref,
    padded_ref,
):
    me = me_ref[0]
    first = pl.program_id(0) == 0
    width = own_ref.shape[1]
    squares = jnp.zeros((LENGTH, 1), jnp.float32)
    inner = jnp.zeros((LENGTH, width), jnp.float32)
    gating = jnp.zeros((LENGTH, width), jnp.float32)
    for offset in range(4):
        at = lax.rem(me + offset, 4)
        if offset == 0:
            piece = own_ref[...].astype(jnp.float32)
        elif offset == 1:
            piece = right_ref[...].astype(jnp.float32)
        elif offset == 3:
            piece = left_ref[...].astype(jnp.float32)
        else:
            piece = jnp.where(
                first, far0_ref[...].astype(jnp.float32), far1_ref[...].astype(jnp.float32)
            )
        squares = squares + jnp.sum(piece * piece, axis=1, keepdims=True)
        scaled = (piece * gain_ref[at]).astype(jnp.bfloat16)
        inner = inner + jnp.dot(scaled, inner_ref[at], preferred_element_type=jnp.float32)
        gating = gating + jnp.dot(scaled, gating_ref[at], preferred_element_type=jnp.float32)
    inverse = lax.rsqrt(squares / D + EPSILON)
    gated = (inner * inverse * jax.nn.sigmoid(gating * inverse)).astype(jnp.bfloat16)
    padded_ref[:LEAD, :] = jnp.zeros((LEAD, width), jnp.float32)
    padded_ref[LEAD:, :] = gated.astype(jnp.float32)
    shift = LEAD - CONV + 1

    def step(n):
        base = n * ROWS_CHUNK
        sums = jnp.zeros((ROWS_CHUNK, 128), jnp.float32)
        square_sums = jnp.zeros((ROWS_CHUNK, 128), jnp.float32)
        for lane in range(0, width, 128):
            total = jnp.zeros((ROWS_CHUNK, 128), jnp.float32)
            for s in range(8):
                part = None
                for j in range(LEAD // 8 + 1):
                    tap = 8 * j + s - shift
                    if tap < 0 or tap >= CONV:
                        continue
                    height = ROWS_CHUNK + (8 if s else 0)
                    term = (
                        padded_ref[pl.ds(base + 8 * j, height), lane : lane + 128]
                        * taps_ref[tap : tap + 1, lane : lane + 128]
                    )
                    part = term if part is None else part + term
                total = total + part[s : s + ROWS_CHUNK]
            out_ref[pl.ds(base, ROWS_CHUNK), lane : lane + 128] = total
            sums = sums + total
            square_sums = square_sums + total * total
        return sums, square_sums

    for n in range(LENGTH // 128):
        pair = [step(2 * n + h) for h in range(2)]
        sums = jnp.concatenate([pair[0][0], pair[1][0]], axis=0)
        square_sums = jnp.concatenate([pair[0][1], pair[1][1]], axis=0)
        stats_ref[0, n : n + 1, :] = jnp.sum(sums.T, axis=0, keepdims=True)
        stats_ref[1, n : n + 1, :] = jnp.sum(square_sums.T, axis=0, keepdims=True)


def token_path(me, own, left, right, far0, far1, gain, inner_weight, gating_weight, taps):
    rows, width = own.shape
    grid_spec = pltpu.PrefetchScalarGridSpec(
        num_scalar_prefetch=1,
        grid=(rows // LENGTH,),
        in_specs=[pl.BlockSpec((LENGTH, width), lambda i, m: (i, 0))] * 3
        + [
            whole((LENGTH, width)),
            whole((LENGTH, width)),
            whole((4, 1, width)),
            whole((4, width, width)),
            whole((4, width, width)),
            whole((CONV, width)),
        ],
        out_specs=[
            pl.BlockSpec((LENGTH, width), lambda i, m: (i, 0)),
            pl.BlockSpec((None, 2, LENGTH // 128, 128), lambda i, m: (i, 0, 0, 0)),
        ],
        scratch_shapes=[pltpu.VMEM((LEAD + LENGTH, width), jnp.float32)],
    )
    return pl.pallas_call(
        token_kernel,
        grid_spec=grid_spec,
        out_shape=[
            jax.ShapeDtypeStruct((rows, width), jnp.float32),
            jax.ShapeDtypeStruct((rows // LENGTH, 2, LENGTH // 128, 128), jnp.float32),
        ],
        cost_estimate=pl.CostEstimate(
            flops=4 * rows * D * width, transcendentals=rows * width, bytes_accessed=10 << 20
        ),
        name="token_path",
    )(
        me,
        own,
        left,
        right,
        far0,
        far1,
        gain.reshape(4, 1, width),
        inner_weight.reshape(4, width, width),
        gating_weight.reshape(4, width, width),
        taps,
    )


def attend_kernel(
    where_ref, conv_ref, stats_ref, gain_ref, gate_ref, arrived_ref, out_ref, held_ref, sems
):
    turn = pl.program_id(0)
    count = where_ref.shape[0]

    @pl.when(turn == 0)
    def _():
        for n in range(count):
            pltpu.make_async_copy(
                arrived_ref.at[where_ref[n]], held_ref.at[n], sems.at[n]
            ).start()

    width = conv_ref.shape[1]
    average = stats_ref[0, pl.ds(turn, 1), :] / D
    variance = stats_ref[1, pl.ds(turn, 1), :] / D - average * average
    spread = lax.rsqrt(variance + EPSILON_NORM)
    average = jnp.broadcast_to(average, (128, 128)).T
    spread = jnp.broadcast_to(spread, (128, 128)).T
    pieces = []
    for lane in range(0, width, 128):
        scaled = (
            (conv_ref[:, lane : lane + 128] - average) * spread * gain_ref[:, lane : lane + 128]
        )
        pieces.append(scaled * jax.nn.sigmoid(scaled))
    conv_out = jnp.concatenate(pieces, axis=1)
    queries = conv_out.astype(jnp.bfloat16)
    weight = jax.nn.sigmoid(gate_ref[...])
    for b in range(2):
        keys, values = [], []
        for p in range(PB):
            n = (turn * 2 + b) * PB + p
            pltpu.make_async_copy(arrived_ref.at[0], held_ref.at[n], sems.at[n]).wait()
            keys.append(held_ref[n, :, :HEAD])
            values.append(held_ref[n, :, HEAD:])
        keys = jnp.concatenate(keys, axis=0)
        values = jnp.concatenate(values, axis=0)
        rows = slice(b * BLOCK, (b + 1) * BLOCK)
        heads = jnp.concatenate([queries[rows, :HEAD], queries[rows, HEAD:]], axis=0)
        scores = lax.dot_general(
            heads, keys, (((1,), (1,)), ((), ())), preferred_element_type=jnp.float32
        ) / math.sqrt(HEAD)
        raised = jnp.exp(scores - jnp.max(scores, axis=1, keepdims=True))
        shares = (raised / jnp.sum(raised, axis=1, keepdims=True)).astype(jnp.bfloat16)
        attended = jnp.dot(shares, values, preferred_element_type=jnp.float32)
        attended = jnp.concatenate([attended[:BLOCK], attended[BLOCK:]], axis=1)
        out_ref[rows, :] = (conv_out[rows] + weight * attended).astype(jnp.bfloat16)


def attend(where, convolved, stats, channel_gain, retrieval_gate, arrived):
    rows, width = convolved.shape
    count = where.shape[0]
    grid_spec = pltpu.PrefetchScalarGridSpec(
        num_scalar_prefetch=1,
        grid=(rows // 128,),
        in_specs=[
            pl.BlockSpec((128, width), lambda i, w: (i, 0)),
            whole((2, rows // 128, 128)),
            whole((1, width)),
            whole((1, width)),
            pl.BlockSpec(memory_space=pl.ANY),
        ],
        out_specs=pl.BlockSpec((128, width), lambda i, w: (i, 0)),
        scratch_shapes=[
            pltpu.VMEM((count, PROWS, 2 * HEAD), jnp.bfloat16),
            pltpu.SemaphoreType.DMA((count,)),
        ],
    )
    return pl.pallas_call(
        attend_kernel,
        grid_spec=grid_spec,
        out_shape=jax.ShapeDtypeStruct((rows, width), jnp.bfloat16),
        cost_estimate=pl.CostEstimate(
            flops=4 * rows * 2 * PB * PROWS * HEAD,
            transcendentals=2 * rows * width,
            bytes_accessed=5 << 20,
        ),
        name="attend",
    )(
        where,
        convolved,
        stats,
        channel_gain.reshape(1, width),
        retrieval_gate.reshape(1, width),
        arrived,
    )


def body(
    tokens,
    token_gain,
    inner_weight,
    gating_weight,
    filter_taps,
    channel_gain,
    retrieval_gate,
    passage_store,
    passage_gain,
    keys_weight,
    values_weight,
    owners,
    local_slots,
):
    st = lax.axis_size(ST)
    me = lax.axis_index("tp").astype(jnp.int32).reshape(1)
    left = lax.ppermute(tokens, "tp", ring(4, 1))
    right = lax.ppermute(tokens, "tp", ring(4, -1))
    far0 = lax.ppermute(left[:LENGTH], "tp", ring(4, 1))
    far1 = lax.ppermute(right[LENGTH:], "tp", ring(4, -1))

    asked = owners.reshape(-1)
    slots = local_slots.reshape(-1)
    wanted = jnp.sum(
        jnp.where(asked[:, None] == jnp.arange(st, dtype=jnp.int32)[None, :], slots[:, None], 0),
        axis=0,
    )
    sent = lax.all_to_all(wanted[:, None], ST, split_axis=0, concat_axis=0, tiled=True)
    own = project_passages(passage_store, passage_gain, keys_weight, values_weight)
    own = own.reshape(-1, PROWS, 2 * HEAD)
    arrived = lax.all_to_all(own[sent[:, 0]], ST, split_axis=0, concat_axis=0, tiled=True)

    convolved, stats = token_path(
        me, tokens, left, right, far0, far1, token_gain, inner_weight, gating_weight, filter_taps
    )
    stats = lax.psum(stats, "tp")
    stats = stats.transpose(1, 0, 2, 3).reshape(2, -1, 128)
    return attend(asked, convolved, stats, channel_gain, retrieval_gate, arrived)


def solution(mesh):
    st, tp = mesh.devices.shape
    fine = Mesh(mesh.devices.reshape(st // 8, 4, 2, tp), ST + ("tp",))
    placed = (
        P(ST, "tp"),
        P(),
        P(None, "tp"),
        P(None, "tp"),
        P(None, "tp"),
        P("tp"),
        P("tp"),
        P(ST, None, None),
        P(),
        P(None, "tp"),
        P(None, "tp"),
        P(ST, None),
        P(ST, None),
    )
    return jax.shard_map(
        body, mesh=fine, in_specs=placed, out_specs=P(ST, "tp"), check_vma=False
    )
```

time: 212 us -> 146 us (0.69)
  Pallas kernels: 0 us -> 34.5 us
  other arithmetic: 35.6 us -> 1.33 us
  matrix products: 27.4 us -> 0 us
  local copies, waits for them, and re-layouts: 25.1 us -> 7.18 us
  between operations: 13.7 us -> 0.22 us
  waiting for transfers between devices: 81.1 us -> 68.4 us
  blocking collectives: 0 us -> 9.86 us
  starting transfers between devices: 28.8 us -> 24.4 us
    all_to_all x4 -> x2, waiting for transfers between devices: 80.4 us -> 32.9 us  [the longest x1 30.1 us: body(): lax.all_to_all(own[sent[:, 0]], ST, split_axis=0, concat_axis=0, tiled=True)]
    ppermute x0 -> x4, waiting for transfers between devices: none -> 35.6 us  [the longest x1 23.2 us: body(): left = lax.ppermute(tokens, 'tp', ring(4, 1))]
    pallas_call x0 -> x3, Pallas kernels: none -> 34.5 us  [the longest x1 15.5 us: token_path(): pl.pallas_call(token_kernel, grid_spec=grid_spec, out_shape=[jax.ShapeDty...]
    dot_general x6 -> x0, matrix products: 27.4 us -> none  [the longest x1 11.9 us: project_passages(): jnp.dot(normed, keys_weight, preferred_element_type=jnp.float32)]
    reduce_sum x7 -> x1, other arithmetic: 21.3 us -> 0.09 us  [body(): jnp.sum(jnp.where(asked[:, None] == jnp.arange(st, dtype=jnp.int32)[None,...]
    convert_element_type x3 -> x0, other arithmetic: 12.1 us -> none  [the longest x1 10.2 us: project_passages(): normed = (flat_rows * inverse * passage_gain).astype(jnp.bfloat16)]
    gather x3 -> x1, local copies, waits for them, and re-layouts: 15.4 us -> 4.01 us  [body(): own[sent[:, 0]]]
    psum x0 -> x1, blocking collectives: none -> 9.86 us  [body(): stats = lax.psum(stats, 'tp')]
  transfers between devices with their start and end apart: 5 -> 6, of which waited for: 3 -> 5; matrix products, arithmetic and copies ran while one was open for 35% -> 1% of each run, Pallas kernels for 0% -> 15%
where the time goes in v1:
time: 146 us
  waiting for transfers between devices  68.4 us (47%)
  Pallas kernels  34.5 us (24%)
  starting transfers between devices  24.4 us (17%)
  blocking collectives  9.86 us (7%)
  local copies, waits for them, and re-layouts  7.18 us (5%)
    all_to_all x1, waiting for transfers between devices, body(): lax.all_to_all(own[sent[:, 0]], ST, split_axis=0, concat_axis=0, tiled=True)  30.1 us
    ppermute x1, waiting for transfers between devices, body(): left = lax.ppermute(tokens, 'tp', ring(4, 1))  23.2 us
    pallas_call x1, Pallas kernels, token_path(): pl.pallas_call(token_kernel, grid_spec=grid_spec, out_shape=[jax.ShapeDty...  15.5 us
    pallas_call x1, Pallas kernels, attend(): pl.pallas_call(attend_kernel, grid_spec=grid_spec, out_shape=jax.ShapeDty...  12.2 us
    all_to_all x1, starting transfers between devices, body(): lax.all_to_all(wanted[:, None], ST, split_axis=0, concat_axis=0, tiled=True)  12.1 us
    ppermute x1, waiting for transfers between devices, body(): far0 = lax.ppermute(left[:LENGTH], 'tp', ring(4, 1))  10.8 us
    psum x1, blocking collectives, body(): stats = lax.psum(stats, 'tp')  9.86 us
    all_to_all x1, starting transfers between devices, body(): lax.all_to_all(own[sent[:, 0]], ST, split_axis=0, concat_axis=0, tiled=True)  7.78 us
  transfers between devices with their start and end apart: 6, of which 5 were waited for; matrix products, arithmetic and copies ran while one was open for 1% of the time, Pallas kernels for 15%

profile of v1, /device:TPU:2, one launch (start us, length us, event | category | flops | bytes accessed | tf_op | source)
XLA Modules:
  0.0 145.9 jit_solution(9333970272545070902)
XLA Ops:
  0.0 0.8 copy.28
  0.8 0.1 reshape.65.where_ref
  0.9 0.8 copy.30
  1.6 0.1 broadcast_in_dim.17
  1.7 0.1 select_reduce_fusion
  1.8 0.7 copy.31
  2.5 12.1 %all-to-all-start = ((s32[64,1,1]{2,1,0:T(1,128)}), s32[64,1,1]{2,1,0:T(1,128)S(1)}, u32[]{:S(2)}, u32[]{:S(2)}) async-start(s32[64,1,1]{2,1,0:T(1,128)} %copy.31), calls=%async_computation | async-start | bytes 65536 | tf_op jit(solution)/shard_map/all_to_all | solution.py:303
  14.6 6.8 %project_passages.1 = bf16[1024,512]{1,0:T(8,128)(2,1)} custom-call(bf16[1024,2048]{1,0:T(8,128)(2,1)} %bitcast.22, f32[1,2048]{1,0:T(1,128)} %bitcast.25, bf16[2048,256]{1,0:T(8,128)(2,1)} %keys_ref.1, bf16[2048,256]{1,0:T(8,128)(2,1)} %values_ref.1), custom_call_target="tpu_custom_call" | custom-call | flops 2147483648 | bytes 7340032 | tf_op jit(solution)/shard_map/project_passages/pallas_call | solution.py:49
  21.4 2.8 %all-to-all-done = s32[64,1,1]{2,1,0:T(1,128)S(1)} async-done(((s32[64,1,1]{2,1,0:T(1,128)}), s32[64,1,1]{2,1,0:T(1,128)S(1)}, u32[]{:S(2)}, u32[]{:S(2)}) %all-to-all-start) | async-done | bytes 288 | tf_op jit(solution)/shard_map/all_to_all | solution.py:303
  24.2 1.2 reduce
  25.5 4.0 %gather_fusion = bf16[64,64,512]{2,1,0:T(8,128)(2,1)} fusion(bf16[16,64,512]{2,1,0:T(8,128)(2,1)} %bitcast.16, s32[1024]{0:T(1024)S(1)} %pad_clamp_fusion), kind=kCustom, calls=%fused_computation | custom fusion | bytes 8388864 | tf_op jit(solution)/shard_map/gather | solution.py:306
  29.5 7.8 %all-to-all-start.1 = ((bf16[64,64,512]{2,1,0:T(8,128)(2,1)}), bf16[64,64,512]{2,1,0:T(8,128)(2,1)}, u32[]{:S(2)}, u32[]{:S(2)}) async-start(bf16[64,64,512]{2,1,0:T(8,128)(2,1)} %gather_fusion), calls=%async_computation.1 | async-start | bytes 8388608 | tf_op jit(solution)/shard_map/all_to_all | solution.py:306
  37.3 1.6 %collective-permute-start = (bf16[1024,512]{1,0:T(8,128)(2,1)}, bf16[1024,512]{1,0:T(8,128)(2,1)S(1)}, u32[]{:S(2)}, u32[]{:S(2)}) collective-permute-start(bf16[1024,512]{1,0:T(8,128)(2,1)} %own_ref.1), channel_id=1, source_target_pairs={{0,1},{1,2},{2,3},{3,0},{4,5},{5,6},{6,7},{7,4},{8,9},{9,10},{10,1... | collective-permute-start | bytes 3145736 | tf_op jit(solution)/shard_map/ppermute | solution.py:292
  38.8 0.5 collective-permute-start.1
  39.4 23.2 %collective-permute-done.left_ref = bf16[1024,512]{1,0:T(8,128)(2,1)S(1)} collective-permute-done((bf16[1024,512]{1,0:T(8,128)(2,1)}, bf16[1024,512]{1,0:T(8,128)(2,1)S(1)}, u32[]{:S(2)}, u32[]{:S(2)}) %collective-permute-start) | collective-permute-done | bytes 1048608 | tf_op jit(solution)/shard_map/ppermute | solution.py:292
  62.6 1.6 %collective-permute-start.2 = (bf16[512,512]{1,0:T(8,128)(2,1)S(1)}, bf16[512,512]{1,0:T(8,128)(2,1)}, u32[]{:S(2)}, u32[]{:S(2)}) collective-permute-start(bf16[512,512]{1,0:T(8,128)(2,1)S(1)} %slice.10), channel_id=1, source_target_pairs={{0,1},{1,2},{2,3},{3,0},{4,5},{5,6},{6,7},{7,4},{8,9},{9,10},{10,1... | collective-permute-start | bytes 1572872 | tf_op jit(solution)/shard_map/ppermute | solution.py:294
  64.3 0.8 collective-permute-start.3
  65.0 10.8 %collective-permute-done.2.far0_ref = bf16[512,512]{1,0:T(8,128)(2,1)} collective-permute-done((bf16[512,512]{1,0:T(8,128)(2,1)S(1)}, bf16[512,512]{1,0:T(8,128)(2,1)}, u32[]{:S(2)}, u32[]{:S(2)}) %collective-permute-start.2) | collective-permute-done | bytes 524320 | tf_op jit(solution)/shard_map/ppermute | solution.py:294
  75.9 1.5 %collective-permute-done.3.far1_ref = bf16[512,512]{1,0:T(8,128)(2,1)} collective-permute-done((bf16[512,512]{1,0:T(8,128)(2,1)S(1)}, bf16[512,512]{1,0:T(8,128)(2,1)}, u32[]{:S(2)}, u32[]{:S(2)}) %collective-permute-start.3) | collective-permute-done | bytes 524320 | tf_op jit(solution)/shard_map/ppermute | solution.py:295
  77.4 15.5 %token_path.1 = (f32[1024,512]{1,0:T(8,128)}, f32[2,2,4,128]{3,2,1,0:T(4,128)}) custom-call(s32[1]{0:T(128)} %bitcast.me_ref, bf16[1024,512]{1,0:T(8,128)(2,1)} %own_ref.1, bf16[1024,512]{1,0:T(8,128)(2,1)} %copy-done, bf16[1024,512]{1,0:T(8,128)(2,1)} %copy-done.1, bf16[512,512]{1,0:T(8,128)(2,1)} %collective-permute-done.2.far0_ref, ...), custom_call_target="tpu_custom_call" | custom-call | flops 4294967296 | bytes 10485760 | tf_op jit(solution)/shard_map/token_path/pallas_call | solution.py:162
  92.9 0.7 copy.29
  93.6 9.9 %psum.7.stats_ref = f32[2,8,128]{2,1,0:T(8,128)} all-reduce(f32[2,8,128]{2,1,0:T(8,128)S(1)} %bitcast.17), channel_id=1, replica_groups=mesh['z'=8,'y'=4,'c'=2,'tp'=4] {'tp'}, use_global_device_ids=true, to_apply=%region_0.1 | all-reduce | flops 2048 | bytes 16384 | tf_op jit(solution)/shard_map/psum | solution.py:311
  103.4 30.1 %all-to-all-done.1.arrived_ref = bf16[64,64,512]{2,1,0:T(8,128)(2,1)} async-done(((bf16[64,64,512]{2,1,0:T(8,128)(2,1)}), bf16[64,64,512]{2,1,0:T(8,128)(2,1)}, u32[]{:S(2)}, u32[]{:S(2)}) %all-to-all-start.1) | async-done | bytes 4194336 | tf_op jit(solution)/shard_map/all_to_all | solution.py:306
  133.5 12.2 %attend.1 = bf16[1024,512]{1,0:T(8,128)(2,1)} custom-call(s32[32]{0:T(128)} %copy-done.2, f32[1024,512]{1,0:T(8,128)} %get-tuple-element.7.conv_ref, f32[2,8,128]{2,1,0:T(8,128)} %psum.7.stats_ref, f32[1,512]{1,0:T(1,128)} %bitcast.19, f32[1,512]{1,0:T(1,128)} %bitcast.20, bf16[64,64,512]{2,1,0:T(8,128)(2,1)} %all-to-all-done.1.arrived_ref), custom_call_target="tpu_custom_call" | custom-call | flops 268435456 | bytes 5242880 | tf_op jit(solution)/shard_map/attend/pallas_call | solution.py:255
  (11 shorter events, 0.1 us)
Async XLA Ops:
  0.8 28.6 %copy-start.2 = (s32[32]{0:T(128)}, s32[32]{0:T(128)S(1)}, u32[]{:S(2)}) copy-start(s32[32]{0:T(128)S(1)} %reshape.65.where_ref) | copy-start | bytes 388
  2.5 21.7 %all-to-all-start = ((s32[64,1,1]{2,1,0:T(1,128)}), s32[64,1,1]{2,1,0:T(1,128)S(1)}, u32[]{:S(2)}, u32[]{:S(2)}) async-start(s32[64,1,1]{2,1,0:T(1,128)} %copy.31), calls=%async_computation | async-start | bytes 65536 | tf_op jit(solution)/shard_map/all_to_all | solution.py:303
  29.5 104.0 %all-to-all-start.1 = ((bf16[64,64,512]{2,1,0:T(8,128)(2,1)}), bf16[64,64,512]{2,1,0:T(8,128)(2,1)}, u32[]{:S(2)}, u32[]{:S(2)}) async-start(bf16[64,64,512]{2,1,0:T(8,128)(2,1)} %gather_fusion), calls=%async_computation.1 | async-start | bytes 8388608 | tf_op jit(solution)/shard_map/all_to_all | solution.py:306
  37.3 25.3 %collective-permute-start = (bf16[1024,512]{1,0:T(8,128)(2,1)}, bf16[1024,512]{1,0:T(8,128)(2,1)S(1)}, u32[]{:S(2)}, u32[]{:S(2)}) collective-permute-start(bf16[1024,512]{1,0:T(8,128)(2,1)} %own_ref.1), channel_id=1, source_target_pairs={{0,1},{1,2},{2,3},{3,0},{4,5},{5,6},{6,7},{7,4},{8,9},{9,10},{10,1... | collective-permute-start | bytes 3145736 | tf_op jit(solution)/shard_map/ppermute | solution.py:292
  38.8 25.4 %collective-permute-start.1 = (bf16[1024,512]{1,0:T(8,128)(2,1)}, bf16[1024,512]{1,0:T(8,128)(2,1)S(1)}, u32[]{:S(2)}, u32[]{:S(2)}) collective-permute-start(bf16[1024,512]{1,0:T(8,128)(2,1)} %own_ref.1), channel_id=1, source_target_pairs={{0,3},{1,0},{2,1},{3,2},{4,7},{5,4},{6,5},{7,6},{8,11},{9,8},{10,9... | collective-permute-start | bytes 3145736 | tf_op jit(solution)/shard_map/ppermute | solution.py:293
  62.6 14.8 %copy-start = (bf16[1024,512]{1,0:T(8,128)(2,1)}, bf16[1024,512]{1,0:T(8,128)(2,1)S(1)}, u32[]{:S(2)}) copy-start(bf16[1024,512]{1,0:T(8,128)(2,1)S(1)} %collective-permute-done.left_ref) | copy-start | bytes 3145732
  62.6 13.2 %collective-permute-start.2 = (bf16[512,512]{1,0:T(8,128)(2,1)S(1)}, bf16[512,512]{1,0:T(8,128)(2,1)}, u32[]{:S(2)}, u32[]{:S(2)}) collective-permute-start(bf16[512,512]{1,0:T(8,128)(2,1)S(1)} %slice.10), channel_id=1, source_target_pairs={{0,1},{1,2},{2,3},{3,0},{4,5},{5,6},{6,7},{7,4},{8,9},{9,10},{10,1... | collective-permute-start | bytes 1572872 | tf_op jit(solution)/shard_map/ppermute | solution.py:294
  64.2 13.2 %copy-start.1 = (bf16[1024,512]{1,0:T(8,128)(2,1)}, bf16[1024,512]{1,0:T(8,128)(2,1)S(1)}, u32[]{:S(2)}) copy-start(bf16[1024,512]{1,0:T(8,128)(2,1)S(1)} %collective-permute-done.1.right_ref) | copy-start | bytes 3145732
  64.3 13.1 %collective-permute-start.3 = (bf16[512,512]{1,0:T(8,128)(2,1)S(1)}, bf16[512,512]{1,0:T(8,128)(2,1)}, u32[]{:S(2)}, u32[]{:S(2)}) collective-permute-start(bf16[512,512]{1,0:T(8,128)(2,1)S(1)} %slice.11), channel_id=1, source_target_pairs={{0,3},{1,0},{2,1},{3,2},{4,7},{5,4},{6,5},{7,6},{8,11},{9,8},{10,9... | collective-permute-start | bytes 1572872 | tf_op jit(solution)/shard_map/ppermute | solution.py:295

commit v2 on v1

--- a/solution.py
+++ b/solution.py
@@ -20,6 +20,7 @@
 ST = ("z", "y", "c")
 LEAD = 32
 ROWS_CHUNK = 64
+GROUPS = ((0, -1, 1), (-2, 2), (-3, 3), (4,))
 
 
 def ring(size, step):
@@ -184,69 +185,109 @@
     )
 
 
-def attend_kernel(
-    where_ref, conv_ref, stats_ref, gain_ref, gate_ref, arrived_ref, out_ref, held_ref, sems
-):
+def finish_kernel(conv_ref, stats_ref, gain_ref, out_ref):
+    width = conv_ref.shape[1]
+    turn = pl.program_id(0)
+    for n in range(conv_ref.shape[0] // 128):
+        at = turn * (conv_ref.shape[0] // 128) + n
+        rows = slice(n * 128, (n + 1) * 128)
+        average = stats_ref[0, pl.ds(at, 1), :] / D
+        variance = stats_ref[1, pl.ds(at, 1), :] / D - average * average
+        spread = lax.rsqrt(variance + EPSILON_NORM)
+        average = jnp.broadcast_to(average, (128, 128)).T
+        spread = jnp.broadcast_to(spread, (128, 128)).T
+        for lane in range(0, width, 128):
+            part = slice(lane, lane + 128)
+            scaled = (conv_ref[rows, part] - average) * spread * gain_ref[:, part]
+            out_ref[rows, part] = scaled * jax.nn.sigmoid(scaled)
+
+
+def finish(convolved, stats, channel_gain):
+    rows, width = convolved.shape
+    tile = 512
+    return pl.pallas_call(
+        finish_kernel,
+        grid=(rows // tile,),
+        in_specs=[
+            pl.BlockSpec((tile, width), lambda i: (i, 0)),
+            whole((2, rows // 128, 128)),
+            whole((1, width)),
+        ],
+        out_specs=pl.BlockSpec((tile, width), lambda i: (i, 0)),
+        out_shape=jax.ShapeDtypeStruct((rows, width), jnp.float32),
+        cost_estimate=pl.CostEstimate(
+            flops=8 * rows * width, transcendentals=rows * width, bytes_accessed=4 << 20
+        ),
+        name="finish",
+    )(convolved, stats, channel_gain.reshape(1, width))
+
+
+def attend_kernel(plane_ref, where_ref, conv_ref, gate_ref, *refs):
+    groups, (out_ref, held_ref, sems) = refs[:4], refs[4:]
     turn = pl.program_id(0)
     count = where_ref.shape[0]
+    here = plane_ref[0]
 
     @pl.when(turn == 0)
     def _():
         for n in range(count):
-            pltpu.make_async_copy(
-                arrived_ref.at[where_ref[n]], held_ref.at[n], sems.at[n]
-            ).start()
-
-    width = conv_ref.shape[1]
-    average = stats_ref[0, pl.ds(turn, 1), :] / D
-    variance = stats_ref[1, pl.ds(turn, 1), :] / D - average * average
-    spread = lax.rsqrt(variance + EPSILON_NORM)
-    average = jnp.broadcast_to(average, (128, 128)).T
-    spread = jnp.broadcast_to(spread, (128, 128)).T
-    pieces = []
-    for lane in range(0, width, 128):
-        scaled = (
-            (conv_ref[:, lane : lane + 128] - average) * spread * gain_ref[:, lane : lane + 128]
-        )
-        pieces.append(scaled * jax.nn.sigmoid(scaled))
-    conv_out = jnp.concatenate(pieces, axis=1)
-    queries = conv_out.astype(jnp.bfloat16)
+            owner = where_ref[n]
+            away = lax.rem(owner // 8 - here + 8, 8)
+            column = lax.rem(owner, 8)
+            for group, steps in enumerate(GROUPS):
+                for k, distance in enumerate(steps):
+
+                    @pl.when(away == distance % 8)
+                    def _():
+                        pltpu.make_async_copy(
+                            groups[group].at[column * len(steps) + k], held_ref.at[n], sems.at[n]
+                        ).start()
+
+    blocks = conv_ref.shape[0] // BLOCK
     weight = jax.nn.sigmoid(gate_ref[...])
-    for b in range(2):
-        keys, values = [], []
-        for p in range(PB):
-            n = (turn * 2 + b) * PB + p
-            pltpu.make_async_copy(arrived_ref.at[0], held_ref.at[n], sems.at[n]).wait()
-            keys.append(held_ref[n, :, :HEAD])
-            values.append(held_ref[n, :, HEAD:])
-        keys = jnp.concatenate(keys, axis=0)
-        values = jnp.concatenate(values, axis=0)
+    queries = conv_ref[...].astype(jnp.bfloat16)
+    for n in range(blocks * PB):
+        at = turn * blocks * PB + n
+        pltpu.make_async_copy(groups[0].at[0], held_ref.at[at], sems.at[at]).wait()
+    scores = []
+    for b in range(blocks):
+        held = held_ref[pl.ds((turn * blocks + b) * PB, PB)].reshape(PB * PROWS, 2 * HEAD)
         rows = slice(b * BLOCK, (b + 1) * BLOCK)
         heads = jnp.concatenate([queries[rows, :HEAD], queries[rows, HEAD:]], axis=0)
-        scores = lax.dot_general(
-            heads, keys, (((1,), (1,)), ((), ())), preferred_element_type=jnp.float32
-        ) / math.sqrt(HEAD)
-        raised = jnp.exp(scores - jnp.max(scores, axis=1, keepdims=True))
-        shares = (raised / jnp.sum(raised, axis=1, keepdims=True)).astype(jnp.bfloat16)
-        attended = jnp.dot(shares, values, preferred_element_type=jnp.float32)
+        scores.append(
+            lax.dot_general(
+                heads,
+                held[:, :HEAD],
+                (((1,), (1,)), ((), ())),
+                preferred_element_type=jnp.float32,
+            )
+            / math.sqrt(HEAD)
+        )
+    shares = []
+    for b in range(blocks):
+        raised = jnp.exp(scores[b] - jnp.max(scores[b], axis=1, keepdims=True))
+        shares.append((raised / jnp.sum(raised, axis=1, keepdims=True)).astype(jnp.bfloat16))
+    for b in range(blocks):
+        held = held_ref[pl.ds((turn * blocks + b) * PB, PB)].reshape(PB * PROWS, 2 * HEAD)
+        attended = jnp.dot(shares[b], held[:, HEAD:], preferred_element_type=jnp.float32)
         attended = jnp.concatenate([attended[:BLOCK], attended[BLOCK:]], axis=1)
-        out_ref[rows, :] = (conv_out[rows] + weight * attended).astype(jnp.bfloat16)
-
-
-def attend(where, convolved, stats, channel_gain, retrieval_gate, arrived):
-    rows, width = convolved.shape
+        rows = slice(b * BLOCK, (b + 1) * BLOCK)
+        out_ref[rows, :] = (conv_ref[rows, :] + weight * attended).astype(jnp.bfloat16)
+
+
+def attend(plane, where, conv_out, retrieval_gate, groups):
+    rows, width = conv_out.shape
     count = where.shape[0]
+    tile = 512
     grid_spec = pltpu.PrefetchScalarGridSpec(
-        num_scalar_prefetch=1,
-        grid=(rows // 128,),
+        num_scalar_prefetch=2,
+        grid=(rows // tile,),
         in_specs=[
-            pl.BlockSpec((128, width), lambda i, w: (i, 0)),
-            whole((2, rows // 128, 128)),
+            pl.BlockSpec((tile, width), lambda i, *_: (i, 0)),
             whole((1, width)),
-            whole((1, width)),
-            pl.BlockSpec(memory_space=pl.ANY),
-        ],
-        out_specs=pl.BlockSpec((128, width), lambda i, w: (i, 0)),
+        ]
+        + [pl.BlockSpec(memory_space=pl.ANY)] * len(groups),
+        out_specs=pl.BlockSpec((tile, width), lambda i, *_: (i, 0)),
         scratch_shapes=[
             pltpu.VMEM((count, PROWS, 2 * HEAD), jnp.bfloat16),
             pltpu.SemaphoreType.DMA((count,)),
@@ -258,21 +299,74 @@
         out_shape=jax.ShapeDtypeStruct((rows, width), jnp.bfloat16),
         cost_estimate=pl.CostEstimate(
             flops=4 * rows * 2 * PB * PROWS * HEAD,
-            transcendentals=2 * rows * width,
+            transcendentals=rows * 2 * PB * PROWS,
             bytes_accessed=5 << 20,
         ),
         name="attend",
-    )(
-        where,
-        convolved,
-        stats,
-        channel_gain.reshape(1, width),
-        retrieval_gate.reshape(1, width),
-        arrived,
-    )
-
-
-def body(
+    )(plane, where, conv_out, retrieval_gate.reshape(1, width), *groups)
+
+
+def pick_kernel(plane_ref, table_ref, own_ref, below_ref, above_ref, *refs):
+    outs, sems = refs[:-1], refs[-1]
+    here = plane_ref[0]
+
+    def slot(reader_plane, reader, owner_plane):
+        at = lax.rem(here + reader_plane + 8, 8) * 8 + reader
+        return table_ref[at * 8 + lax.rem(here + owner_plane + 8, 8)]
+
+    half = PROWS // 2
+    for reader in range(8):
+        for step in (1, 2):
+            for side, source in ((1, below_ref), (-1, above_ref)):
+                n = 2 * step - (1 if side == 1 else 0)
+                taken = slot(side * step, reader, -side)
+                pltpu.make_async_copy(
+                    source.at[taken], outs[n].at[reader], sems.at[n]
+                ).start()
+        for n, side, source, at in ((5, 1, below_ref, 0), (6, -1, above_ref, half)):
+            taken = slot(3 * side, reader, -side)
+            pltpu.make_async_copy(
+                source.at[taken, pl.ds(at, half)], outs[n].at[reader], sems.at[n]
+            ).start()
+    for reader in range(8):
+        for k, source in enumerate((own_ref, below_ref, above_ref)):
+            taken = slot(0, reader, (0, -1, 1)[k])
+            pltpu.make_async_copy(
+                source.at[taken], outs[0].at[reader * 3 + k], sems.at[0]
+            ).start()
+    for n, out in enumerate(outs):
+        pltpu.make_async_copy(out, out, sems.at[n]).wait()
+
+
+def pick(plane, table, own, below, above):
+    shapes = [(24, PROWS)] + [(8, PROWS)] * 4 + [(8, PROWS // 2)] * 2
+    grid_spec = pltpu.PrefetchScalarGridSpec(
+        num_scalar_prefetch=2,
+        grid=(1,),
+        in_specs=[pl.BlockSpec(memory_space=pl.ANY)] * 3,
+        out_specs=[pl.BlockSpec(memory_space=pl.ANY)] * len(shapes),
+        scratch_shapes=[pltpu.SemaphoreType.DMA((len(shapes),))],
+    )
+    return pl.pallas_call(
+        pick_kernel,
+        grid_spec=grid_spec,
+        out_shape=[
+            jax.ShapeDtypeStruct((*shape, 2 * HEAD), jnp.bfloat16) for shape in shapes
+        ],
+        cost_estimate=pl.CostEstimate(flops=0, transcendentals=0, bytes_accessed=8 << 20),
+        name="pick",
+    )(plane, table, own, below, above)
+
+
+def shift(value, axis, step):
+    return lax.ppermute(value, axis, ring(lax.axis_size(axis), step))
+
+
+def exchange(value, axes):
+    return lax.all_to_all(value, axes, split_axis=0, concat_axis=0, tiled=True)
+
+
+def layer(
     tokens,
     token_gain,
     inner_weight,
@@ -287,30 +381,61 @@
     owners,
     local_slots,
 ):
-    st = lax.axis_size(ST)
     me = lax.axis_index("tp").astype(jnp.int32).reshape(1)
-    left = lax.ppermute(tokens, "tp", ring(4, 1))
-    right = lax.ppermute(tokens, "tp", ring(4, -1))
-    far0 = lax.ppermute(left[:LENGTH], "tp", ring(4, 1))
-    far1 = lax.ppermute(right[LENGTH:], "tp", ring(4, -1))
+    plane = lax.axis_index("z").astype(jnp.int32).reshape(1)
+    left = shift(tokens, "tp", 1)
+    right = shift(tokens, "tp", -1)
+    far0 = shift(left[:LENGTH], "tp", 1)
+    far1 = shift(right[LENGTH:], "tp", -1)
+
+    own = project_passages(passage_store, passage_gain, keys_weight, values_weight)
+    own = own.reshape(-1, PROWS, 2 * HEAD)
+    below = shift(own, "z", 1)
+    above = shift(own, "z", -1)
 
     asked = owners.reshape(-1)
     slots = local_slots.reshape(-1)
     wanted = jnp.sum(
-        jnp.where(asked[:, None] == jnp.arange(st, dtype=jnp.int32)[None, :], slots[:, None], 0),
+        jnp.where(asked[:, None] == jnp.arange(64, dtype=jnp.int32)[None, :], slots[:, None], 0),
         axis=0,
     )
-    sent = lax.all_to_all(wanted[:, None], ST, split_axis=0, concat_axis=0, tiled=True)
-    own = project_passages(passage_store, passage_gain, keys_weight, values_weight)
-    own = own.reshape(-1, PROWS, 2 * HEAD)
-    arrived = lax.all_to_all(own[sent[:, 0]], ST, split_axis=0, concat_axis=0, tiled=True)
+    wanted = jnp.broadcast_to(wanted.reshape(1, 8, 8).transpose(0, 2, 1), (8, 8, 8))
+    table = exchange(wanted.reshape(64, 8), ST)
+
+    near, up1, down1, up2, down2, up3, down3 = pick(
+        plane, table.reshape(-1), own, below, above
+    )
+    up3 = shift(up3, "z", 3)
+    down3 = shift(down3, "z", -3)
+    up1 = shift(up1, "z", 1)
+    down1 = shift(down1, "z", -1)
+    up2 = shift(up2, "z", 2)
+    down2 = shift(down2, "z", -2)
+    side = ("y", "c")
+    groups = [
+        exchange(near.reshape(8, 3 * PROWS, -1), side),
+        exchange(jnp.concatenate([up1, down1], axis=1), side),
+        exchange(jnp.concatenate([up2, down2], axis=1), side),
+        exchange(jnp.concatenate([up3, down3], axis=1), side),
+    ]
+    groups = [group.reshape(-1, PROWS, 2 * HEAD) for group in groups]
 
     convolved, stats = token_path(
-        me, tokens, left, right, far0, far1, token_gain, inner_weight, gating_weight, filter_taps
+        me,
+        tokens,
+        left,
+        right,
+        far0,
+        far1,
+        token_gain,
+        inner_weight,
+        gating_weight,
+        filter_taps,
     )
     stats = lax.psum(stats, "tp")
     stats = stats.transpose(1, 0, 2, 3).reshape(2, -1, 128)
-    return attend(asked, convolved, stats, channel_gain, retrieval_gate, arrived)
+    conv_out = finish(convolved, stats, channel_gain)
+    return attend(plane, asked, conv_out, retrieval_gate, groups)
 
 
 def solution(mesh):
@@ -331,6 +456,4 @@
         P(ST, None),
         P(ST, None),
     )
-    return jax.shard_map(
-        body, mesh=fine, in_specs=placed, out_specs=P(ST, "tp"), check_vma=False
-    )
+    return jax.shard_map(layer, mesh=fine, in_specs=placed, out_specs=P(ST, "tp"), check_vma=False)

time: 146 us -> 314 us (2.15); the launches traced: 146 us -> 311 us
  Pallas kernels: 34.5 us -> 160 us
  starting transfers between devices: 24.4 us -> 40.9 us
  blocking collectives: 9.86 us -> 22.8 us
  waiting for transfers between devices: 68.4 us -> 75.4 us
    pallas_call x0 -> x2, Pallas kernels: none -> 132 us  [the longest x1 129 us: pick(): pl.pallas_call(pick_kernel, grid_spec=grid_spec, out_shape=[jax.ShapeDtyp...]
    ppermute x4 -> x12, waiting for transfers between devices: 35.6 us -> 53.6 us  [shift(): return lax.ppermute(value, axis, ring(lax.axis_size(axis), step))]
    ppermute x4 -> x12, starting transfers between devices: 4.46 us -> 19.8 us  [shift(): return lax.ppermute(value, axis, ring(lax.axis_size(axis), step))]
    all_to_all x0 -> x1, blocking collectives: none -> 13.6 us  [exchange(): return lax.all_to_all(value, axes, split_axis=0, concat_axis=0, tiled=True)]
    all_to_all x2 -> x4, waiting for transfers between devices: 32.9 us -> 21.7 us  [exchange(): return lax.all_to_all(value, axes, split_axis=0, concat_axis=0, tiled=True)]
    pallas_call x1, Pallas kernels: 12.2 us -> 5.61 us  [attend(): pl.pallas_call(attend_kernel, grid_spec=grid_spec, out_shape=jax.ShapeDty...]
    gather x1 -> x0, local copies, waits for them, and re-layouts: 4.01 us -> none  [body(): own[sent[:, 0]]]
    all_to_all x2 -> x4, starting transfers between devices: 19.9 us -> 21.1 us  [exchange(): return lax.all_to_all(value, axes, split_axis=0, concat_axis=0, tiled=True)]
  transfers between devices with their start and end apart: 6 -> 16, of which waited for: 5 -> 8; matrix products, arithmetic and copies ran while one was open for 1% -> 3% of each run, Pallas kernels for 15% -> 6%
where the time goes in v2:
time: 314 us; the launch traced here: 311 us
  Pallas kernels  160 us (51%)
  waiting for transfers between devices  75.4 us (24%)
  starting transfers between devices  40.9 us (13%)
  blocking collectives  22.8 us (7%)
  local copies, waits for them, and re-layouts  8.37 us (3%)
    pallas_call x1, Pallas kernels, pick(): pl.pallas_call(pick_kernel, grid_spec=grid_spec, out_shape=[jax.ShapeDtyp...  129 us
    ppermute x12, waiting for transfers between devices, shift(): return lax.ppermute(value, axis, ring(lax.axis_size(axis), step))  53.6 us
    all_to_all x4, waiting for transfers between devices, exchange(): return lax.all_to_all(value, axes, split_axis=0, concat_axis=0, tiled=True)  21.7 us
    all_to_all x4, starting transfers between devices, exchange(): return lax.all_to_all(value, axes, split_axis=0, concat_axis=0, tiled=True)  21.1 us
    ppermute x12, starting transfers between devices, shift(): return lax.ppermute(value, axis, ring(lax.axis_size(axis), step))  19.8 us
    pallas_call x1, Pallas kernels, token_path(): pl.pallas_call(token_kernel, grid_spec=grid_spec, out_shape=[jax.ShapeDty...  15.6 us
    all_to_all x1, blocking collectives, exchange(): return lax.all_to_all(value, axes, split_axis=0, concat_axis=0, tiled=True)  13.6 us
    psum x1, blocking collectives, layer(): stats = lax.psum(stats, 'tp')  9.26 us
  transfers between devices with their start and end apart: 16, of which 8 were waited for; matrix products, arithmetic and copies ran while one was open for 3% of the time, Pallas kernels for 6%

profile of v2, /device:TPU:2, one launch (start us, length us, event | category | flops | bytes accessed | tf_op | source)
XLA Modules:
  0.0 310.7 jit_solution(11841016507549240674)
XLA Ops:
  0.0 6.8 %project_passages.1 = bf16[1024,512]{1,0:T(8,128)(2,1)} custom-call(bf16[1024,2048]{1,0:T(8,128)(2,1)} %bitcast.31, f32[1,2048]{1,0:T(1,128)} %bitcast.34, bf16[2048,256]{1,0:T(8,128)(2,1)} %keys_ref.1, bf16[2048,256]{1,0:T(8,128)(2,1)} %values_ref.1), custom_call_target="tpu_custom_call" | custom-call | flops 2147483648 | bytes 7340032 | tf_op jit(solution)/shard_map/project_passages/pallas_call | solution.py:50
  6.8 1.9 collective-permute-start.4
  8.8 4.0 %collective-permute-start.5 = (bf16[16,64,512]{2,1,0:T(8,128)(2,1)}, bf16[16,64,512]{2,1,0:T(8,128)(2,1)S(1)}, u32[]{:S(2)}, u32[]{:S(2)}) collective-permute-start(bf16[16,64,512]{2,1,0:T(8,128)(2,1)} %bitcast.23), channel_id=1, source_target_pairs={{0,224},{32,0},{64,32},{96,64},{128,96},{160,128},{192,160},{224,1... | collective-permute-start | bytes 3145736 | tf_op jit(solution)/shard_map/ppermute | solution.py:362
  13.9 9.5 %all-to-all-start = ((s32[64,1,8]{2,1,0:T(1,128)}), s32[64,1,8]{2,1,0:T(1,128)S(1)}, u32[]{:S(2)}, u32[]{:S(2)}) async-start(s32[64,1,8]{2,1,0:T(1,128)} %bitcast.11), calls=%async_computation | async-start | bytes 65536 | tf_op jit(solution)/shard_map/all_to_all | solution.py:366
  23.4 17.7 %all-to-all-done = s32[64,1,8]{2,1,0:T(1,128)S(1)} async-done(((s32[64,1,8]{2,1,0:T(1,128)}), s32[64,1,8]{2,1,0:T(1,128)S(1)}, u32[]{:S(2)}, u32[]{:S(2)}) %all-to-all-start) | async-done | bytes 2080 | tf_op jit(solution)/shard_map/all_to_all | solution.py:366
  44.5 128.9 %pick.1 = (bf16[24,64,512]{2,1,0:T(8,128)(2,1)}, bf16[8,64,512]{2,1,0:T(8,128)(2,1)}, bf16[8,64,512]{2,1,0:T(8,128)(2,1)}, bf16[8,64,512]{2,1,0:T(8,128)(2,1)}, ...) custom-call(s32[1]{0:T(128)} %bitcast.plane_ref, s32[512]{0:T(512)} %reshape.71.table_ref, ...), custom_call_target="tpu_custom_call" | custom-call | bytes 8388608 | tf_op jit(solution)/shard_map/pick/pallas_call | solution.py:350
  173.5 2.9 collective-permute-start.11
  177.4 15.9 %collective-permute-done.11 = bf16[8,32,512]{2,1,0:T(8,128)(2,1)S(1)} collective-permute-done((bf16[8,32,512]{2,1,0:T(8,128)(2,1)}, bf16[8,32,512]{2,1,0:T(8,128)(2,1)S(1)}, u32[]{:S(2)}, u32[]{:S(2)}) %collective-permute-start.11) | collective-permute-done | bytes 262176 | tf_op jit(solution)/shard_map/ppermute | solution.py:362
  193.2 4.4 %collective-permute-done.10 = bf16[8,32,512]{2,1,0:T(8,128)(2,1)S(1)} collective-permute-done((bf16[8,32,512]{2,1,0:T(8,128)(2,1)}, bf16[8,32,512]{2,1,0:T(8,128)(2,1)S(1)}, u32[]{:S(2)}, u32[]{:S(2)}) %collective-permute-start.10) | collective-permute-done | bytes 262176 | tf_op jit(solution)/shard_map/ppermute | solution.py:362
  197.7 13.6 %all_to_all.29.refs_3_ = bf16[8,64,512]{2,1,0:T(8,128)(2,1)} all-to-all(bf16[8,64,512]{2,1,0:T(8,128)(2,1)S(1)} %pad_maximum_fusion.2), channel_id=1, replica_groups=mesh['z'=8,'y'=4,'c'=2,'tp'=4] {'y','c'}, dimensions={0} | all-to-all | bytes 1048576 | tf_op jit(solution)/shard_map/all_to_all | solution.py:366
  211.3 3.6 %all-to-all-start.1 = ((bf16[8,192,512]{2,1,0:T(8,128)(2,1)}), bf16[8,192,512]{2,1,0:T(8,128)(2,1)S(1)}, u32[]{:S(2)}, u32[]{:S(2)}) async-start(bf16[8,192,512]{2,1,0:T(8,128)(2,1)} %bitcast.15), calls=%async_computation.1 | async-start | bytes 3145728 | tf_op jit(solution)/shard_map/all_to_all | solution.py:366
  215.1 2.1 collective-permute-start.6
  219.2 10.3 %collective-permute-done.7 = bf16[8,64,512]{2,1,0:T(8,128)(2,1)S(1)} collective-permute-done((bf16[8,64,512]{2,1,0:T(8,128)(2,1)S(1)}, bf16[8,64,512]{2,1,0:T(8,128)(2,1)S(1)}, u32[]{:S(2)}, u32[]{:S(2)}) %collective-permute-start.7) | collective-permute-done | bytes 524320 | tf_op jit(solution)/shard_map/ppermute | solution.py:362
  232.3 4.0 %all-to-all-done.1 = bf16[8,192,512]{2,1,0:T(8,128)(2,1)S(1)} async-done(((bf16[8,192,512]{2,1,0:T(8,128)(2,1)}), bf16[8,192,512]{2,1,0:T(8,128)(2,1)S(1)}, u32[]{:S(2)}, u32[]{:S(2)}) %all-to-all-start.1) | async-done | bytes 1572896 | tf_op jit(solution)/shard_map/all_to_all | solution.py:366
  236.4 3.6 %all-to-all-start.2 = ((bf16[8,128,512]{2,1,0:T(8,128)(2,1)}), bf16[8,128,512]{2,1,0:T(8,128)(2,1)S(1)}, u32[]{:S(2)}, u32[]{:S(2)}) async-start(bf16[8,128,512]{2,1,0:T(8,128)(2,1)} %pad_maximum_fusion), calls=%async_computation.2 | async-start | bytes 2097152 | tf_op jit(solution)/shard_map/all_to_all | solution.py:366
  239.9 3.7 %collective-permute-start.9 = (bf16[8,64,512]{2,1,0:T(8,128)(2,1)}, bf16[8,64,512]{2,1,0:T(8,128)(2,1)S(1)}, u32[]{:S(2)}, u32[]{:S(2)}) collective-permute-start(bf16[8,64,512]{2,1,0:T(8,128)(2,1)} %get-tuple-element.20), channel_id=1, source_target_pairs={{0,192},{32,224},{64,0},{96,32},{128,64},{160,96},{192,128},{224,1... | collective-permute-start | bytes 1572872 | tf_op jit(solution)/shard_map/ppermute | solution.py:362
  246.3 1.9 slice.9
  248.7 17.7 %collective-permute-done.9 = bf16[8,64,512]{2,1,0:T(8,128)(2,1)S(1)} collective-permute-done((bf16[8,64,512]{2,1,0:T(8,128)(2,1)}, bf16[8,64,512]{2,1,0:T(8,128)(2,1)S(1)}, u32[]{:S(2)}, u32[]{:S(2)}) %collective-permute-start.9) | collective-permute-done | bytes 524320 | tf_op jit(solution)/shard_map/ppermute | solution.py:362
  266.4 3.5 %collective-permute-done.8 = bf16[8,64,512]{2,1,0:T(8,128)(2,1)S(1)} collective-permute-done((bf16[8,64,512]{2,1,0:T(8,128)(2,1)}, bf16[8,64,512]{2,1,0:T(8,128)(2,1)S(1)}, u32[]{:S(2)}, u32[]{:S(2)}) %collective-permute-start.8) | collective-permute-done | bytes 524320 | tf_op jit(solution)/shard_map/ppermute | solution.py:362
  271.0 4.4 %all-to-all-start.3 = ((bf16[8,128,512]{2,1,0:T(8,128)(2,1)}), bf16[8,128,512]{2,1,0:T(8,128)(2,1)S(1)}, u32[]{:S(2)}, u32[]{:S(2)}) async-start(bf16[8,128,512]{2,1,0:T(8,128)(2,1)} %pad_maximum_fusion.1), calls=%async_computation.3 | async-start | bytes 2097152 | tf_op jit(solution)/shard_map/all_to_all | solution.py:366
  275.4 15.6 %token_path.1 = (f32[1024,512]{1,0:T(8,128)}, f32[2,2,4,128]{3,2,1,0:T(4,128)}) custom-call(s32[1]{0:T(128)} %bitcast.1.me_ref, bf16[1024,512]{1,0:T(8,128)(2,1)} %own_ref.1, bf16[1024,512]{1,0:T(8,128)(2,1)} %collective-permute-done.left_ref, bf16[1024,512]{1,0:T(8,128)(2,1)} %collective-permute-done.1.right_ref, ...), custom_call_target="tpu_custom_call" | custom-call | flops 4294967296 | bytes 10485760 | tf_op jit(solution)/shard_map/token_path/pallas_call | solution.py:163
  291.7 9.3 %psum.7.stats_ref = f32[2,8,128]{2,1,0:T(8,128)} all-reduce(f32[2,8,128]{2,1,0:T(8,128)S(1)} %bitcast.25), channel_id=1, replica_groups=mesh['z'=8,'y'=4,'c'=2,'tp'=4] {'tp'}, use_global_device_ids=true, to_apply=%region_0.1 | all-reduce | flops 2048 | bytes 16384 | tf_op jit(solution)/shard_map/psum | solution.py:435
  301.0 2.9 finish.1.conv_ref
  304.9 5.6 %attend.1 = bf16[1024,512]{1,0:T(8,128)(2,1)} custom-call(s32[1]{0:T(128)} %bitcast.plane_ref, s32[32]{0:T(128)} %copy-done.5, f32[1024,512]{1,0:T(8,128)} %finish.1.conv_ref, f32[1,512]{1,0:T(1,128)} %bitcast.30, bf16[24,64,512]{2,1,0:T(8,128)(2,1)} %bitcast.19, bf16[16,64,512]{2,1,0:T(8,128)(2,1)} %bitcast.20, bf16[16,64,512]{2,1,0:T(8,128)(2,1)} %bitcast.21, ...), custom_call_target="tpu_custom_call" | custom-call | flops 268435456 | bytes 5242880 | tf_op jit(solution)/shard_map/attend/pallas_call | solution.py:296
  (52 shorter events, 16.6 us)
Async XLA Ops:
  0.0 12.7 %copy-start.6 = (s32[16,2]{0,1:T(2,128)S(1)}, s32[16,2]{0,1:T(2,128)}, u32[]{:S(2)}) copy-start(s32[16,2]{0,1:T(2,128)} %param.24) | copy-start | bytes 388
  0.0 12.9 %copy-start.7 = (s32[16,2]{0,1:T(2,128)S(1)}, s32[16,2]{0,1:T(2,128)}, u32[]{:S(2)}) copy-start(s32[16,2]{0,1:T(2,128)} %param.25) | copy-start | bytes 388
  6.8 36.3 %collective-permute-start.4 = (bf16[16,64,512]{2,1,0:T(8,128)(2,1)}, bf16[16,64,512]{2,1,0:T(8,128)(2,1)S(1)}, u32[]{:S(2)}, u32[]{:S(2)}) collective-permute-start(bf16[16,64,512]{2,1,0:T(8,128)(2,1)} %bitcast.22), channel_id=1, source_target_pairs={{0,32},{32,64},{64,96},{96,128},{128,160},{160,192},{192,224},{224... | collective-permute-start | bytes 3145736 | tf_op jit(solution)/shard_map/ppermute | solution.py:362
  8.8 34.4 %collective-permute-start.5 = (bf16[16,64,512]{2,1,0:T(8,128)(2,1)}, bf16[16,64,512]{2,1,0:T(8,128)(2,1)S(1)}, u32[]{:S(2)}, u32[]{:S(2)}) collective-permute-start(bf16[16,64,512]{2,1,0:T(8,128)(2,1)} %bitcast.23), channel_id=1, source_target_pairs={{0,224},{32,0},{64,32},{96,64},{128,96},{160,128},{192,160},{224,1... | collective-permute-start | bytes 3145736 | tf_op jit(solution)/shard_map/ppermute | solution.py:362
  12.9 184.8 %copy-start.5 = (s32[32]{0:T(128)}, s32[32]{0:T(128)S(1)}, u32[]{:S(2)}) copy-start(s32[32]{0:T(128)S(1)} %reshape.62.where_ref) | copy-start | bytes 388
  13.9 27.2 %all-to-all-start = ((s32[64,1,8]{2,1,0:T(1,128)}), s32[64,1,8]{2,1,0:T(1,128)S(1)}, u32[]{:S(2)}, u32[]{:S(2)}) async-start(s32[64,1,8]{2,1,0:T(1,128)} %bitcast.11), calls=%async_computation | async-start | bytes 65536 | tf_op jit(solution)/shard_map/all_to_all | solution.py:366
  43.2 1.3 copy-start.4
  173.5 19.8 %collective-permute-start.11 = (bf16[8,32,512]{2,1,0:T(8,128)(2,1)}, bf16[8,32,512]{2,1,0:T(8,128)(2,1)S(1)}, u32[]{:S(2)}, u32[]{:S(2)}) collective-permute-start(bf16[8,32,512]{2,1,0:T(8,128)(2,1)} %get-tuple-element.22), channel_id=1, source_target_pairs={{0,160},{32,192},{64,224},{96,0},{128,32},{160,64},{192,96},{224,1... | collective-permute-start | bytes 786440 | tf_op jit(solution)/shard_map/ppermute | solution.py:362
  176.4 21.3 %collective-permute-start.10 = (bf16[8,32,512]{2,1,0:T(8,128)(2,1)}, bf16[8,32,512]{2,1,0:T(8,128)(2,1)S(1)}, u32[]{:S(2)}, u32[]{:S(2)}) collective-permute-start(bf16[8,32,512]{2,1,0:T(8,128)(2,1)} %get-tuple-element.21), channel_id=1, source_target_pairs={{0,96},{32,128},{64,160},{96,192},{128,224},{160,0},{192,32},{224,... | collective-permute-start | bytes 786440 | tf_op jit(solution)/shard_map/ppermute | solution.py:362
  197.7 17.2 %copy-start.9 = (bf16[8,64,512]{2,1,0:T(8,128)(2,1)S(1)}, bf16[8,64,512]{2,1,0:T(8,128)(2,1)}, u32[]{:S(2)}) copy-start(bf16[8,64,512]{2,1,0:T(8,128)(2,1)} %get-tuple-element.18) | copy-start | bytes 1572868
  197.7 17.3 %copy-start.8 = (bf16[8,64,512]{2,1,0:T(8,128)(2,1)S(1)}, bf16[8,64,512]{2,1,0:T(8,128)(2,1)}, u32[]{:S(2)}) copy-start(bf16[8,64,512]{2,1,0:T(8,128)(2,1)} %get-tuple-element.17) | copy-start | bytes 1572868
  211.3 25.1 %all-to-all-start.1 = ((bf16[8,192,512]{2,1,0:T(8,128)(2,1)}), bf16[8,192,512]{2,1,0:T(8,128)(2,1)S(1)}, u32[]{:S(2)}, u32[]{:S(2)}) async-start(bf16[8,192,512]{2,1,0:T(8,128)(2,1)} %bitcast.15), calls=%async_computation.1 | async-start | bytes 3145728 | tf_op jit(solution)/shard_map/all_to_all | solution.py:366
  214.9 14.5 %collective-permute-start.7 = (bf16[8,64,512]{2,1,0:T(8,128)(2,1)S(1)}, bf16[8,64,512]{2,1,0:T(8,128)(2,1)S(1)}, u32[]{:S(2)}, u32[]{:S(2)}) collective-permute-start(bf16[8,64,512]{2,1,0:T(8,128)(2,1)S(1)} %copy-done.9), channel_id=1, source_target_pairs={{0,224},{32,0},{64,32},{96,64},{128,96},{160,128},{192,160},{224,1... | collective-permute-start | bytes 1572872 | tf_op jit(solution)/shard_map/ppermute | solution.py:362
  215.1 16.2 %collective-permute-start.6 = (bf16[8,64,512]{2,1,0:T(8,128)(2,1)S(1)}, bf16[8,64,512]{2,1,0:T(8,128)(2,1)S(1)}, u32[]{:S(2)}, u32[]{:S(2)}) collective-permute-start(bf16[8,64,512]{2,1,0:T(8,128)(2,1)S(1)} %copy-done.8), channel_id=1, source_target_pairs={{0,32},{32,64},{64,96},{96,128},{128,160},{160,192},{192,224},{224... | collective-permute-start | bytes 1572872 | tf_op jit(solution)/shard_map/ppermute | solution.py:362
  217.1 26.5 %collective-permute-start = (bf16[1024,512]{1,0:T(8,128)(2,1)}, bf16[1024,512]{1,0:T(8,128)(2,1)}, u32[]{:S(2)}, u32[]{:S(2)}) collective-permute-start(bf16[1024,512]{1,0:T(8,128)(2,1)} %own_ref.1), channel_id=1, source_target_pairs={{0,1},{1,2},{2,3},{3,0},{4,5},{5,6},{6,7},{7,4},{8,9},{9,10},{10,1... | collective-permute-start | bytes 3145736 | tf_op jit(solution)/shard_map/ppermute | solution.py:362
  218.6 27.7 %collective-permute-start.1 = (bf16[1024,512]{1,0:T(8,128)(2,1)}, bf16[1024,512]{1,0:T(8,128)(2,1)}, u32[]{:S(2)}, u32[]{:S(2)}) collective-permute-start(bf16[1024,512]{1,0:T(8,128)(2,1)} %own_ref.1), channel_id=1, source_target_pairs={{0,3},{1,0},{2,1},{3,2},{4,7},{5,4},{6,5},{7,6},{8,11},{9,8},{10,9... | collective-permute-start | bytes 3145736 | tf_op jit(solution)/shard_map/ppermute | solution.py:362
  236.4 11.8 %copy-start = (bf16[8,192,512]{2,1,0:T(8,128)(2,1)}, bf16[8,192,512]{2,1,0:T(8,128)(2,1)S(1)}, u32[]{:S(2)}) copy-start(bf16[8,192,512]{2,1,0:T(8,128)(2,1)S(1)} %all-to-all-done.1) | copy-start | bytes 4718596
  236.4 34.6 %all-to-all-start.2 = ((bf16[8,128,512]{2,1,0:T(8,128)(2,1)}), bf16[8,128,512]{2,1,0:T(8,128)(2,1)S(1)}, u32[]{:S(2)}, u32[]{:S(2)}) async-start(bf16[8,128,512]{2,1,0:T(8,128)(2,1)} %pad_maximum_fusion), calls=%async_computation.2 | async-start | bytes 2097152 | tf_op jit(solution)/shard_map/all_to_all | solution.py:366
  239.9 26.5 %collective-permute-start.9 = (bf16[8,64,512]{2,1,0:T(8,128)(2,1)}, bf16[8,64,512]{2,1,0:T(8,128)(2,1)S(1)}, u32[]{:S(2)}, u32[]{:S(2)}) collective-permute-start(bf16[8,64,512]{2,1,0:T(8,128)(2,1)} %get-tuple-element.20), channel_id=1, source_target_pairs={{0,192},{32,224},{64,0},{96,32},{128,64},{160,96},{192,128},{224,1... | collective-permute-start | bytes 1572872 | tf_op jit(solution)/shard_map/ppermute | solution.py:362
  243.6 26.3 %collective-permute-start.8 = (bf16[8,64,512]{2,1,0:T(8,128)(2,1)}, bf16[8,64,512]{2,1,0:T(8,128)(2,1)S(1)}, u32[]{:S(2)}, u32[]{:S(2)}) collective-permute-start(bf16[8,64,512]{2,1,0:T(8,128)(2,1)} %get-tuple-element.19), channel_id=1, source_target_pairs={{0,64},{32,96},{64,128},{96,160},{128,192},{160,224},{192,0},{224,... | collective-permute-start | bytes 1572872 | tf_op jit(solution)/shard_map/ppermute | solution.py:362
  244.7 30.7 %collective-permute-start.2 = (bf16[512,512]{1,0:T(8,128)(2,1)S(1)}, bf16[512,512]{1,0:T(8,128)(2,1)}, u32[]{:S(2)}, u32[]{:S(2)}) collective-permute-start(bf16[512,512]{1,0:T(8,128)(2,1)S(1)} %slice.8), channel_id=1, source_target_pairs={{0,1},{1,2},{2,3},{3,0},{4,5},{5,6},{6,7},{7,4},{8,9},{9,10},{10,1... | collective-permute-start | bytes 1572872 | tf_op jit(solution)/shard_map/ppermute | solution.py:362
  248.2 27.2 %collective-permute-start.3 = (bf16[512,512]{1,0:T(8,128)(2,1)}, bf16[512,512]{1,0:T(8,128)(2,1)}, u32[]{:S(2)}, u32[]{:S(2)}) collective-permute-start(bf16[512,512]{1,0:T(8,128)(2,1)} %slice.9), channel_id=1, source_target_pairs={{0,3},{1,0},{2,1},{3,2},{4,7},{5,4},{6,5},{7,6},{8,11},{9,8},{10,9... | collective-permute-start | bytes 1572872 | tf_op jit(solution)/shard_map/ppermute | solution.py:362
  271.0 20.0 %copy-start.1 = (bf16[8,128,512]{2,1,0:T(8,128)(2,1)}, bf16[8,128,512]{2,1,0:T(8,128)(2,1)S(1)}, u32[]{:S(2)}) copy-start(bf16[8,128,512]{2,1,0:T(8,128)(2,1)S(1)} %all-to-all-done.2) | copy-start | bytes 3145732
  271.0 32.9 %all-to-all-start.3 = ((bf16[8,128,512]{2,1,0:T(8,128)(2,1)}), bf16[8,128,512]{2,1,0:T(8,128)(2,1)S(1)}, u32[]{:S(2)}, u32[]{:S(2)}) async-start(bf16[8,128,512]{2,1,0:T(8,128)(2,1)} %pad_maximum_fusion.1), calls=%async_computation.3 | async-start | bytes 2097152 | tf_op jit(solution)/shard_map/all_to_all | solution.py:366
  (2 other events, 2.0 us)

commit v3 on v2

--- a/solution.py
+++ b/solution.py
@@ -20,7 +20,6 @@
 ST = ("z", "y", "c")
 LEAD = 32
 ROWS_CHUNK = 64
-GROUPS = ((0, -1, 1), (-2, 2), (-3, 3), (4,))
 
 
 def ring(size, step):
@@ -223,10 +222,11 @@
 
 
 def attend_kernel(plane_ref, where_ref, conv_ref, gate_ref, *refs):
-    groups, (out_ref, held_ref, sems) = refs[:4], refs[4:]
+    near_ref, far_ref, upper_ref, lower_ref, out_ref, held_ref, sems = refs
     turn = pl.program_id(0)
     count = where_ref.shape[0]
     here = plane_ref[0]
+    half = PROWS // 2
 
     @pl.when(turn == 0)
     def _():
@@ -234,21 +234,41 @@
             owner = where_ref[n]
             away = lax.rem(owner // 8 - here + 8, 8)
             column = lax.rem(owner, 8)
-            for group, steps in enumerate(GROUPS):
-                for k, distance in enumerate(steps):
-
-                    @pl.when(away == distance % 8)
-                    def _():
-                        pltpu.make_async_copy(
-                            groups[group].at[column * len(steps) + k], held_ref.at[n], sems.at[n]
-                        ).start()
+            close = (away <= 1) | (away == 7)
+
+            @pl.when(close)
+            def _():
+                k = jnp.where(away == 7, 1, 2 * away)
+                at = pl.multiple_of(k * PROWS, PROWS)
+                pltpu.make_async_copy(
+                    near_ref.at[column, pl.ds(at, PROWS)], held_ref.at[n], sems.at[n]
+                ).start()
+
+            @pl.when(away == 4)
+            def _():
+                pltpu.make_async_copy(
+                    upper_ref.at[column], held_ref.at[n, pl.ds(0, half)], sems.at[n]
+                ).start()
+                pltpu.make_async_copy(
+                    lower_ref.at[column], held_ref.at[n, pl.ds(half, half)], sems.at[n]
+                ).start()
+
+            @pl.when(jnp.logical_not(close) & (away != 4))
+            def _():
+                k = jnp.where(away < 4, 2 * away - 3, 12 - 2 * away)
+                at = pl.multiple_of(k * PROWS, PROWS)
+                pltpu.make_async_copy(
+                    far_ref.at[column, pl.ds(at, PROWS)], held_ref.at[n], sems.at[n]
+                ).start()
 
     blocks = conv_ref.shape[0] // BLOCK
     weight = jax.nn.sigmoid(gate_ref[...])
     queries = conv_ref[...].astype(jnp.bfloat16)
     for n in range(blocks * PB):
         at = turn * blocks * PB + n
-        pltpu.make_async_copy(groups[0].at[0], held_ref.at[at], sems.at[at]).wait()
+        pltpu.make_async_copy(
+            far_ref.at[0, pl.ds(0, PROWS)], held_ref.at[at], sems.at[at]
+        ).wait()
     scores = []
     for b in range(blocks):
         held = held_ref[pl.ds((turn * blocks + b) * PB, PB)].reshape(PB * PROWS, 2 * HEAD)
@@ -309,53 +329,71 @@
 def pick_kernel(plane_ref, table_ref, own_ref, below_ref, above_ref, *refs):
     outs, sems = refs[:-1], refs[-1]
     here = plane_ref[0]
+    half = PROWS // 2
 
     def slot(reader_plane, reader, owner_plane):
         at = lax.rem(here + reader_plane + 8, 8) * 8 + reader
-        return table_ref[at * 8 + lax.rem(here + owner_plane + 8, 8)]
-
-    half = PROWS // 2
+        return table_ref[at, lax.rem(here + owner_plane + 8, 8)]
+
     for reader in range(8):
-        for step in (1, 2):
-            for side, source in ((1, below_ref), (-1, above_ref)):
-                n = 2 * step - (1 if side == 1 else 0)
-                taken = slot(side * step, reader, -side)
-                pltpu.make_async_copy(
-                    source.at[taken], outs[n].at[reader], sems.at[n]
-                ).start()
-        for n, side, source, at in ((5, 1, below_ref, 0), (6, -1, above_ref, half)):
-            taken = slot(3 * side, reader, -side)
+        for k, (source, owner_plane) in enumerate(((own_ref, 0), (below_ref, -1), (above_ref, 1))):
             pltpu.make_async_copy(
-                source.at[taken, pl.ds(at, half)], outs[n].at[reader], sems.at[n]
+                source.at[slot(0, reader, owner_plane)],
+                outs[0].at[reader, pl.ds(k * PROWS, PROWS)],
+                sems.at[0],
+            ).start()
+        for source, side, at in ((below_ref, 1, 0), (above_ref, -1, half)):
+            pltpu.make_async_copy(
+                source.at[slot(3 * side, reader, -side), pl.ds(at, half)],
+                outs[0].at[reader, pl.ds(3 * PROWS + at, half)],
+                sems.at[0],
             ).start()
     for reader in range(8):
-        for k, source in enumerate((own_ref, below_ref, above_ref)):
-            taken = slot(0, reader, (0, -1, 1)[k])
+        for n, (source, side, steps) in enumerate(
+            ((below_ref, 1, 1), (above_ref, -1, 1), (below_ref, 1, 2), (above_ref, -1, 2))
+        ):
             pltpu.make_async_copy(
-                source.at[taken], outs[0].at[reader * 3 + k], sems.at[0]
+                source.at[slot(side * steps, reader, -side)],
+                outs[1 + n].at[reader],
+                sems.at[1 + n],
             ).start()
     for n, out in enumerate(outs):
         pltpu.make_async_copy(out, out, sems.at[n]).wait()
 
 
 def pick(plane, table, own, below, above):
-    shapes = [(24, PROWS)] + [(8, PROWS)] * 4 + [(8, PROWS // 2)] * 2
-    grid_spec = pltpu.PrefetchScalarGridSpec(
-        num_scalar_prefetch=2,
-        grid=(1,),
-        in_specs=[pl.BlockSpec(memory_space=pl.ANY)] * 3,
+    shapes = [(8, 4 * PROWS)] + [(8, PROWS)] * 4
+    return pl.pallas_call(
+        pick_kernel,
+        in_specs=[pl.BlockSpec(memory_space=pltpu.SMEM)] * 2
+        + [pl.BlockSpec(memory_space=pltpu.VMEM)] * 3,
         out_specs=[pl.BlockSpec(memory_space=pl.ANY)] * len(shapes),
         scratch_shapes=[pltpu.SemaphoreType.DMA((len(shapes),))],
-    )
-    return pl.pallas_call(
-        pick_kernel,
-        grid_spec=grid_spec,
         out_shape=[
             jax.ShapeDtypeStruct((*shape, 2 * HEAD), jnp.bfloat16) for shape in shapes
         ],
         cost_estimate=pl.CostEstimate(flops=0, transcendentals=0, bytes_accessed=8 << 20),
         name="pick",
     )(plane, table, own, below, above)
+
+
+def join_kernel(*refs):
+    for n, ref in enumerate(refs[:-1]):
+        refs[-1][n * PROWS : (n + 1) * PROWS, :] = ref[...]
+
+
+def join(parts):
+    tile = (None, PROWS, 2 * HEAD)
+    count = len(parts)
+    return pl.pallas_call(
+        join_kernel,
+        grid=(8,),
+        in_specs=[pl.BlockSpec(tile, lambda i: (i, 0, 0))] * count,
+        out_specs=pl.BlockSpec((None, count * PROWS, 2 * HEAD), lambda i: (i, 0, 0)),
+        out_shape=jax.ShapeDtypeStruct((8, count * PROWS, 2 * HEAD), jnp.bfloat16),
+        cost_estimate=pl.CostEstimate(flops=0, transcendentals=0, bytes_accessed=4 << 20),
+        name="join",
+    )(*parts)
 
 
 def shift(value, axis, step):
@@ -402,23 +440,15 @@
     wanted = jnp.broadcast_to(wanted.reshape(1, 8, 8).transpose(0, 2, 1), (8, 8, 8))
     table = exchange(wanted.reshape(64, 8), ST)
 
-    near, up1, down1, up2, down2, up3, down3 = pick(
-        plane, table.reshape(-1), own, below, above
-    )
-    up3 = shift(up3, "z", 3)
-    down3 = shift(down3, "z", -3)
-    up1 = shift(up1, "z", 1)
-    down1 = shift(down1, "z", -1)
-    up2 = shift(up2, "z", 2)
-    down2 = shift(down2, "z", -2)
+    near, up1, down1, up2, down2 = pick(plane, table, own, below, above)
     side = ("y", "c")
-    groups = [
-        exchange(near.reshape(8, 3 * PROWS, -1), side),
-        exchange(jnp.concatenate([up1, down1], axis=1), side),
-        exchange(jnp.concatenate([up2, down2], axis=1), side),
-        exchange(jnp.concatenate([up3, down3], axis=1), side),
-    ]
-    groups = [group.reshape(-1, PROWS, 2 * HEAD) for group in groups]
+    near = exchange(near, side)
+    far = [shift(up1, "z", 1), shift(down1, "z", -1), shift(up2, "z", 2), shift(down2, "z", -2)]
+    far = join(far)
+    far = exchange(far, side)
+    split = 3 * PROWS + PROWS // 2
+    upper = shift(near[:, 3 * PROWS : split], "z", 3)
+    lower = shift(near[:, split:], "z", -3)
 
     convolved, stats = token_path(
         me,
@@ -435,7 +465,7 @@
     stats = lax.psum(stats, "tp")
     stats = stats.transpose(1, 0, 2, 3).reshape(2, -1, 128)
     conv_out = finish(convolved, stats, channel_gain)
-    return attend(plane, asked, conv_out, retrieval_gate, groups)
+    return attend(plane, asked, conv_out, retrieval_gate, (near, far, upper, lower))
 
 
 def solution(mesh):

time: 314 us -> 156 us (0.50)
  the two profiles are of different devices: /device:TPU:2 before, /device:TPU:8 now
where the time goes in v3:
time: 156 us; the launch traced here: 155 us
  waiting for transfers between devices  50.7 us (32%)
  starting transfers between devices  45.1 us (29%)
  Pallas kernels  40.4 us (26%)
  blocking collectives  11.3 us (7%)
  local copies, waits for them, and re-layouts  6.9 us (4%)
    ppermute x12, waiting for transfers between devices, shift(): return lax.ppermute(value, axis, ring(lax.axis_size(axis), step))  33.9 us
    ppermute x12, starting transfers between devices, shift(): return lax.ppermute(value, axis, ring(lax.axis_size(axis), step))  25.9 us
    all_to_all x3, starting transfers between devices, exchange(): return lax.all_to_all(value, axes, split_axis=0, concat_axis=0, tiled=True)  19.2 us
    all_to_all x3, waiting for transfers between devices, exchange(): return lax.all_to_all(value, axes, split_axis=0, concat_axis=0, tiled=True)  16.8 us
    pallas_call x1, Pallas kernels, token_path(): pl.pallas_call(token_kernel, grid_spec=grid_spec, out_shape=[jax.ShapeDty...  15.5 us
    psum x1, blocking collectives, layer(): stats = lax.psum(stats, 'tp')  11.3 us
    pallas_call x1, Pallas kernels, project_passages(): pl.pallas_call(project_kernel, grid=(count // tile,), in_specs=[pl.BlockS...  6.83 us
    pallas_call x1, Pallas kernels, attend(): pl.pallas_call(attend_kernel, grid_spec=grid_spec, out_shape=jax.ShapeDty...  5.63 us
  transfers between devices with their start and end apart: 15, of which 6 were waited for; matrix products, arithmetic and copies ran while one was open for 3% of the time, Pallas kernels for 16%

profile of v3, /device:TPU:8, one launch (start us, length us, event | category | flops | bytes accessed | tf_op | source)
XLA Modules:
  0.0 154.8 jit_solution(17666886903319159460)
XLA Ops:
  0.0 6.8 %project_passages.1 = bf16[1024,512]{1,0:T(8,128)(2,1)} custom-call(bf16[1024,2048]{1,0:T(8,128)(2,1)} %bitcast.26, f32[1,2048]{1,0:T(1,128)} %bitcast.29, bf16[2048,256]{1,0:T(8,128)(2,1)} %keys_ref.1, bf16[2048,256]{1,0:T(8,128)(2,1)} %values_ref.1), custom_call_target="tpu_custom_call" | custom-call | flops 2147483648 | bytes 7340032 | tf_op jit(solution)/shard_map/project_passages/pallas_call | solution.py:49
  6.8 1.9 %collective-permute-start.4 = (bf16[16,64,512]{2,1,0:T(8,128)(2,1)}, bf16[16,64,512]{2,1,0:T(8,128)(2,1)S(1)}, u32[]{:S(2)}, u32[]{:S(2)}) collective-permute-start(bf16[16,64,512]{2,1,0:T(8,128)(2,1)} %bitcast.16), channel_id=1, source_target_pairs={{0,32},{32,64},{64,96},{96,128},{128,160},{160,192},{192,224},{224... | collective-permute-start | bytes 3145736 | tf_op jit(solution)/shard_map/ppermute | solution.py:400
  8.8 3.9 %collective-permute-start.5 = (bf16[16,64,512]{2,1,0:T(8,128)(2,1)}, bf16[16,64,512]{2,1,0:T(8,128)(2,1)S(1)}, u32[]{:S(2)}, u32[]{:S(2)}) collective-permute-start(bf16[16,64,512]{2,1,0:T(8,128)(2,1)} %bitcast.17), channel_id=1, source_target_pairs={{0,224},{32,0},{64,32},{96,64},{128,96},{160,128},{192,160},{224,1... | collective-permute-start | bytes 3145736 | tf_op jit(solution)/shard_map/ppermute | solution.py:400
  13.9 9.5 %all-to-all-start = ((s32[64,1,8]{2,1,0:T(1,128)}), s32[64,1,8]{2,1,0:T(1,128)S(1)}, u32[]{:S(2)}, u32[]{:S(2)}) async-start(s32[64,1,8]{2,1,0:T(1,128)} %bitcast.11), calls=%async_computation | async-start | bytes 65536 | tf_op jit(solution)/shard_map/all_to_all | solution.py:404
  23.4 16.8 %all-to-all-done = s32[64,1,8]{2,1,0:T(1,128)S(1)} async-done(((s32[64,1,8]{2,1,0:T(1,128)}), s32[64,1,8]{2,1,0:T(1,128)S(1)}, u32[]{:S(2)}, u32[]{:S(2)}) %all-to-all-start) | async-done | bytes 2080 | tf_op jit(solution)/shard_map/all_to_all | solution.py:404
  41.6 3.9 %pick.1 = (bf16[8,256,512]{2,1,0:T(8,128)(2,1)}, bf16[8,64,512]{2,1,0:T(8,128)(2,1)}, bf16[8,64,512]{2,1,0:T(8,128)(2,1)}, bf16[8,64,512]{2,1,0:T(8,128)(2,1)}, bf16[8,64,512]{2,1,0:T(8,128)(2,1)}) custom-call(s32[1]{0:T(128)} %bitcast.plane_ref, s32[64,8]{1,0:T(8,128)} %bitcast.19, bf16[16,64,512]{2,1,0:T(8,128)(2,1)} %bitcast.18, ...), custom_call_target="tpu_custom_call" | custom-call | bytes 8388608 | tf_op jit(solution)/shard_map/pick/pallas_call | solution.py:366
  45.5 4.9 %all-to-all-start.1 = ((bf16[8,256,512]{2,1,0:T(8,128)(2,1)}), bf16[8,256,512]{2,1,0:T(8,128)(2,1)S(1)}, u32[]{:S(2)}, u32[]{:S(2)}) async-start(bf16[8,256,512]{2,1,0:T(8,128)(2,1)} %get-tuple-element.14), calls=%async_computation.1 | async-start | bytes 4194304 | tf_op jit(solution)/shard_map/all_to_all | solution.py:404
  50.4 2.7 %collective-permute-start.6 = (bf16[8,64,512]{2,1,0:T(8,128)(2,1)}, bf16[8,64,512]{2,1,0:T(8,128)(2,1)S(1)}, u32[]{:S(2)}, u32[]{:S(2)}) collective-permute-start(bf16[8,64,512]{2,1,0:T(8,128)(2,1)} %get-tuple-element.15), channel_id=1, source_target_pairs={{0,32},{32,64},{64,96},{96,128},{128,160},{160,192},{192,224},{224... | collective-permute-start | bytes 1572872 | tf_op jit(solution)/shard_map/ppermute | solution.py:400
  53.6 1.6 %collective-permute-start.8 = (bf16[8,64,512]{2,1,0:T(8,128)(2,1)}, bf16[8,64,512]{2,1,0:T(8,128)(2,1)}, u32[]{:S(2)}, u32[]{:S(2)}) collective-permute-start(bf16[8,64,512]{2,1,0:T(8,128)(2,1)} %get-tuple-element.17), channel_id=1, source_target_pairs={{0,64},{32,96},{64,128},{96,160},{128,192},{160,224},{192,0},{224,... | collective-permute-start | bytes 1572872 | tf_op jit(solution)/shard_map/ppermute | solution.py:400
  55.2 2.6 %collective-permute-start.9 = (bf16[8,64,512]{2,1,0:T(8,128)(2,1)}, bf16[8,64,512]{2,1,0:T(8,128)(2,1)}, u32[]{:S(2)}, u32[]{:S(2)}) collective-permute-start(bf16[8,64,512]{2,1,0:T(8,128)(2,1)} %get-tuple-element.18), channel_id=1, source_target_pairs={{0,192},{32,224},{64,0},{96,32},{128,64},{160,96},{192,128},{224,1... | collective-permute-start | bytes 1572872 | tf_op jit(solution)/shard_map/ppermute | solution.py:400
  57.8 1.5 collective-permute-start
  59.3 8.1 %collective-permute-done.6.refs_0_ = bf16[8,64,512]{2,1,0:T(8,128)(2,1)S(1)} collective-permute-done((bf16[8,64,512]{2,1,0:T(8,128)(2,1)}, bf16[8,64,512]{2,1,0:T(8,128)(2,1)S(1)}, u32[]{:S(2)}, u32[]{:S(2)}) %collective-permute-start.6) | collective-permute-done | bytes 524320 | tf_op jit(solution)/shard_map/ppermute | solution.py:400
  67.3 2.8 %collective-permute-start.1 = (bf16[1024,512]{1,0:T(8,128)(2,1)}, bf16[1024,512]{1,0:T(8,128)(2,1)}, u32[]{:S(2)}, u32[]{:S(2)}) collective-permute-start(bf16[1024,512]{1,0:T(8,128)(2,1)} %own_ref.1), channel_id=1, source_target_pairs={{0,3},{1,0},{2,1},{3,2},{4,7},{5,4},{6,5},{7,6},{8,11},{9,8},{10,9... | collective-permute-start | bytes 3145736 | tf_op jit(solution)/shard_map/ppermute | solution.py:400
  70.1 18.7 %collective-permute-done.8.refs_2_ = bf16[8,64,512]{2,1,0:T(8,128)(2,1)} collective-permute-done((bf16[8,64,512]{2,1,0:T(8,128)(2,1)}, bf16[8,64,512]{2,1,0:T(8,128)(2,1)}, u32[]{:S(2)}, u32[]{:S(2)}) %collective-permute-start.8) | collective-permute-done | bytes 524320 | tf_op jit(solution)/shard_map/ppermute | solution.py:400
  89.7 5.6 %join.1 = bf16[8,256,512]{2,1,0:T(8,128)(2,1)} custom-call(bf16[8,64,512]{2,1,0:T(8,128)(2,1)} %copy-done.3, bf16[8,64,512]{2,1,0:T(8,128)(2,1)} %copy-done.4, bf16[8,64,512]{2,1,0:T(8,128)(2,1)} %collective-permute-done.8.refs_2_, bf16[8,64,512]{2,1,0:T(8,128)(2,1)} %collective-permute-done.9.refs_3_), custom_call_target="tpu_custom_call" | custom-call | bytes 4194304 | tf_op jit(solution)/shard_map/join/pallas_call | solution.py:388
  95.3 4.8 %all-to-all-start.2 = ((bf16[8,256,512]{2,1,0:T(8,128)(2,1)}), bf16[8,256,512]{2,1,0:T(8,128)(2,1)}, u32[]{:S(2)}, u32[]{:S(2)}) async-start(bf16[8,256,512]{2,1,0:T(8,128)(2,1)} %join.1), calls=%async_computation.2 | async-start | bytes 4194304 | tf_op jit(solution)/shard_map/all_to_all | solution.py:404
  101.2 1.6 %collective-permute-start.2 = (bf16[512,512]{1,0:T(8,128)(2,1)S(1)}, bf16[512,512]{1,0:T(8,128)(2,1)}, u32[]{:S(2)}, u32[]{:S(2)}) collective-permute-start(bf16[512,512]{1,0:T(8,128)(2,1)S(1)} %slice.16), channel_id=1, source_target_pairs={{0,1},{1,2},{2,3},{3,0},{4,5},{5,6},{6,7},{7,4},{8,9},{9,10},{10,1... | collective-permute-start | bytes 1572872 | tf_op jit(solution)/shard_map/ppermute | solution.py:400
  103.9 1.8 %collective-permute-start.3 = (bf16[512,512]{1,0:T(8,128)(2,1)S(1)}, bf16[512,512]{1,0:T(8,128)(2,1)}, u32[]{:S(2)}, u32[]{:S(2)}) collective-permute-start(bf16[512,512]{1,0:T(8,128)(2,1)S(1)} %slice.17), channel_id=1, source_target_pairs={{0,3},{1,0},{2,1},{3,2},{4,7},{5,4},{6,5},{7,6},{8,11},{9,8},{10,9... | collective-permute-start | bytes 1572872 | tf_op jit(solution)/shard_map/ppermute | solution.py:400
  106.4 5.0 %collective-permute-start.11 = (bf16[8,32,512]{2,1,0:T(8,128)(2,1)S(1)}, bf16[8,32,512]{2,1,0:T(8,128)(2,1)S(1)}, u32[]{:S(2)}, u32[]{:S(2)}) collective-permute-start(bf16[8,32,512]{2,1,0:T(8,128)(2,1)S(1)} %get-tuple-element.19), channel_id=1, source_target_pairs={{0,160},{32,192},{64,224},{96,0},{128,32},{160,64},{192,96},{224,1... | collective-permute-start | bytes 786440 | tf_op jit(solution)/shard_map/ppermute | solution.py:400
  111.5 5.1 %collective-permute-done.2.far0_ref = bf16[512,512]{1,0:T(8,128)(2,1)} collective-permute-done((bf16[512,512]{1,0:T(8,128)(2,1)S(1)}, bf16[512,512]{1,0:T(8,128)(2,1)}, u32[]{:S(2)}, u32[]{:S(2)}) %collective-permute-start.2) | collective-permute-done | bytes 524320 | tf_op jit(solution)/shard_map/ppermute | solution.py:400
  117.7 15.5 %token_path.1 = (f32[1024,512]{1,0:T(8,128)}, f32[2,2,4,128]{3,2,1,0:T(4,128)}) custom-call(s32[1]{0:T(128)} %bitcast.1.me_ref, bf16[1024,512]{1,0:T(8,128)(2,1)} %own_ref.1, bf16[1024,512]{1,0:T(8,128)(2,1)} %collective-permute-done.left_ref, bf16[1024,512]{1,0:T(8,128)(2,1)} %collective-permute-done.1.right_ref, ...), custom_call_target="tpu_custom_call" | custom-call | flops 4294967296 | bytes 10485760 | tf_op jit(solution)/shard_map/token_path/pallas_call | solution.py:162
  133.9 11.3 %psum.7.stats_ref = f32[2,8,128]{2,1,0:T(8,128)} all-reduce(f32[2,8,128]{2,1,0:T(8,128)S(1)} %bitcast.20), channel_id=1, replica_groups=mesh['z'=8,'y'=4,'c'=2,'tp'=4] {'tp'}, use_global_device_ids=true, to_apply=%region_0.1 | all-reduce | flops 2048 | bytes 16384 | tf_op jit(solution)/shard_map/psum | solution.py:465
  145.2 2.9 %finish.1.conv_ref = f32[1024,512]{1,0:T(8,128)} custom-call(f32[1024,512]{1,0:T(8,128)} %get-tuple-element.12.conv_ref, f32[2,8,128]{2,1,0:T(8,128)} %psum.7.stats_ref, f32[1,512]{1,0:T(1,128)} %bitcast.24), custom_call_target="tpu_custom_call" | custom-call | flops 4194304 | bytes 4194304 | tf_op jit(solution)/shard_map/finish/pallas_call | solution.py:207
  149.0 5.6 %attend.1 = bf16[1024,512]{1,0:T(8,128)(2,1)} custom-call(s32[1]{0:T(128)} %bitcast.plane_ref, s32[32]{0:T(128)} %copy-done.8, f32[1024,512]{1,0:T(8,128)} %finish.1.conv_ref, f32[1,512]{1,0:T(1,128)} %bitcast.25, bf16[8,256,512]{2,1,0:T(8,128)(2,1)} %copy-done, bf16[8,256,512]{2,1,0:T(8,128)(2,1)} %all-to-all-done.2.refs_1_, bf16[8,32,512]{2,1,0:T(8,128)(2,1)} %copy-done.5, ...), custom_call_target="tpu_custom_call" | custom-call | flops 268435456 | bytes 5242880 | tf_op jit(solution)/shard_map/attend/pallas_call | solution.py:316
  (47 shorter events, 9.6 us)
Async XLA Ops:
  0.0 12.7 %copy-start.9 = (s32[16,2]{0,1:T(2,128)S(1)}, s32[16,2]{0,1:T(2,128)}, u32[]{:S(2)}) copy-start(s32[16,2]{0,1:T(2,128)} %param.24) | copy-start | bytes 388
  0.0 12.9 %copy-start.10 = (s32[16,2]{0,1:T(2,128)S(1)}, s32[16,2]{0,1:T(2,128)}, u32[]{:S(2)}) copy-start(s32[16,2]{0,1:T(2,128)} %param.25) | copy-start | bytes 388
  6.8 33.4 %collective-permute-start.4 = (bf16[16,64,512]{2,1,0:T(8,128)(2,1)}, bf16[16,64,512]{2,1,0:T(8,128)(2,1)S(1)}, u32[]{:S(2)}, u32[]{:S(2)}) collective-permute-start(bf16[16,64,512]{2,1,0:T(8,128)(2,1)} %bitcast.16), channel_id=1, source_target_pairs={{0,32},{32,64},{64,96},{96,128},{128,160},{160,192},{192,224},{224... | collective-permute-start | bytes 3145736 | tf_op jit(solution)/shard_map/ppermute | solution.py:400
  8.8 31.5 %collective-permute-start.5 = (bf16[16,64,512]{2,1,0:T(8,128)(2,1)}, bf16[16,64,512]{2,1,0:T(8,128)(2,1)S(1)}, u32[]{:S(2)}, u32[]{:S(2)}) collective-permute-start(bf16[16,64,512]{2,1,0:T(8,128)(2,1)} %bitcast.17), channel_id=1, source_target_pairs={{0,224},{32,0},{64,32},{96,64},{128,96},{160,128},{192,160},{224,1... | collective-permute-start | bytes 3145736 | tf_op jit(solution)/shard_map/ppermute | solution.py:400
  12.9 32.6 %copy-start.8 = (s32[32]{0:T(128)}, s32[32]{0:T(128)S(1)}, u32[]{:S(2)}) copy-start(s32[32]{0:T(128)S(1)} %reshape.46.where_ref) | copy-start | bytes 388
  13.9 26.3 %all-to-all-start = ((s32[64,1,8]{2,1,0:T(1,128)}), s32[64,1,8]{2,1,0:T(1,128)S(1)}, u32[]{:S(2)}, u32[]{:S(2)}) async-start(s32[64,1,8]{2,1,0:T(1,128)} %bitcast.11), calls=%async_computation | async-start | bytes 65536 | tf_op jit(solution)/shard_map/all_to_all | solution.py:404
  40.2 1.0 copy-start.1
  40.2 1.3 copy-start.2
  45.5 49.7 %all-to-all-start.1 = ((bf16[8,256,512]{2,1,0:T(8,128)(2,1)}), bf16[8,256,512]{2,1,0:T(8,128)(2,1)S(1)}, u32[]{:S(2)}, u32[]{:S(2)}) async-start(bf16[8,256,512]{2,1,0:T(8,128)(2,1)} %get-tuple-element.14), calls=%async_computation.1 | async-start | bytes 4194304 | tf_op jit(solution)/shard_map/all_to_all | solution.py:404
  50.4 16.9 %collective-permute-start.6 = (bf16[8,64,512]{2,1,0:T(8,128)(2,1)}, bf16[8,64,512]{2,1,0:T(8,128)(2,1)S(1)}, u32[]{:S(2)}, u32[]{:S(2)}) collective-permute-start(bf16[8,64,512]{2,1,0:T(8,128)(2,1)} %get-tuple-element.15), channel_id=1, source_target_pairs={{0,32},{32,64},{64,96},{96,128},{128,160},{160,192},{192,224},{224... | collective-permute-start | bytes 1572872 | tf_op jit(solution)/shard_map/ppermute | solution.py:400
  53.1 17.0 %collective-permute-start.7 = (bf16[8,64,512]{2,1,0:T(8,128)(2,1)}, bf16[8,64,512]{2,1,0:T(8,128)(2,1)S(1)}, u32[]{:S(2)}, u32[]{:S(2)}) collective-permute-start(bf16[8,64,512]{2,1,0:T(8,128)(2,1)} %get-tuple-element.16), channel_id=1, source_target_pairs={{0,224},{32,0},{64,32},{96,64},{128,96},{160,128},{192,160},{224,1... | collective-permute-start | bytes 1572872 | tf_op jit(solution)/shard_map/ppermute | solution.py:400
  53.6 35.1 %collective-permute-start.8 = (bf16[8,64,512]{2,1,0:T(8,128)(2,1)}, bf16[8,64,512]{2,1,0:T(8,128)(2,1)}, u32[]{:S(2)}, u32[]{:S(2)}) collective-permute-start(bf16[8,64,512]{2,1,0:T(8,128)(2,1)} %get-tuple-element.17), channel_id=1, source_target_pairs={{0,64},{32,96},{64,128},{96,160},{128,192},{160,224},{192,0},{224,... | collective-permute-start | bytes 1572872 | tf_op jit(solution)/shard_map/ppermute | solution.py:400
  55.2 34.4 %collective-permute-start.9 = (bf16[8,64,512]{2,1,0:T(8,128)(2,1)}, bf16[8,64,512]{2,1,0:T(8,128)(2,1)}, u32[]{:S(2)}, u32[]{:S(2)}) collective-permute-start(bf16[8,64,512]{2,1,0:T(8,128)(2,1)} %get-tuple-element.18), channel_id=1, source_target_pairs={{0,192},{32,224},{64,0},{96,32},{128,64},{160,96},{192,128},{224,1... | collective-permute-start | bytes 1572872 | tf_op jit(solution)/shard_map/ppermute | solution.py:400
  57.8 42.3 %collective-permute-start = (bf16[1024,512]{1,0:T(8,128)(2,1)}, bf16[1024,512]{1,0:T(8,128)(2,1)}, u32[]{:S(2)}, u32[]{:S(2)}) collective-permute-start(bf16[1024,512]{1,0:T(8,128)(2,1)} %own_ref.1), channel_id=1, source_target_pairs={{0,1},{1,2},{2,3},{3,0},{4,5},{5,6},{6,7},{7,4},{8,9},{9,10},{10,1... | collective-permute-start | bytes 3145736 | tf_op jit(solution)/shard_map/ppermute | solution.py:400
  67.3 22.3 %copy-start.3 = (bf16[8,64,512]{2,1,0:T(8,128)(2,1)}, bf16[8,64,512]{2,1,0:T(8,128)(2,1)S(1)}, u32[]{:S(2)}) copy-start(bf16[8,64,512]{2,1,0:T(8,128)(2,1)S(1)} %collective-permute-done.6.refs_0_) | copy-start | bytes 1572868
  67.3 35.4 %collective-permute-start.1 = (bf16[1024,512]{1,0:T(8,128)(2,1)}, bf16[1024,512]{1,0:T(8,128)(2,1)}, u32[]{:S(2)}, u32[]{:S(2)}) collective-permute-start(bf16[1024,512]{1,0:T(8,128)(2,1)} %own_ref.1), channel_id=1, source_target_pairs={{0,3},{1,0},{2,1},{3,2},{4,7},{5,4},{6,5},{7,6},{8,11},{9,8},{10,9... | collective-permute-start | bytes 3145736 | tf_op jit(solution)/shard_map/ppermute | solution.py:400
  70.1 19.6 %copy-start.4 = (bf16[8,64,512]{2,1,0:T(8,128)(2,1)}, bf16[8,64,512]{2,1,0:T(8,128)(2,1)S(1)}, u32[]{:S(2)}) copy-start(bf16[8,64,512]{2,1,0:T(8,128)(2,1)S(1)} %collective-permute-done.7.refs_1_) | copy-start | bytes 1572868
  95.3 10.4 %copy-start = (bf16[8,256,512]{2,1,0:T(8,128)(2,1)}, bf16[8,256,512]{2,1,0:T(8,128)(2,1)S(1)}, u32[]{:S(2)}) copy-start(bf16[8,256,512]{2,1,0:T(8,128)(2,1)S(1)} %all-to-all-done.1.refs_0_) | copy-start | bytes 6291460
  95.3 52.9 %all-to-all-start.2 = ((bf16[8,256,512]{2,1,0:T(8,128)(2,1)}), bf16[8,256,512]{2,1,0:T(8,128)(2,1)}, u32[]{:S(2)}, u32[]{:S(2)}) async-start(bf16[8,256,512]{2,1,0:T(8,128)(2,1)} %join.1), calls=%async_computation.2 | async-start | bytes 4194304 | tf_op jit(solution)/shard_map/all_to_all | solution.py:404
  101.2 15.3 %collective-permute-start.2 = (bf16[512,512]{1,0:T(8,128)(2,1)S(1)}, bf16[512,512]{1,0:T(8,128)(2,1)}, u32[]{:S(2)}, u32[]{:S(2)}) collective-permute-start(bf16[512,512]{1,0:T(8,128)(2,1)S(1)} %slice.16), channel_id=1, source_target_pairs={{0,1},{1,2},{2,3},{3,0},{4,5},{5,6},{6,7},{7,4},{8,9},{9,10},{10,1... | collective-permute-start | bytes 1572872 | tf_op jit(solution)/shard_map/ppermute | solution.py:400
  103.9 13.8 %collective-permute-start.3 = (bf16[512,512]{1,0:T(8,128)(2,1)S(1)}, bf16[512,512]{1,0:T(8,128)(2,1)}, u32[]{:S(2)}, u32[]{:S(2)}) collective-permute-start(bf16[512,512]{1,0:T(8,128)(2,1)S(1)} %slice.17), channel_id=1, source_target_pairs={{0,3},{1,0},{2,1},{3,2},{4,7},{5,4},{6,5},{7,6},{8,11},{9,8},{10,9... | collective-permute-start | bytes 1572872 | tf_op jit(solution)/shard_map/ppermute | solution.py:400
  106.4 41.7 %collective-permute-start.10 = (bf16[8,32,512]{2,1,0:T(8,128)(2,1)}, bf16[8,32,512]{2,1,0:T(8,128)(2,1)S(1)}, u32[]{:S(2)}, u32[]{:S(2)}) collective-permute-start(bf16[8,32,512]{2,1,0:T(8,128)(2,1)} %get-tuple-element.20), channel_id=1, source_target_pairs={{0,96},{32,128},{64,160},{96,192},{128,224},{160,0},{192,32},{224,... | collective-permute-start | bytes 786440 | tf_op jit(solution)/shard_map/ppermute | solution.py:400
  106.4 41.7 %collective-permute-start.11 = (bf16[8,32,512]{2,1,0:T(8,128)(2,1)S(1)}, bf16[8,32,512]{2,1,0:T(8,128)(2,1)S(1)}, u32[]{:S(2)}, u32[]{:S(2)}) collective-permute-start(bf16[8,32,512]{2,1,0:T(8,128)(2,1)S(1)} %get-tuple-element.19), channel_id=1, source_target_pairs={{0,160},{32,192},{64,224},{96,0},{128,32},{160,64},{192,96},{224,1... | collective-permute-start | bytes 786440 | tf_op jit(solution)/shard_map/ppermute | solution.py:400
  148.2 0.8 copy-start.6
  (2 other events, 1.3 us)

commit v4 on v3

--- a/solution.py
+++ b/solution.py
@@ -1,3 +1,4 @@
+import functools
 import math
 
 import jax
@@ -69,8 +70,7 @@
     own_ref,
     left_ref,
     right_ref,
-    far0_ref,
-    far1_ref,
+    far_ref,
     gain_ref,
     inner_ref,
     gating_ref,
@@ -80,7 +80,6 @@
     padded_ref,
 ):
     me = me_ref[0]
-    first = pl.program_id(0) == 0
     width = own_ref.shape[1]
     squares = jnp.zeros((LENGTH, 1), jnp.float32)
     inner = jnp.zeros((LENGTH, width), jnp.float32)
@@ -94,9 +93,7 @@
         elif offset == 3:
             piece = left_ref[...].astype(jnp.float32)
         else:
-            piece = jnp.where(
-                first, far0_ref[...].astype(jnp.float32), far1_ref[...].astype(jnp.float32)
-            )
+            piece = far_ref[...].astype(jnp.float32)
         squares = squares + jnp.sum(piece * piece, axis=1, keepdims=True)
         scaled = (piece * gain_ref[at]).astype(jnp.bfloat16)
         inner = inner + jnp.dot(scaled, inner_ref[at], preferred_element_type=jnp.float32)
@@ -139,15 +136,13 @@
         stats_ref[1, n : n + 1, :] = jnp.sum(square_sums.T, axis=0, keepdims=True)
 
 
-def token_path(me, own, left, right, far0, far1, gain, inner_weight, gating_weight, taps):
+def token_path(me, own, left, right, far, gain, inner_weight, gating_weight, taps):
     rows, width = own.shape
     grid_spec = pltpu.PrefetchScalarGridSpec(
         num_scalar_prefetch=1,
         grid=(rows // LENGTH,),
-        in_specs=[pl.BlockSpec((LENGTH, width), lambda i, m: (i, 0))] * 3
+        in_specs=[pl.BlockSpec((LENGTH, width), lambda i, m: (i, 0))] * 4
         + [
-            whole((LENGTH, width)),
-            whole((LENGTH, width)),
             whole((4, 1, width)),
             whole((4, width, width)),
             whole((4, width, width)),
@@ -175,8 +170,7 @@
         own,
         left,
         right,
-        far0,
-        far1,
+        far,
         gain.reshape(4, 1, width),
         inner_weight.reshape(4, width, width),
         gating_weight.reshape(4, width, width),
@@ -377,23 +371,33 @@
     )(plane, table, own, below, above)
 
 
-def join_kernel(*refs):
-    for n, ref in enumerate(refs[:-1]):
-        refs[-1][n * PROWS : (n + 1) * PROWS, :] = ref[...]
-
-
-def join(parts):
-    tile = (None, PROWS, 2 * HEAD)
-    count = len(parts)
-    return pl.pallas_call(
-        join_kernel,
-        grid=(8,),
-        in_specs=[pl.BlockSpec(tile, lambda i: (i, 0, 0))] * count,
-        out_specs=pl.BlockSpec((None, count * PROWS, 2 * HEAD), lambda i: (i, 0, 0)),
-        out_shape=jax.ShapeDtypeStruct((8, count * PROWS, 2 * HEAD), jnp.bfloat16),
-        cost_estimate=pl.CostEstimate(flops=0, transcendentals=0, bytes_accessed=4 << 20),
-        name="join",
-    )(*parts)
+def fill_kernel(*refs, at):
+    first_ref, second_ref, out_ref, sems = refs[0], refs[1], refs[-2], refs[-1]
+    copies = [
+        pltpu.make_async_copy(
+            ref, out_ref.at[:, pl.ds((at + n) * PROWS, PROWS)], sems.at[n]
+        )
+        for n, ref in enumerate((first_ref, second_ref))
+    ]
+    for copy in copies:
+        copy.start()
+    for copy in copies:
+        copy.wait()
+
+
+def fill(first, second, at, into=None):
+    held = [] if into is None else [into]
+    return pl.pallas_call(
+        functools.partial(fill_kernel, at=at),
+        in_specs=[pl.BlockSpec(memory_space=pltpu.VMEM)] * 2
+        + [pl.BlockSpec(memory_space=pl.ANY)] * len(held),
+        out_specs=pl.BlockSpec(memory_space=pl.ANY),
+        scratch_shapes=[pltpu.SemaphoreType.DMA((2,))],
+        out_shape=jax.ShapeDtypeStruct((8, 4 * PROWS, 2 * HEAD), jnp.bfloat16),
+        input_output_aliases={2: 0} if held else {},
+        cost_estimate=pl.CostEstimate(flops=0, transcendentals=0, bytes_accessed=2 << 20),
+        name="fill",
+    )(first, second, *held)
 
 
 def shift(value, axis, step):
@@ -423,8 +427,7 @@
     plane = lax.axis_index("z").astype(jnp.int32).reshape(1)
     left = shift(tokens, "tp", 1)
     right = shift(tokens, "tp", -1)
-    far0 = shift(left[:LENGTH], "tp", 1)
-    far1 = shift(right[LENGTH:], "tp", -1)
+    far = shift(tokens, "tp", 2)
 
     own = project_passages(passage_store, passage_gain, keys_weight, values_weight)
     own = own.reshape(-1, PROWS, 2 * HEAD)
@@ -443,9 +446,13 @@
     near, up1, down1, up2, down2 = pick(plane, table, own, below, above)
     side = ("y", "c")
     near = exchange(near, side)
-    far = [shift(up1, "z", 1), shift(down1, "z", -1), shift(up2, "z", 2), shift(down2, "z", -2)]
-    far = join(far)
-    far = exchange(far, side)
+    up1 = shift(up1, "z", 1)
+    down1 = shift(down1, "z", -1)
+    up2 = shift(up2, "z", 2)
+    down2 = shift(down2, "z", -2)
+    away = fill(up1, down1, 0)
+    away = fill(up2, down2, 2, away)
+    away = exchange(away, side)
     split = 3 * PROWS + PROWS // 2
     upper = shift(near[:, 3 * PROWS : split], "z", 3)
     lower = shift(near[:, split:], "z", -3)
@@ -455,8 +462,7 @@
         tokens,
         left,
         right,
-        far0,
-        far1,
+        far,
         token_gain,
         inner_weight,
         gating_weight,
@@ -465,7 +471,7 @@
     stats = lax.psum(stats, "tp")
     stats = stats.transpose(1, 0, 2, 3).reshape(2, -1, 128)
     conv_out = finish(convolved, stats, channel_gain)
-    return attend(plane, asked, conv_out, retrieval_gate, (near, far, upper, lower))
+    return attend(plane, asked, conv_out, retrieval_gate, (near, away, upper, lower))
 
 
 def solution(mesh):

time: 156 us -> 184 us (1.18)
  the two profiles are of different devices: /device:TPU:8 before, /device:TPU:2 now
where the time goes in v4:
time: 184 us; the launch traced here: 182 us
  waiting for transfers between devices  88.3 us (48%)
  starting transfers between devices  40.1 us (22%)
  Pallas kernels  38.9 us (21%)
  blocking collectives  9.27 us (5%)
  local copies, waits for them, and re-layouts  4.79 us (3%)
    ppermute x11, waiting for transfers between devices, shift(): return lax.ppermute(value, axis, ring(lax.axis_size(axis), step))  70.6 us
    ppermute x11, starting transfers between devices, shift(): return lax.ppermute(value, axis, ring(lax.axis_size(axis), step))  22.6 us
    all_to_all x3, waiting for transfers between devices, exchange(): return lax.all_to_all(value, axes, split_axis=0, concat_axis=0, tiled=True)  17.7 us
    all_to_all x3, starting transfers between devices, exchange(): return lax.all_to_all(value, axes, split_axis=0, concat_axis=0, tiled=True)  17.5 us
    pallas_call x1, Pallas kernels, token_path(): pl.pallas_call(token_kernel, grid_spec=grid_spec, out_shape=[jax.ShapeDty...  15.3 us
    psum x1, blocking collectives, layer(): stats = lax.psum(stats, 'tp')  9.27 us
    pallas_call x1, Pallas kernels, project_passages(): pl.pallas_call(project_kernel, grid=(count // tile,), in_specs=[pl.BlockS...  6.84 us
    pallas_call x1, Pallas kernels, attend(): pl.pallas_call(attend_kernel, grid_spec=grid_spec, out_shape=jax.ShapeDty...  5.63 us
  transfers between devices with their start and end apart: 14, of which 8 were waited for; matrix products, arithmetic and copies ran while one was open for 1% of the time, Pallas kernels for 12%

profile of v4, /device:TPU:2, one launch (start us, length us, event | category | flops | bytes accessed | tf_op | source)
XLA Modules:
  0.0 181.9 jit_solution(2487528556723852355)
XLA Ops:
  0.0 6.8 %project_passages.1 = bf16[1024,512]{1,0:T(8,128)(2,1)} custom-call(bf16[1024,2048]{1,0:T(8,128)(2,1)} %bitcast.26, f32[1,2048]{1,0:T(1,128)} %bitcast.29, bf16[2048,256]{1,0:T(8,128)(2,1)} %keys_ref.1, bf16[2048,256]{1,0:T(8,128)(2,1)} %values_ref.1), custom_call_target="tpu_custom_call" | custom-call | flops 2147483648 | bytes 7340032 | tf_op jit(solution)/shard_map/project_passages/pallas_call | solution.py:50
  6.8 1.9 %collective-permute-start.3 = (bf16[16,64,512]{2,1,0:T(8,128)(2,1)}, bf16[16,64,512]{2,1,0:T(8,128)(2,1)S(1)}, u32[]{:S(2)}, u32[]{:S(2)}) collective-permute-start(bf16[16,64,512]{2,1,0:T(8,128)(2,1)} %bitcast.16), channel_id=1, source_target_pairs={{0,32},{32,64},{64,96},{96,128},{128,160},{160,192},{192,224},{224... | collective-permute-start | bytes 3145736 | tf_op jit(solution)/shard_map/ppermute | solution.py:404
  8.8 4.0 %collective-permute-start.4 = (bf16[16,64,512]{2,1,0:T(8,128)(2,1)}, bf16[16,64,512]{2,1,0:T(8,128)(2,1)S(1)}, u32[]{:S(2)}, u32[]{:S(2)}) collective-permute-start(bf16[16,64,512]{2,1,0:T(8,128)(2,1)} %bitcast.17), channel_id=1, source_target_pairs={{0,224},{32,0},{64,32},{96,64},{128,96},{160,128},{192,160},{224,1... | collective-permute-start | bytes 3145736 | tf_op jit(solution)/shard_map/ppermute | solution.py:404
  13.9 9.5 %all-to-all-start = ((s32[64,1,8]{2,1,0:T(1,128)}), s32[64,1,8]{2,1,0:T(1,128)S(1)}, u32[]{:S(2)}, u32[]{:S(2)}) async-start(s32[64,1,8]{2,1,0:T(1,128)} %bitcast.11), calls=%async_computation | async-start | bytes 65536 | tf_op jit(solution)/shard_map/all_to_all | solution.py:408
  23.4 17.7 %all-to-all-done = s32[64,1,8]{2,1,0:T(1,128)S(1)} async-done(((s32[64,1,8]{2,1,0:T(1,128)}), s32[64,1,8]{2,1,0:T(1,128)S(1)}, u32[]{:S(2)}, u32[]{:S(2)}) %all-to-all-start) | async-done | bytes 2080 | tf_op jit(solution)/shard_map/all_to_all | solution.py:408
  42.4 3.9 %pick.1 = (bf16[8,256,512]{2,1,0:T(8,128)(2,1)}, bf16[8,64,512]{2,1,0:T(8,128)(2,1)}, bf16[8,64,512]{2,1,0:T(8,128)(2,1)}, bf16[8,64,512]{2,1,0:T(8,128)(2,1)}, bf16[8,64,512]{2,1,0:T(8,128)(2,1)}) custom-call(s32[1]{0:T(128)} %bitcast.plane_ref, s32[64,8]{1,0:T(8,128)} %bitcast.19, bf16[16,64,512]{2,1,0:T(8,128)(2,1)} %bitcast.18, ...), custom_call_target="tpu_custom_call" | custom-call | bytes 8388608 | tf_op jit(solution)/shard_map/pick/pallas_call | solution.py:360
  46.3 3.6 %all-to-all-start.1 = ((bf16[8,256,512]{2,1,0:T(8,128)(2,1)}), bf16[8,256,512]{2,1,0:T(8,128)(2,1)S(1)}, u32[]{:S(2)}, u32[]{:S(2)}) async-start(bf16[8,256,512]{2,1,0:T(8,128)(2,1)} %get-tuple-element.14), calls=%async_computation.1 | async-start | bytes 4194304 | tf_op jit(solution)/shard_map/all_to_all | solution.py:408
  50.0 2.8 %collective-permute-start.7 = (bf16[8,64,512]{2,1,0:T(8,128)(2,1)}, bf16[8,64,512]{2,1,0:T(8,128)(2,1)}, u32[]{:S(2)}, u32[]{:S(2)}) collective-permute-start(bf16[8,64,512]{2,1,0:T(8,128)(2,1)} %get-tuple-element.17), channel_id=1, source_target_pairs={{0,32},{32,64},{64,96},{96,128},{128,160},{160,192},{192,224},{224... | collective-permute-start | bytes 1572872 | tf_op jit(solution)/shard_map/ppermute | solution.py:404
  53.3 1.6 collective-permute-start.5
  54.9 2.6 %collective-permute-start.6 = (bf16[8,64,512]{2,1,0:T(8,128)(2,1)}, bf16[8,64,512]{2,1,0:T(8,128)(2,1)S(1)}, u32[]{:S(2)}, u32[]{:S(2)}) collective-permute-start(bf16[8,64,512]{2,1,0:T(8,128)(2,1)} %get-tuple-element.16), channel_id=1, source_target_pairs={{0,192},{32,224},{64,0},{96,32},{128,64},{160,96},{192,128},{224,1... | collective-permute-start | bytes 1572872 | tf_op jit(solution)/shard_map/ppermute | solution.py:404
  57.4 9.4 %collective-permute-done.7.refs_0_ = bf16[8,64,512]{2,1,0:T(8,128)(2,1)} collective-permute-done((bf16[8,64,512]{2,1,0:T(8,128)(2,1)}, bf16[8,64,512]{2,1,0:T(8,128)(2,1)}, u32[]{:S(2)}, u32[]{:S(2)}) %collective-permute-start.7) | collective-permute-done | bytes 524320 | tf_op jit(solution)/shard_map/ppermute | solution.py:404
  66.8 1.7 collective-permute-done.8.refs_1_
  68.5 2.2 %fill.2.refs_2_ = bf16[8,256,512]{2,1,0:T(8,128)(2,1)} custom-call(bf16[8,64,512]{2,1,0:T(8,128)(2,1)} %collective-permute-done.7.refs_0_, bf16[8,64,512]{2,1,0:T(8,128)(2,1)} %collective-permute-done.8.refs_1_), custom_call_target="tpu_custom_call" | custom-call | bytes 2097152 | tf_op jit(solution)/shard_map/fill/pallas_call | solution.py:390
  70.7 17.8 %collective-permute-done.5.refs_0_ = bf16[8,64,512]{2,1,0:T(8,128)(2,1)S(1)} collective-permute-done((bf16[8,64,512]{2,1,0:T(8,128)(2,1)}, bf16[8,64,512]{2,1,0:T(8,128)(2,1)S(1)}, u32[]{:S(2)}, u32[]{:S(2)}) %collective-permute-start.5) | collective-permute-done | bytes 524320 | tf_op jit(solution)/shard_map/ppermute | solution.py:404
  90.2 2.2 %fill.3 = bf16[8,256,512]{2,1,0:T(8,128)(2,1)} custom-call(bf16[8,64,512]{2,1,0:T(8,128)(2,1)} %copy-done.3, bf16[8,64,512]{2,1,0:T(8,128)(2,1)} %copy-done.4, bf16[8,256,512]{2,1,0:T(8,128)(2,1)} %fill.2.refs_2_), custom_call_target="tpu_custom_call", output_to_operand_aliasing={{}: (2, {})} | custom-call | bytes 2097152 | tf_op jit(solution)/shard_map/fill/pallas_call | solution.py:390
  92.4 4.5 %all-to-all-start.2 = ((bf16[8,256,512]{2,1,0:T(8,128)(2,1)}), bf16[8,256,512]{2,1,0:T(8,128)(2,1)}, u32[]{:S(2)}, u32[]{:S(2)}) async-start(bf16[8,256,512]{2,1,0:T(8,128)(2,1)} %fill.3), calls=%async_computation.2 | async-start | bytes 4194304 | tf_op jit(solution)/shard_map/all_to_all | solution.py:408
  98.9 2.1 %collective-permute-start.2 = (bf16[1024,512]{1,0:T(8,128)(2,1)}, bf16[1024,512]{1,0:T(8,128)(2,1)}, u32[]{:S(2)}, u32[]{:S(2)}) collective-permute-start(bf16[1024,512]{1,0:T(8,128)(2,1)} %own_ref.1), channel_id=1, source_target_pairs={{0,2},{1,3},{2,0},{3,1},{4,6},{5,7},{6,4},{7,5},{8,10},{9,11},{10,... | collective-permute-start | bytes 3145736 | tf_op jit(solution)/shard_map/ppermute | solution.py:404
  101.2 5.0 %collective-permute-start.10 = (bf16[8,32,512]{2,1,0:T(8,128)(2,1)S(1)}, bf16[8,32,512]{2,1,0:T(8,128)(2,1)S(1)}, u32[]{:S(2)}, u32[]{:S(2)}) collective-permute-start(bf16[8,32,512]{2,1,0:T(8,128)(2,1)S(1)} %get-tuple-element.19), channel_id=1, source_target_pairs={{0,160},{32,192},{64,224},{96,0},{128,32},{160,64},{192,96},{224,1... | collective-permute-start | bytes 786440 | tf_op jit(solution)/shard_map/ppermute | solution.py:404
  106.2 17.0 %collective-permute-done.left_ref = bf16[1024,512]{1,0:T(8,128)(2,1)} collective-permute-done((bf16[1024,512]{1,0:T(8,128)(2,1)}, bf16[1024,512]{1,0:T(8,128)(2,1)}, u32[]{:S(2)}, u32[]{:S(2)}) %collective-permute-start) | collective-permute-done | bytes 1048608 | tf_op jit(solution)/shard_map/ppermute | solution.py:404
  124.1 23.0 %collective-permute-done.2.far_ref = bf16[1024,512]{1,0:T(8,128)(2,1)} collective-permute-done((bf16[1024,512]{1,0:T(8,128)(2,1)}, bf16[1024,512]{1,0:T(8,128)(2,1)}, u32[]{:S(2)}, u32[]{:S(2)}) %collective-permute-start.2) | collective-permute-done | bytes 1048608 | tf_op jit(solution)/shard_map/ppermute | solution.py:404
  147.1 15.3 %token_path.1 = (f32[1024,512]{1,0:T(8,128)}, f32[2,2,4,128]{3,2,1,0:T(4,128)}) custom-call(s32[1]{0:T(128)} %bitcast.1.me_ref, bf16[1024,512]{1,0:T(8,128)(2,1)} %own_ref.1, bf16[1024,512]{1,0:T(8,128)(2,1)} %collective-permute-done.left_ref, bf16[1024,512]{1,0:T(8,128)(2,1)} %collective-permute-done.1.right_ref, ...), custom_call_target="tpu_custom_call" | custom-call | flops 4294967296 | bytes 10485760 | tf_op jit(solution)/shard_map/token_path/pallas_call | solution.py:157
  163.1 9.3 %psum.7.stats_ref = f32[2,8,128]{2,1,0:T(8,128)} all-reduce(f32[2,8,128]{2,1,0:T(8,128)S(1)} %bitcast.20), channel_id=1, replica_groups=mesh['z'=8,'y'=4,'c'=2,'tp'=4] {'tp'}, use_global_device_ids=true, to_apply=%region_0.1 | all-reduce | flops 2048 | bytes 16384 | tf_op jit(solution)/shard_map/psum | solution.py:471
  172.4 2.9 %finish.1.conv_ref = f32[1024,512]{1,0:T(8,128)} custom-call(f32[1024,512]{1,0:T(8,128)} %get-tuple-element.12.conv_ref, f32[2,8,128]{2,1,0:T(8,128)} %psum.7.stats_ref, f32[1,512]{1,0:T(1,128)} %bitcast.24), custom_call_target="tpu_custom_call" | custom-call | flops 4194304 | bytes 4194304 | tf_op jit(solution)/shard_map/finish/pallas_call | solution.py:201
  176.1 5.6 %attend.1 = bf16[1024,512]{1,0:T(8,128)(2,1)} custom-call(s32[1]{0:T(128)} %bitcast.plane_ref, s32[32]{0:T(128)} %copy-done.8, f32[1024,512]{1,0:T(8,128)} %finish.1.conv_ref, f32[1,512]{1,0:T(1,128)} %bitcast.25, bf16[8,256,512]{2,1,0:T(8,128)(2,1)} %copy-done, bf16[8,256,512]{2,1,0:T(8,128)(2,1)} %all-to-all-done.2.refs_1_, bf16[8,32,512]{2,1,0:T(8,128)(2,1)} %copy-done.5, ...), custom_call_target="tpu_custom_call" | custom-call | flops 268435456 | bytes 5242880 | tf_op jit(solution)/shard_map/attend/pallas_call | solution.py:310
  (44 shorter events, 9.3 us)
Async XLA Ops:
  0.0 12.7 %copy-start.9 = (s32[16,2]{0,1:T(2,128)S(1)}, s32[16,2]{0,1:T(2,128)}, u32[]{:S(2)}) copy-start(s32[16,2]{0,1:T(2,128)} %param.24) | copy-start | bytes 388
  0.0 12.9 %copy-start.10 = (s32[16,2]{0,1:T(2,128)S(1)}, s32[16,2]{0,1:T(2,128)}, u32[]{:S(2)}) copy-start(s32[16,2]{0,1:T(2,128)} %param.25) | copy-start | bytes 388
  6.8 34.3 %collective-permute-start.3 = (bf16[16,64,512]{2,1,0:T(8,128)(2,1)}, bf16[16,64,512]{2,1,0:T(8,128)(2,1)S(1)}, u32[]{:S(2)}, u32[]{:S(2)}) collective-permute-start(bf16[16,64,512]{2,1,0:T(8,128)(2,1)} %bitcast.16), channel_id=1, source_target_pairs={{0,32},{32,64},{64,96},{96,128},{128,160},{160,192},{192,224},{224... | collective-permute-start | bytes 3145736 | tf_op jit(solution)/shard_map/ppermute | solution.py:404
  8.8 32.4 %collective-permute-start.4 = (bf16[16,64,512]{2,1,0:T(8,128)(2,1)}, bf16[16,64,512]{2,1,0:T(8,128)(2,1)S(1)}, u32[]{:S(2)}, u32[]{:S(2)}) collective-permute-start(bf16[16,64,512]{2,1,0:T(8,128)(2,1)} %bitcast.17), channel_id=1, source_target_pairs={{0,224},{32,0},{64,32},{96,64},{128,96},{160,128},{192,160},{224,1... | collective-permute-start | bytes 3145736 | tf_op jit(solution)/shard_map/ppermute | solution.py:404
  12.9 33.4 %copy-start.8 = (s32[32]{0:T(128)}, s32[32]{0:T(128)S(1)}, u32[]{:S(2)}) copy-start(s32[32]{0:T(128)S(1)} %reshape.46.where_ref) | copy-start | bytes 388
  13.9 27.2 %all-to-all-start = ((s32[64,1,8]{2,1,0:T(1,128)}), s32[64,1,8]{2,1,0:T(1,128)S(1)}, u32[]{:S(2)}, u32[]{:S(2)}) async-start(s32[64,1,8]{2,1,0:T(1,128)} %bitcast.11), calls=%async_computation | async-start | bytes 65536 | tf_op jit(solution)/shard_map/all_to_all | solution.py:408
  41.1 1.0 copy-start.1
  41.1 1.3 copy-start.2
  46.3 46.1 %all-to-all-start.1 = ((bf16[8,256,512]{2,1,0:T(8,128)(2,1)}), bf16[8,256,512]{2,1,0:T(8,128)(2,1)S(1)}, u32[]{:S(2)}, u32[]{:S(2)}) async-start(bf16[8,256,512]{2,1,0:T(8,128)(2,1)} %get-tuple-element.14), calls=%async_computation.1 | async-start | bytes 4194304 | tf_op jit(solution)/shard_map/all_to_all | solution.py:408
  50.0 16.9 %collective-permute-start.7 = (bf16[8,64,512]{2,1,0:T(8,128)(2,1)}, bf16[8,64,512]{2,1,0:T(8,128)(2,1)}, u32[]{:S(2)}, u32[]{:S(2)}) collective-permute-start(bf16[8,64,512]{2,1,0:T(8,128)(2,1)} %get-tuple-element.17), channel_id=1, source_target_pairs={{0,32},{32,64},{64,96},{96,128},{128,160},{160,192},{192,224},{224... | collective-permute-start | bytes 1572872 | tf_op jit(solution)/shard_map/ppermute | solution.py:404
  52.7 15.8 %collective-permute-start.8 = (bf16[8,64,512]{2,1,0:T(8,128)(2,1)}, bf16[8,64,512]{2,1,0:T(8,128)(2,1)}, u32[]{:S(2)}, u32[]{:S(2)}) collective-permute-start(bf16[8,64,512]{2,1,0:T(8,128)(2,1)} %get-tuple-element.18), channel_id=1, source_target_pairs={{0,224},{32,0},{64,32},{96,64},{128,96},{160,128},{192,160},{224,1... | collective-permute-start | bytes 1572872 | tf_op jit(solution)/shard_map/ppermute | solution.py:404
  53.3 35.2 %collective-permute-start.5 = (bf16[8,64,512]{2,1,0:T(8,128)(2,1)}, bf16[8,64,512]{2,1,0:T(8,128)(2,1)S(1)}, u32[]{:S(2)}, u32[]{:S(2)}) collective-permute-start(bf16[8,64,512]{2,1,0:T(8,128)(2,1)} %get-tuple-element.15), channel_id=1, source_target_pairs={{0,64},{32,96},{64,128},{96,160},{128,192},{160,224},{192,0},{224,... | collective-permute-start | bytes 1572872 | tf_op jit(solution)/shard_map/ppermute | solution.py:404
  54.9 34.5 %collective-permute-start.6 = (bf16[8,64,512]{2,1,0:T(8,128)(2,1)}, bf16[8,64,512]{2,1,0:T(8,128)(2,1)S(1)}, u32[]{:S(2)}, u32[]{:S(2)}) collective-permute-start(bf16[8,64,512]{2,1,0:T(8,128)(2,1)} %get-tuple-element.16), channel_id=1, source_target_pairs={{0,192},{32,224},{64,0},{96,32},{128,64},{160,96},{192,128},{224,1... | collective-permute-start | bytes 1572872 | tf_op jit(solution)/shard_map/ppermute | solution.py:404
  88.5 0.9 copy-start.3
  89.4 0.8 copy-start.4
  92.4 8.6 %copy-start = (bf16[8,256,512]{2,1,0:T(8,128)(2,1)}, bf16[8,256,512]{2,1,0:T(8,128)(2,1)S(1)}, u32[]{:S(2)}) copy-start(bf16[8,256,512]{2,1,0:T(8,128)(2,1)S(1)} %all-to-all-done.1.refs_0_) | copy-start | bytes 6291460
  92.4 82.8 %all-to-all-start.2 = ((bf16[8,256,512]{2,1,0:T(8,128)(2,1)}), bf16[8,256,512]{2,1,0:T(8,128)(2,1)}, u32[]{:S(2)}, u32[]{:S(2)}) async-start(bf16[8,256,512]{2,1,0:T(8,128)(2,1)} %fill.3), calls=%async_computation.2 | async-start | bytes 4194304 | tf_op jit(solution)/shard_map/all_to_all | solution.py:408
  96.9 26.4 %collective-permute-start = (bf16[1024,512]{1,0:T(8,128)(2,1)}, bf16[1024,512]{1,0:T(8,128)(2,1)}, u32[]{:S(2)}, u32[]{:S(2)}) collective-permute-start(bf16[1024,512]{1,0:T(8,128)(2,1)} %own_ref.1), channel_id=1, source_target_pairs={{0,1},{1,2},{2,3},{3,0},{4,5},{5,6},{6,7},{7,4},{8,9},{9,10},{10,1... | collective-permute-start | bytes 3145736 | tf_op jit(solution)/shard_map/ppermute | solution.py:404
  98.4 25.7 %collective-permute-start.1 = (bf16[1024,512]{1,0:T(8,128)(2,1)}, bf16[1024,512]{1,0:T(8,128)(2,1)}, u32[]{:S(2)}, u32[]{:S(2)}) collective-permute-start(bf16[1024,512]{1,0:T(8,128)(2,1)} %own_ref.1), channel_id=1, source_target_pairs={{0,3},{1,0},{2,1},{3,2},{4,7},{5,4},{6,5},{7,6},{8,11},{9,8},{10,9... | collective-permute-start | bytes 3145736 | tf_op jit(solution)/shard_map/ppermute | solution.py:404
  98.9 48.1 %collective-permute-start.2 = (bf16[1024,512]{1,0:T(8,128)(2,1)}, bf16[1024,512]{1,0:T(8,128)(2,1)}, u32[]{:S(2)}, u32[]{:S(2)}) collective-permute-start(bf16[1024,512]{1,0:T(8,128)(2,1)} %own_ref.1), channel_id=1, source_target_pairs={{0,2},{1,3},{2,0},{3,1},{4,6},{5,7},{6,4},{7,5},{8,10},{9,11},{10,... | collective-permute-start | bytes 3145736 | tf_op jit(solution)/shard_map/ppermute | solution.py:404
  101.1 74.1 %collective-permute-start.9 = (bf16[8,32,512]{2,1,0:T(8,128)(2,1)S(1)}, bf16[8,32,512]{2,1,0:T(8,128)(2,1)S(1)}, u32[]{:S(2)}, u32[]{:S(2)}) collective-permute-start(bf16[8,32,512]{2,1,0:T(8,128)(2,1)S(1)} %get-tuple-element.20), channel_id=1, source_target_pairs={{0,96},{32,128},{64,160},{96,192},{128,224},{160,0},{192,32},{224,... | collective-permute-start | bytes 786440 | tf_op jit(solution)/shard_map/ppermute | solution.py:404
  101.2 74.0 %collective-permute-start.10 = (bf16[8,32,512]{2,1,0:T(8,128)(2,1)S(1)}, bf16[8,32,512]{2,1,0:T(8,128)(2,1)S(1)}, u32[]{:S(2)}, u32[]{:S(2)}) collective-permute-start(bf16[8,32,512]{2,1,0:T(8,128)(2,1)S(1)} %get-tuple-element.19), channel_id=1, source_target_pairs={{0,160},{32,192},{64,224},{96,0},{128,32},{160,64},{192,96},{224,1... | collective-permute-start | bytes 786440 | tf_op jit(solution)/shard_map/ppermute | solution.py:404
  175.2 0.7 copy-start.5
  175.2 0.9 copy-start.6
  (1 other events, 0.6 us)

commit v5 on v4

--- a/solution.py
+++ b/solution.py
@@ -21,6 +21,9 @@
 ST = ("z", "y", "c")
 LEAD = 32
 ROWS_CHUNK = 64
+KEPT = 48
+NEAR_ROWS = 4 * PROWS + 2 * (PROWS - KEPT)
+AWAY_ROWS = 2 * PROWS + 2 * KEPT
 
 
 def ring(size, step):
@@ -216,7 +219,8 @@
 
 
 def attend_kernel(plane_ref, where_ref, conv_ref, gate_ref, *refs):
-    near_ref, far_ref, upper_ref, lower_ref, out_ref, held_ref, sems = refs
+    near_ref, far_ref, upper_ref, lower_ref, upper_rest_ref, lower_rest_ref = refs[:6]
+    out_ref, held_ref, sems = refs[6:]
     turn = pl.program_id(0)
     count = where_ref.shape[0]
     here = plane_ref[0]
@@ -247,13 +251,28 @@
                     lower_ref.at[column], held_ref.at[n, pl.ds(half, half)], sems.at[n]
                 ).start()
 
-            @pl.when(jnp.logical_not(close) & (away != 4))
+            @pl.when((away == 2) | (away == 6))
             def _():
-                k = jnp.where(away < 4, 2 * away - 3, 12 - 2 * away)
-                at = pl.multiple_of(k * PROWS, PROWS)
+                at = pl.multiple_of(jnp.where(away == 2, PROWS, 0), PROWS)
                 pltpu.make_async_copy(
                     far_ref.at[column, pl.ds(at, PROWS)], held_ref.at[n], sems.at[n]
                 ).start()
+
+            for side, at, rest_ref in (
+                (5, 2 * PROWS, upper_rest_ref),
+                (3, 2 * PROWS + KEPT, lower_rest_ref),
+            ):
+
+                @pl.when(away == side)
+                def _():
+                    pltpu.make_async_copy(
+                        far_ref.at[column, pl.ds(at, KEPT)],
+                        held_ref.at[n, pl.ds(0, KEPT)],
+                        sems.at[n],
+                    ).start()
+                    pltpu.make_async_copy(
+                        rest_ref.at[column], held_ref.at[n, pl.ds(KEPT, PROWS - KEPT)], sems.at[n]
+                    ).start()
 
     blocks = conv_ref.shape[0] // BLOCK
     weight = jax.nn.sigmoid(gate_ref[...])
@@ -330,24 +349,33 @@
         return table_ref[at, lax.rem(here + owner_plane + 8, 8)]
 
     for reader in range(8):
-        for k, (source, owner_plane) in enumerate(((own_ref, 0), (below_ref, -1), (above_ref, 1))):
+        at = 0
+        for source, reader_plane, owner_plane, first, rows in (
+            (own_ref, 0, 0, 0, PROWS),
+            (below_ref, 0, -1, 0, PROWS),
+            (above_ref, 0, 1, 0, PROWS),
+            (below_ref, 3, -1, 0, half),
+            (above_ref, -3, 1, half, half),
+            (below_ref, 2, -1, KEPT, PROWS - KEPT),
+            (above_ref, -2, 1, KEPT, PROWS - KEPT),
+        ):
             pltpu.make_async_copy(
-                source.at[slot(0, reader, owner_plane)],
-                outs[0].at[reader, pl.ds(k * PROWS, PROWS)],
+                source.at[slot(reader_plane, reader, owner_plane), pl.ds(first, rows)],
+                outs[0].at[reader, pl.ds(at, rows)],
                 sems.at[0],
             ).start()
-        for source, side, at in ((below_ref, 1, 0), (above_ref, -1, half)):
-            pltpu.make_async_copy(
-                source.at[slot(3 * side, reader, -side), pl.ds(at, half)],
-                outs[0].at[reader, pl.ds(3 * PROWS + at, half)],
-                sems.at[0],
-            ).start()
+            at += rows
     for reader in range(8):
-        for n, (source, side, steps) in enumerate(
-            ((below_ref, 1, 1), (above_ref, -1, 1), (below_ref, 1, 2), (above_ref, -1, 2))
+        for n, (source, side, steps, rows) in enumerate(
+            (
+                (below_ref, 1, 1, PROWS),
+                (above_ref, -1, 1, PROWS),
+                (below_ref, 1, 2, KEPT),
+                (above_ref, -1, 2, KEPT),
+            )
         ):
             pltpu.make_async_copy(
-                source.at[slot(side * steps, reader, -side)],
+                source.at[slot(side * steps, reader, -side), pl.ds(0, rows)],
                 outs[1 + n].at[reader],
                 sems.at[1 + n],
             ).start()
@@ -356,7 +384,7 @@
 
 
 def pick(plane, table, own, below, above):
-    shapes = [(8, 4 * PROWS)] + [(8, PROWS)] * 4
+    shapes = [(8, NEAR_ROWS), (8, PROWS), (8, PROWS), (8, KEPT), (8, KEPT)]
     return pl.pallas_call(
         pick_kernel,
         in_specs=[pl.BlockSpec(memory_space=pltpu.SMEM)] * 2
@@ -373,10 +401,9 @@
 
 def fill_kernel(*refs, at):
     first_ref, second_ref, out_ref, sems = refs[0], refs[1], refs[-2], refs[-1]
+    rows = first_ref.shape[1]
     copies = [
-        pltpu.make_async_copy(
-            ref, out_ref.at[:, pl.ds((at + n) * PROWS, PROWS)], sems.at[n]
-        )
+        pltpu.make_async_copy(ref, out_ref.at[:, pl.ds(at + n * rows, rows)], sems.at[n])
         for n, ref in enumerate((first_ref, second_ref))
     ]
     for copy in copies:
@@ -393,7 +420,7 @@
         + [pl.BlockSpec(memory_space=pl.ANY)] * len(held),
         out_specs=pl.BlockSpec(memory_space=pl.ANY),
         scratch_shapes=[pltpu.SemaphoreType.DMA((2,))],
-        out_shape=jax.ShapeDtypeStruct((8, 4 * PROWS, 2 * HEAD), jnp.bfloat16),
+        out_shape=jax.ShapeDtypeStruct((8, AWAY_ROWS, 2 * HEAD), jnp.bfloat16),
         input_output_aliases={2: 0} if held else {},
         cost_estimate=pl.CostEstimate(flops=0, transcendentals=0, bytes_accessed=2 << 20),
         name="fill",
@@ -451,11 +478,15 @@
     up2 = shift(up2, "z", 2)
     down2 = shift(down2, "z", -2)
     away = fill(up1, down1, 0)
-    away = fill(up2, down2, 2, away)
+    away = fill(up2, down2, 2 * PROWS, away)
     away = exchange(away, side)
-    split = 3 * PROWS + PROWS // 2
-    upper = shift(near[:, 3 * PROWS : split], "z", 3)
-    lower = shift(near[:, split:], "z", -3)
+    half, rest = PROWS // 2, PROWS - KEPT
+    at = 3 * PROWS
+    upper = shift(near[:, at : at + half], "z", 3)
+    lower = shift(near[:, at + half : at + 2 * half], "z", -3)
+    at = 4 * PROWS
+    upper_rest = shift(near[:, at : at + rest], "z", 2)
+    lower_rest = shift(near[:, at + rest : at + 2 * rest], "z", -2)
 
     convolved, stats = token_path(
         me,
@@ -471,7 +502,7 @@
     stats = lax.psum(stats, "tp")
     stats = stats.transpose(1, 0, 2, 3).reshape(2, -1, 128)
     conv_out = finish(convolved, stats, channel_gain)
-    return attend(plane, asked, conv_out, retrieval_gate, (near, away, upper, lower))
+    return attend(plane, asked, conv_out, retrieval_gate, (near, away, upper, lower, upper_rest, lower_rest))
 
 
 def solution(mesh):

time: 184 us -> 180 us (0.978)
  waiting for transfers between devices: 88.3 us -> 77.2 us
  starting transfers between devices: 40.1 us -> 44.3 us
    ppermute x11 -> x13, waiting for transfers between devices: 70.6 us -> 59.5 us  [shift(): return lax.ppermute(value, axis, ring(lax.axis_size(axis), step))]
    ppermute x11 -> x13, starting transfers between devices: 22.6 us -> 26.7 us  [shift(): return lax.ppermute(value, axis, ring(lax.axis_size(axis), step))]
  transfers between devices with their start and end apart: 14 -> 16, of which waited for: 8 -> 7; matrix products, arithmetic and copies ran while one was open for 1% -> 1% of each run, Pallas kernels for 12% -> 13%
where the time goes in v5:
time: 180 us; the launch traced here: 177 us
  waiting for transfers between devices  77.2 us (43%)
  starting transfers between devices  44.3 us (25%)
  Pallas kernels  38.8 us (22%)
  blocking collectives  10.6 us (6%)
  local copies, waits for them, and re-layouts  5.52 us (3%)
    ppermute x13, waiting for transfers between devices, shift(): return lax.ppermute(value, axis, ring(lax.axis_size(axis), step))  59.5 us
    ppermute x13, starting transfers between devices, shift(): return lax.ppermute(value, axis, ring(lax.axis_size(axis), step))  26.7 us
    all_to_all x3, waiting for transfers between devices, exchange(): return lax.all_to_all(value, axes, split_axis=0, concat_axis=0, tiled=True)  17.7 us
    all_to_all x3, starting transfers between devices, exchange(): return lax.all_to_all(value, axes, split_axis=0, concat_axis=0, tiled=True)  17.6 us
    pallas_call x1, Pallas kernels, token_path(): pl.pallas_call(token_kernel, grid_spec=grid_spec, out_shape=[jax.ShapeDty...  15.3 us
    psum x1, blocking collectives, layer(): stats = lax.psum(stats, 'tp')  10.6 us
    pallas_call x1, Pallas kernels, project_passages(): pl.pallas_call(project_kernel, grid=(count // tile,), in_specs=[pl.BlockS...  6.84 us
    pallas_call x1, Pallas kernels, attend(): pl.pallas_call(attend_kernel, grid_spec=grid_spec, out_shape=jax.ShapeDty...  5.64 us
  transfers between devices with their start and end apart: 16, of which 7 were waited for; matrix products, arithmetic and copies ran while one was open for 1% of the time, Pallas kernels for 13%

profile of v5, /device:TPU:2, one launch (start us, length us, event | category | flops | bytes accessed | tf_op | source)
XLA Modules:
  0.0 176.9 jit_solution(11241960522880293872)
XLA Ops:
  0.0 6.8 %project_passages.1 = bf16[1024,512]{1,0:T(8,128)(2,1)} custom-call(bf16[1024,2048]{1,0:T(8,128)(2,1)} %bitcast.26, f32[1,2048]{1,0:T(1,128)} %bitcast.29, bf16[2048,256]{1,0:T(8,128)(2,1)} %keys_ref.1, bf16[2048,256]{1,0:T(8,128)(2,1)} %values_ref.1), custom_call_target="tpu_custom_call" | custom-call | flops 2147483648 | bytes 7340032 | tf_op jit(solution)/shard_map/project_passages/pallas_call | solution.py:53
  6.8 1.9 %collective-permute-start.3 = (bf16[16,64,512]{2,1,0:T(8,128)(2,1)}, bf16[16,64,512]{2,1,0:T(8,128)(2,1)S(1)}, u32[]{:S(2)}, u32[]{:S(2)}) collective-permute-start(bf16[16,64,512]{2,1,0:T(8,128)(2,1)} %bitcast.16), channel_id=1, source_target_pairs={{0,32},{32,64},{64,96},{96,128},{128,160},{160,192},{192,224},{224... | collective-permute-start | bytes 3145736 | tf_op jit(solution)/shard_map/ppermute | solution.py:431
  8.8 4.0 %collective-permute-start.4 = (bf16[16,64,512]{2,1,0:T(8,128)(2,1)}, bf16[16,64,512]{2,1,0:T(8,128)(2,1)S(1)}, u32[]{:S(2)}, u32[]{:S(2)}) collective-permute-start(bf16[16,64,512]{2,1,0:T(8,128)(2,1)} %bitcast.17), channel_id=1, source_target_pairs={{0,224},{32,0},{64,32},{96,64},{128,96},{160,128},{192,160},{224,1... | collective-permute-start | bytes 3145736 | tf_op jit(solution)/shard_map/ppermute | solution.py:431
  13.9 9.5 %all-to-all-start = ((s32[64,1,8]{2,1,0:T(1,128)}), s32[64,1,8]{2,1,0:T(1,128)S(1)}, u32[]{:S(2)}, u32[]{:S(2)}) async-start(s32[64,1,8]{2,1,0:T(1,128)} %bitcast.11), calls=%async_computation | async-start | bytes 65536 | tf_op jit(solution)/shard_map/all_to_all | solution.py:435
  23.4 17.7 %all-to-all-done = s32[64,1,8]{2,1,0:T(1,128)S(1)} async-done(((s32[64,1,8]{2,1,0:T(1,128)}), s32[64,1,8]{2,1,0:T(1,128)S(1)}, u32[]{:S(2)}, u32[]{:S(2)}) %all-to-all-start) | async-done | bytes 2080 | tf_op jit(solution)/shard_map/all_to_all | solution.py:435
  42.5 3.9 %pick.1 = (bf16[8,288,512]{2,1,0:T(8,128)(2,1)}, bf16[8,64,512]{2,1,0:T(8,128)(2,1)}, bf16[8,64,512]{2,1,0:T(8,128)(2,1)}, bf16[8,48,512]{2,1,0:T(8,128)(2,1)}, bf16[8,48,512]{2,1,0:T(8,128)(2,1)}) custom-call(s32[1]{0:T(128)} %bitcast.plane_ref, s32[64,8]{1,0:T(8,128)} %bitcast.19, bf16[16,64,512]{2,1,0:T(8,128)(2,1)} %bitcast.18, ...), custom_call_target="tpu_custom_call" | custom-call | bytes 8388608 | tf_op jit(solution)/shard_map/pick/pallas_call | solution.py:388
  46.4 3.6 %all-to-all-start.1 = ((bf16[8,288,512]{2,1,0:T(8,128)(2,1)}), bf16[8,288,512]{2,1,0:T(8,128)(2,1)S(1)}, u32[]{:S(2)}, u32[]{:S(2)}) async-start(bf16[8,288,512]{2,1,0:T(8,128)(2,1)} %get-tuple-element.14), calls=%async_computation.1 | async-start | bytes 4718592 | tf_op jit(solution)/shard_map/all_to_all | solution.py:435
  50.0 2.8 %collective-permute-start.7 = (bf16[8,64,512]{2,1,0:T(8,128)(2,1)}, bf16[8,64,512]{2,1,0:T(8,128)(2,1)S(1)}, u32[]{:S(2)}, u32[]{:S(2)}) collective-permute-start(bf16[8,64,512]{2,1,0:T(8,128)(2,1)} %get-tuple-element.17), channel_id=1, source_target_pairs={{0,32},{32,64},{64,96},{96,128},{128,160},{160,192},{192,224},{224... | collective-permute-start | bytes 1572872 | tf_op jit(solution)/shard_map/ppermute | solution.py:431
  54.9 2.6 %collective-permute-start.6 = (bf16[8,48,512]{2,1,0:T(8,128)(2,1)}, bf16[8,48,512]{2,1,0:T(8,128)(2,1)}, u32[]{:S(2)}, u32[]{:S(2)}) collective-permute-start(bf16[8,48,512]{2,1,0:T(8,128)(2,1)} %get-tuple-element.16), channel_id=1, source_target_pairs={{0,192},{32,224},{64,0},{96,32},{128,64},{160,96},{192,128},{224,1... | collective-permute-start | bytes 1179656 | tf_op jit(solution)/shard_map/ppermute | solution.py:431
  57.5 9.3 %collective-permute-done.7.refs_0_ = bf16[8,64,512]{2,1,0:T(8,128)(2,1)S(1)} collective-permute-done((bf16[8,64,512]{2,1,0:T(8,128)(2,1)}, bf16[8,64,512]{2,1,0:T(8,128)(2,1)S(1)}, u32[]{:S(2)}, u32[]{:S(2)}) %collective-permute-start.7) | collective-permute-done | bytes 524320 | tf_op jit(solution)/shard_map/ppermute | solution.py:431
  69.3 2.2 %fill.2.refs_2_ = bf16[8,224,512]{2,1,0:T(8,128)(2,1)} custom-call(bf16[8,64,512]{2,1,0:T(8,128)(2,1)} %copy-done.3, bf16[8,64,512]{2,1,0:T(8,128)(2,1)} %copy-done.4), custom_call_target="tpu_custom_call" | custom-call | bytes 2097152 | tf_op jit(solution)/shard_map/fill/pallas_call | solution.py:417
  71.5 11.6 %collective-permute-done.5.refs_0_ = bf16[8,48,512]{2,1,0:T(8,128)(2,1)} collective-permute-done((bf16[8,48,512]{2,1,0:T(8,128)(2,1)}, bf16[8,48,512]{2,1,0:T(8,128)(2,1)}, u32[]{:S(2)}, u32[]{:S(2)}) %collective-permute-start.5) | collective-permute-done | bytes 393248 | tf_op jit(solution)/shard_map/ppermute | solution.py:431
  84.0 2.1 %fill.3 = bf16[8,224,512]{2,1,0:T(8,128)(2,1)} custom-call(bf16[8,48,512]{2,1,0:T(8,128)(2,1)} %collective-permute-done.5.refs_0_, bf16[8,48,512]{2,1,0:T(8,128)(2,1)} %collective-permute-done.6.refs_1_, bf16[8,224,512]{2,1,0:T(8,128)(2,1)} %fill.2.refs_2_), custom_call_target="tpu_custom_call", output_to_operand_aliasing={{}: (2, {})} | custom-call | bytes 2097152 | tf_op jit(solution)/shard_map/fill/pallas_call | solution.py:417
  86.1 4.5 %all-to-all-start.2 = ((bf16[8,224,512]{2,1,0:T(8,128)(2,1)}), bf16[8,224,512]{2,1,0:T(8,128)(2,1)}, u32[]{:S(2)}, u32[]{:S(2)}) async-start(bf16[8,224,512]{2,1,0:T(8,128)(2,1)} %fill.3), calls=%async_computation.2 | async-start | bytes 3670016 | tf_op jit(solution)/shard_map/all_to_all | solution.py:435
  92.6 2.1 %collective-permute-start.2 = (bf16[1024,512]{1,0:T(8,128)(2,1)}, bf16[1024,512]{1,0:T(8,128)(2,1)}, u32[]{:S(2)}, u32[]{:S(2)}) collective-permute-start(bf16[1024,512]{1,0:T(8,128)(2,1)} %own_ref.1), channel_id=1, source_target_pairs={{0,2},{1,3},{2,0},{3,1},{4,6},{5,7},{6,4},{7,5},{8,10},{9,11},{10,... | collective-permute-start | bytes 3145736 | tf_op jit(solution)/shard_map/ppermute | solution.py:431
  94.8 5.0 %collective-permute-start.10 = (bf16[8,32,512]{2,1,0:T(8,128)(2,1)S(1)}, bf16[8,32,512]{2,1,0:T(8,128)(2,1)S(1)}, u32[]{:S(2)}, u32[]{:S(2)}) collective-permute-start(bf16[8,32,512]{2,1,0:T(8,128)(2,1)S(1)} %get-tuple-element.21), channel_id=1, source_target_pairs={{0,160},{32,192},{64,224},{96,0},{128,32},{160,64},{192,96},{224,1... | collective-permute-start | bytes 786440 | tf_op jit(solution)/shard_map/ppermute | solution.py:431
  100.5 16.4 %collective-permute-done.left_ref = bf16[1024,512]{1,0:T(8,128)(2,1)} collective-permute-done((bf16[1024,512]{1,0:T(8,128)(2,1)}, bf16[1024,512]{1,0:T(8,128)(2,1)}, u32[]{:S(2)}, u32[]{:S(2)}) %collective-permute-start) | collective-permute-done | bytes 1048608 | tf_op jit(solution)/shard_map/ppermute | solution.py:431
  116.9 1.7 collective-permute-start.11
  118.6 2.4 %collective-permute-start.12 = (bf16[8,16,512]{2,1,0:T(8,128)(2,1)S(1)}, bf16[8,16,512]{2,1,0:T(8,128)(2,1)S(1)}, u32[]{:S(2)}, u32[]{:S(2)}) collective-permute-start(bf16[8,16,512]{2,1,0:T(8,128)(2,1)S(1)} %get-tuple-element.19), channel_id=1, source_target_pairs={{0,192},{32,224},{64,0},{96,32},{128,64},{160,96},{192,128},{224,1... | collective-permute-start | bytes 393224 | tf_op jit(solution)/shard_map/ppermute | solution.py:431
  121.0 19.7 %collective-permute-done.2.far_ref = bf16[1024,512]{1,0:T(8,128)(2,1)} collective-permute-done((bf16[1024,512]{1,0:T(8,128)(2,1)}, bf16[1024,512]{1,0:T(8,128)(2,1)}, u32[]{:S(2)}, u32[]{:S(2)}) %collective-permute-start.2) | collective-permute-done | bytes 1048608 | tf_op jit(solution)/shard_map/ppermute | solution.py:431
  140.7 15.3 %token_path.1 = (f32[1024,512]{1,0:T(8,128)}, f32[2,2,4,128]{3,2,1,0:T(4,128)}) custom-call(s32[1]{0:T(128)} %bitcast.1.me_ref, bf16[1024,512]{1,0:T(8,128)(2,1)} %own_ref.1, bf16[1024,512]{1,0:T(8,128)(2,1)} %collective-permute-done.left_ref, bf16[1024,512]{1,0:T(8,128)(2,1)} %collective-permute-done.1.right_ref, ...), custom_call_target="tpu_custom_call" | custom-call | flops 4294967296 | bytes 10485760 | tf_op jit(solution)/shard_map/token_path/pallas_call | solution.py:160
  156.7 10.6 %psum.7.stats_ref = f32[2,8,128]{2,1,0:T(8,128)} all-reduce(f32[2,8,128]{2,1,0:T(8,128)S(1)} %bitcast.20), channel_id=1, replica_groups=mesh['z'=8,'y'=4,'c'=2,'tp'=4] {'tp'}, use_global_device_ids=true, to_apply=%region_0.1 | all-reduce | flops 2048 | bytes 16384 | tf_op jit(solution)/shard_map/psum | solution.py:502
  167.3 2.8 %finish.1.conv_ref = f32[1024,512]{1,0:T(8,128)} custom-call(f32[1024,512]{1,0:T(8,128)} %get-tuple-element.12.conv_ref, f32[2,8,128]{2,1,0:T(8,128)} %psum.7.stats_ref, f32[1,512]{1,0:T(1,128)} %bitcast.24), custom_call_target="tpu_custom_call" | custom-call | flops 4194304 | bytes 4194304 | tf_op jit(solution)/shard_map/finish/pallas_call | solution.py:204
  171.1 5.6 %attend.1 = bf16[1024,512]{1,0:T(8,128)(2,1)} custom-call(s32[1]{0:T(128)} %bitcast.plane_ref, s32[32]{0:T(128)} %copy-done.10, f32[1024,512]{1,0:T(8,128)} %finish.1.conv_ref, f32[1,512]{1,0:T(1,128)} %bitcast.25, bf16[8,288,512]{2,1,0:T(8,128)(2,1)} %copy-done, bf16[8,224,512]{2,1,0:T(8,128)(2,1)} %all-to-all-done.2.refs_1_, ...), custom_call_target="tpu_custom_call" | custom-call | flops 268435456 | bytes 5242880 | tf_op jit(solution)/shard_map/attend/pallas_call | solution.py:329
  (53 shorter events, 12.4 us)
Async XLA Ops:
  0.0 12.7 %copy-start.11 = (s32[16,2]{0,1:T(2,128)S(1)}, s32[16,2]{0,1:T(2,128)}, u32[]{:S(2)}) copy-start(s32[16,2]{0,1:T(2,128)} %param.24) | copy-start | bytes 388
  0.0 12.9 %copy-start.12 = (s32[16,2]{0,1:T(2,128)S(1)}, s32[16,2]{0,1:T(2,128)}, u32[]{:S(2)}) copy-start(s32[16,2]{0,1:T(2,128)} %param.25) | copy-start | bytes 388
  6.8 34.3 %collective-permute-start.3 = (bf16[16,64,512]{2,1,0:T(8,128)(2,1)}, bf16[16,64,512]{2,1,0:T(8,128)(2,1)S(1)}, u32[]{:S(2)}, u32[]{:S(2)}) collective-permute-start(bf16[16,64,512]{2,1,0:T(8,128)(2,1)} %bitcast.16), channel_id=1, source_target_pairs={{0,32},{32,64},{64,96},{96,128},{128,160},{160,192},{192,224},{224... | collective-permute-start | bytes 3145736 | tf_op jit(solution)/shard_map/ppermute | solution.py:431
  8.8 32.4 %collective-permute-start.4 = (bf16[16,64,512]{2,1,0:T(8,128)(2,1)}, bf16[16,64,512]{2,1,0:T(8,128)(2,1)S(1)}, u32[]{:S(2)}, u32[]{:S(2)}) collective-permute-start(bf16[16,64,512]{2,1,0:T(8,128)(2,1)} %bitcast.17), channel_id=1, source_target_pairs={{0,224},{32,0},{64,32},{96,64},{128,96},{160,128},{192,160},{224,1... | collective-permute-start | bytes 3145736 | tf_op jit(solution)/shard_map/ppermute | solution.py:431
  12.9 33.5 %copy-start.10 = (s32[32]{0:T(128)}, s32[32]{0:T(128)S(1)}, u32[]{:S(2)}) copy-start(s32[32]{0:T(128)S(1)} %reshape.46.where_ref) | copy-start | bytes 388
  13.9 27.2 %all-to-all-start = ((s32[64,1,8]{2,1,0:T(1,128)}), s32[64,1,8]{2,1,0:T(1,128)S(1)}, u32[]{:S(2)}, u32[]{:S(2)}) async-start(s32[64,1,8]{2,1,0:T(1,128)} %bitcast.11), calls=%async_computation | async-start | bytes 65536 | tf_op jit(solution)/shard_map/all_to_all | solution.py:435
  41.1 1.0 copy-start.1
  41.1 1.3 copy-start.2
  46.4 39.6 %all-to-all-start.1 = ((bf16[8,288,512]{2,1,0:T(8,128)(2,1)}), bf16[8,288,512]{2,1,0:T(8,128)(2,1)S(1)}, u32[]{:S(2)}, u32[]{:S(2)}) async-start(bf16[8,288,512]{2,1,0:T(8,128)(2,1)} %get-tuple-element.14), calls=%async_computation.1 | async-start | bytes 4718592 | tf_op jit(solution)/shard_map/all_to_all | solution.py:435
  50.0 16.8 %collective-permute-start.7 = (bf16[8,64,512]{2,1,0:T(8,128)(2,1)}, bf16[8,64,512]{2,1,0:T(8,128)(2,1)S(1)}, u32[]{:S(2)}, u32[]{:S(2)}) collective-permute-start(bf16[8,64,512]{2,1,0:T(8,128)(2,1)} %get-tuple-element.17), channel_id=1, source_target_pairs={{0,32},{32,64},{64,96},{96,128},{128,160},{160,192},{192,224},{224... | collective-permute-start | bytes 1572872 | tf_op jit(solution)/shard_map/ppermute | solution.py:431
  52.8 15.7 %collective-permute-start.8 = (bf16[8,64,512]{2,1,0:T(8,128)(2,1)}, bf16[8,64,512]{2,1,0:T(8,128)(2,1)S(1)}, u32[]{:S(2)}, u32[]{:S(2)}) collective-permute-start(bf16[8,64,512]{2,1,0:T(8,128)(2,1)} %get-tuple-element.18), channel_id=1, source_target_pairs={{0,224},{32,0},{64,32},{96,64},{128,96},{160,128},{192,160},{224,1... | collective-permute-start | bytes 1572872 | tf_op jit(solution)/shard_map/ppermute | solution.py:431
  53.4 29.7 %collective-permute-start.5 = (bf16[8,48,512]{2,1,0:T(8,128)(2,1)}, bf16[8,48,512]{2,1,0:T(8,128)(2,1)}, u32[]{:S(2)}, u32[]{:S(2)}) collective-permute-start(bf16[8,48,512]{2,1,0:T(8,128)(2,1)} %get-tuple-element.15), channel_id=1, source_target_pairs={{0,64},{32,96},{64,128},{96,160},{128,192},{160,224},{192,0},{224,... | collective-permute-start | bytes 1179656 | tf_op jit(solution)/shard_map/ppermute | solution.py:431
  54.9 29.0 %collective-permute-start.6 = (bf16[8,48,512]{2,1,0:T(8,128)(2,1)}, bf16[8,48,512]{2,1,0:T(8,128)(2,1)}, u32[]{:S(2)}, u32[]{:S(2)}) collective-permute-start(bf16[8,48,512]{2,1,0:T(8,128)(2,1)} %get-tuple-element.16), channel_id=1, source_target_pairs={{0,192},{32,224},{64,0},{96,32},{128,64},{160,96},{192,128},{224,1... | collective-permute-start | bytes 1179656 | tf_op jit(solution)/shard_map/ppermute | solution.py:431
  66.8 1.7 copy-start.3
  86.1 13.8 %copy-start = (bf16[8,288,512]{2,1,0:T(8,128)(2,1)}, bf16[8,288,512]{2,1,0:T(8,128)(2,1)S(1)}, u32[]{:S(2)}) copy-start(bf16[8,288,512]{2,1,0:T(8,128)(2,1)S(1)} %all-to-all-done.1.refs_0_) | copy-start | bytes 7077892
  86.1 84.1 %all-to-all-start.2 = ((bf16[8,224,512]{2,1,0:T(8,128)(2,1)}), bf16[8,224,512]{2,1,0:T(8,128)(2,1)}, u32[]{:S(2)}, u32[]{:S(2)}) async-start(bf16[8,224,512]{2,1,0:T(8,128)(2,1)} %fill.3), calls=%async_computation.2 | async-start | bytes 3670016 | tf_op jit(solution)/shard_map/all_to_all | solution.py:435
  90.5 26.4 %collective-permute-start = (bf16[1024,512]{1,0:T(8,128)(2,1)}, bf16[1024,512]{1,0:T(8,128)(2,1)}, u32[]{:S(2)}, u32[]{:S(2)}) collective-permute-start(bf16[1024,512]{1,0:T(8,128)(2,1)} %own_ref.1), channel_id=1, source_target_pairs={{0,1},{1,2},{2,3},{3,0},{4,5},{5,6},{6,7},{7,4},{8,9},{9,10},{10,1... | collective-permute-start | bytes 3145736 | tf_op jit(solution)/shard_map/ppermute | solution.py:431
  92.0 26.6 %collective-permute-start.1 = (bf16[1024,512]{1,0:T(8,128)(2,1)}, bf16[1024,512]{1,0:T(8,128)(2,1)}, u32[]{:S(2)}, u32[]{:S(2)}) collective-permute-start(bf16[1024,512]{1,0:T(8,128)(2,1)} %own_ref.1), channel_id=1, source_target_pairs={{0,3},{1,0},{2,1},{3,2},{4,7},{5,4},{6,5},{7,6},{8,11},{9,8},{10,9... | collective-permute-start | bytes 3145736 | tf_op jit(solution)/shard_map/ppermute | solution.py:431
  92.6 48.1 %collective-permute-start.2 = (bf16[1024,512]{1,0:T(8,128)(2,1)}, bf16[1024,512]{1,0:T(8,128)(2,1)}, u32[]{:S(2)}, u32[]{:S(2)}) collective-permute-start(bf16[1024,512]{1,0:T(8,128)(2,1)} %own_ref.1), channel_id=1, source_target_pairs={{0,2},{1,3},{2,0},{3,1},{4,6},{5,7},{6,4},{7,5},{8,10},{9,11},{10,... | collective-permute-start | bytes 3145736 | tf_op jit(solution)/shard_map/ppermute | solution.py:431
  94.7 75.5 %collective-permute-start.9 = (bf16[8,32,512]{2,1,0:T(8,128)(2,1)S(1)}, bf16[8,32,512]{2,1,0:T(8,128)(2,1)S(1)}, u32[]{:S(2)}, u32[]{:S(2)}) collective-permute-start(bf16[8,32,512]{2,1,0:T(8,128)(2,1)S(1)} %get-tuple-element.22), channel_id=1, source_target_pairs={{0,96},{32,128},{64,160},{96,192},{128,224},{160,0},{192,32},{224,... | collective-permute-start | bytes 786440 | tf_op jit(solution)/shard_map/ppermute | solution.py:431
  94.8 75.4 %collective-permute-start.10 = (bf16[8,32,512]{2,1,0:T(8,128)(2,1)S(1)}, bf16[8,32,512]{2,1,0:T(8,128)(2,1)S(1)}, u32[]{:S(2)}, u32[]{:S(2)}) collective-permute-start(bf16[8,32,512]{2,1,0:T(8,128)(2,1)S(1)} %get-tuple-element.21), channel_id=1, source_target_pairs={{0,160},{32,192},{64,224},{96,0},{128,32},{160,64},{192,96},{224,1... | collective-permute-start | bytes 786440 | tf_op jit(solution)/shard_map/ppermute | solution.py:431
  116.9 53.3 %collective-permute-start.11 = (bf16[8,16,512]{2,1,0:T(8,128)(2,1)}, bf16[8,16,512]{2,1,0:T(8,128)(2,1)S(1)}, u32[]{:S(2)}, u32[]{:S(2)}) collective-permute-start(bf16[8,16,512]{2,1,0:T(8,128)(2,1)} %get-tuple-element.20), channel_id=1, source_target_pairs={{0,64},{32,96},{64,128},{96,160},{128,192},{160,224},{192,0},{224,... | collective-permute-start | bytes 393224 | tf_op jit(solution)/shard_map/ppermute | solution.py:431
  118.6 51.5 %collective-permute-start.12 = (bf16[8,16,512]{2,1,0:T(8,128)(2,1)S(1)}, bf16[8,16,512]{2,1,0:T(8,128)(2,1)S(1)}, u32[]{:S(2)}, u32[]{:S(2)}) collective-permute-start(bf16[8,16,512]{2,1,0:T(8,128)(2,1)S(1)} %get-tuple-element.19), channel_id=1, source_target_pairs={{0,192},{32,224},{64,0},{96,32},{128,64},{160,96},{192,128},{224,1... | collective-permute-start | bytes 393224 | tf_op jit(solution)/shard_map/ppermute | solution.py:431
  170.2 0.9 copy-start.6
  (5 other events, 3.6 us)

commit v6 on v5

--- a/solution.py
+++ b/solution.py
@@ -21,7 +21,7 @@
 ST = ("z", "y", "c")
 LEAD = 32
 ROWS_CHUNK = 64
-KEPT = 48
+KEPT = 56
 NEAR_ROWS = 4 * PROWS + 2 * (PROWS - KEPT)
 AWAY_ROWS = 2 * PROWS + 2 * KEPT
 
@@ -219,8 +219,7 @@
 
 
 def attend_kernel(plane_ref, where_ref, conv_ref, gate_ref, *refs):
-    near_ref, far_ref, upper_ref, lower_ref, upper_rest_ref, lower_rest_ref = refs[:6]
-    out_ref, held_ref, sems = refs[6:]
+    near_ref, far_ref, upper_ref, lower_ref, out_ref, held_ref, sems = refs
     turn = pl.program_id(0)
     count = where_ref.shape[0]
     here = plane_ref[0]
@@ -245,10 +244,14 @@
             @pl.when(away == 4)
             def _():
                 pltpu.make_async_copy(
-                    upper_ref.at[column], held_ref.at[n, pl.ds(0, half)], sems.at[n]
+                    upper_ref.at[column, pl.ds(0, half)],
+                    held_ref.at[n, pl.ds(0, half)],
+                    sems.at[n],
                 ).start()
                 pltpu.make_async_copy(
-                    lower_ref.at[column], held_ref.at[n, pl.ds(half, half)], sems.at[n]
+                    lower_ref.at[column, pl.ds(0, half)],
+                    held_ref.at[n, pl.ds(half, half)],
+                    sems.at[n],
                 ).start()
 
             @pl.when((away == 2) | (away == 6))
@@ -259,8 +262,8 @@
                 ).start()
 
             for side, at, rest_ref in (
-                (5, 2 * PROWS, upper_rest_ref),
-                (3, 2 * PROWS + KEPT, lower_rest_ref),
+                (5, 2 * PROWS, upper_ref),
+                (3, 2 * PROWS + KEPT, lower_ref),
             ):
 
                 @pl.when(away == side)
@@ -271,7 +274,9 @@
                         sems.at[n],
                     ).start()
                     pltpu.make_async_copy(
-                        rest_ref.at[column], held_ref.at[n, pl.ds(KEPT, PROWS - KEPT)], sems.at[n]
+                        rest_ref.at[column, pl.ds(half, PROWS - KEPT)],
+                        held_ref.at[n, pl.ds(KEPT, PROWS - KEPT)],
+                        sems.at[n],
                     ).start()
 
     blocks = conv_ref.shape[0] // BLOCK
@@ -355,9 +360,9 @@
             (below_ref, 0, -1, 0, PROWS),
             (above_ref, 0, 1, 0, PROWS),
             (below_ref, 3, -1, 0, half),
+            (own_ref, 3, 0, KEPT, PROWS - KEPT),
             (above_ref, -3, 1, half, half),
-            (below_ref, 2, -1, KEPT, PROWS - KEPT),
-            (above_ref, -2, 1, KEPT, PROWS - KEPT),
+            (own_ref, -3, 0, KEPT, PROWS - KEPT),
         ):
             pltpu.make_async_copy(
                 source.at[slot(reader_plane, reader, owner_plane), pl.ds(first, rows)],
@@ -480,13 +485,9 @@
     away = fill(up1, down1, 0)
     away = fill(up2, down2, 2 * PROWS, away)
     away = exchange(away, side)
-    half, rest = PROWS // 2, PROWS - KEPT
-    at = 3 * PROWS
-    upper = shift(near[:, at : at + half], "z", 3)
-    lower = shift(near[:, at + half : at + 2 * half], "z", -3)
-    at = 4 * PROWS
-    upper_rest = shift(near[:, at : at + rest], "z", 2)
-    lower_rest = shift(near[:, at + rest : at + 2 * rest], "z", -2)
+    split = (3 * PROWS + NEAR_ROWS) // 2
+    upper = shift(near[:, 3 * PROWS : split], "z", 3)
+    lower = shift(near[:, split:], "z", -3)
 
     convolved, stats = token_path(
         me,
@@ -502,7 +503,7 @@
     stats = lax.psum(stats, "tp")
     stats = stats.transpose(1, 0, 2, 3).reshape(2, -1, 128)
     conv_out = finish(convolved, stats, channel_gain)
-    return attend(plane, asked, conv_out, retrieval_gate, (near, away, upper, lower, upper_rest, lower_rest))
+    return attend(plane, asked, conv_out, retrieval_gate, (near, away, upper, lower))
 
 
 def solution(mesh):

time: 180 us -> 180 us (level)
  waiting for transfers between devices: 77.2 us -> 84.8 us
  starting transfers between devices: 44.3 us -> 40.2 us
    ppermute x13 -> x11, waiting for transfers between devices: 59.5 us -> 67.1 us  [shift(): return lax.ppermute(value, axis, ring(lax.axis_size(axis), step))]
    ppermute x13 -> x11, starting transfers between devices: 26.7 us -> 22.6 us  [shift(): return lax.ppermute(value, axis, ring(lax.axis_size(axis), step))]
  transfers between devices with their start and end apart: 16 -> 14, of which waited for: 7 -> 8; matrix products, arithmetic and copies ran while one was open for 1% -> 1% of each run, Pallas kernels for 13% -> 13%
where the time goes in v6:
time: 180 us; the launch traced here: 178 us
  waiting for transfers between devices  84.8 us (47%)
  starting transfers between devices  40.2 us (22%)
  Pallas kernels  38.9 us (22%)
  blocking collectives  9.27 us (5%)
  local copies, waits for them, and re-layouts  4.8 us (3%)
    ppermute x11, waiting for transfers between devices, shift(): return lax.ppermute(value, axis, ring(lax.axis_size(axis), step))  67.1 us
    ppermute x11, starting transfers between devices, shift(): return lax.ppermute(value, axis, ring(lax.axis_size(axis), step))  22.6 us
    all_to_all x3, waiting for transfers between devices, exchange(): return lax.all_to_all(value, axes, split_axis=0, concat_axis=0, tiled=True)  17.7 us
    all_to_all x3, starting transfers between devices, exchange(): return lax.all_to_all(value, axes, split_axis=0, concat_axis=0, tiled=True)  17.6 us
    pallas_call x1, Pallas kernels, token_path(): pl.pallas_call(token_kernel, grid_spec=grid_spec, out_shape=[jax.ShapeDty...  15.3 us
    psum x1, blocking collectives, layer(): stats = lax.psum(stats, 'tp')  9.27 us
    pallas_call x1, Pallas kernels, project_passages(): pl.pallas_call(project_kernel, grid=(count // tile,), in_specs=[pl.BlockS...  6.84 us
    pallas_call x1, Pallas kernels, attend(): pl.pallas_call(attend_kernel, grid_spec=grid_spec, out_shape=jax.ShapeDty...  5.64 us
  transfers between devices with their start and end apart: 14, of which 8 were waited for; matrix products, arithmetic and copies ran while one was open for 1% of the time, Pallas kernels for 13%

profile of v6, /device:TPU:2, one launch (start us, length us, event | category | flops | bytes accessed | tf_op | source)
XLA Modules:
  0.0 178.3 jit_solution(11842210346309672297)
XLA Ops:
  0.0 6.8 %project_passages.1 = bf16[1024,512]{1,0:T(8,128)(2,1)} custom-call(bf16[1024,2048]{1,0:T(8,128)(2,1)} %bitcast.26, f32[1,2048]{1,0:T(1,128)} %bitcast.29, bf16[2048,256]{1,0:T(8,128)(2,1)} %keys_ref.1, bf16[2048,256]{1,0:T(8,128)(2,1)} %values_ref.1), custom_call_target="tpu_custom_call" | custom-call | flops 2147483648 | bytes 7340032 | tf_op jit(solution)/shard_map/project_passages/pallas_call | solution.py:53
  6.8 1.9 %collective-permute-start.3 = (bf16[16,64,512]{2,1,0:T(8,128)(2,1)}, bf16[16,64,512]{2,1,0:T(8,128)(2,1)S(1)}, u32[]{:S(2)}, u32[]{:S(2)}) collective-permute-start(bf16[16,64,512]{2,1,0:T(8,128)(2,1)} %bitcast.16), channel_id=1, source_target_pairs={{0,32},{32,64},{64,96},{96,128},{128,160},{160,192},{192,224},{224... | collective-permute-start | bytes 3145736 | tf_op jit(solution)/shard_map/ppermute | solution.py:436
  8.8 4.0 %collective-permute-start.4 = (bf16[16,64,512]{2,1,0:T(8,128)(2,1)}, bf16[16,64,512]{2,1,0:T(8,128)(2,1)S(1)}, u32[]{:S(2)}, u32[]{:S(2)}) collective-permute-start(bf16[16,64,512]{2,1,0:T(8,128)(2,1)} %bitcast.17), channel_id=1, source_target_pairs={{0,224},{32,0},{64,32},{96,64},{128,96},{160,128},{192,160},{224,1... | collective-permute-start | bytes 3145736 | tf_op jit(solution)/shard_map/ppermute | solution.py:436
  13.9 9.5 %all-to-all-start = ((s32[64,1,8]{2,1,0:T(1,128)}), s32[64,1,8]{2,1,0:T(1,128)S(1)}, u32[]{:S(2)}, u32[]{:S(2)}) async-start(s32[64,1,8]{2,1,0:T(1,128)} %bitcast.11), calls=%async_computation | async-start | bytes 65536 | tf_op jit(solution)/shard_map/all_to_all | solution.py:440
  23.4 17.7 %all-to-all-done = s32[64,1,8]{2,1,0:T(1,128)S(1)} async-done(((s32[64,1,8]{2,1,0:T(1,128)}), s32[64,1,8]{2,1,0:T(1,128)S(1)}, u32[]{:S(2)}, u32[]{:S(2)}) %all-to-all-start) | async-done | bytes 2080 | tf_op jit(solution)/shard_map/all_to_all | solution.py:440
  42.5 3.9 %pick.1 = (bf16[8,272,512]{2,1,0:T(8,128)(2,1)}, bf16[8,64,512]{2,1,0:T(8,128)(2,1)}, bf16[8,64,512]{2,1,0:T(8,128)(2,1)}, bf16[8,56,512]{2,1,0:T(8,128)(2,1)}, bf16[8,56,512]{2,1,0:T(8,128)(2,1)}) custom-call(s32[1]{0:T(128)} %bitcast.plane_ref, s32[64,8]{1,0:T(8,128)} %bitcast.19, bf16[16,64,512]{2,1,0:T(8,128)(2,1)} %bitcast.18, ...), custom_call_target="tpu_custom_call" | custom-call | bytes 8388608 | tf_op jit(solution)/shard_map/pick/pallas_call | solution.py:393
  46.4 3.6 %all-to-all-start.1 = ((bf16[8,272,512]{2,1,0:T(8,128)(2,1)}), bf16[8,272,512]{2,1,0:T(8,128)(2,1)S(1)}, u32[]{:S(2)}, u32[]{:S(2)}) async-start(bf16[8,272,512]{2,1,0:T(8,128)(2,1)} %get-tuple-element.14), calls=%async_computation.1 | async-start | bytes 4456448 | tf_op jit(solution)/shard_map/all_to_all | solution.py:440
  50.0 2.8 %collective-permute-start.7 = (bf16[8,64,512]{2,1,0:T(8,128)(2,1)}, bf16[8,64,512]{2,1,0:T(8,128)(2,1)S(1)}, u32[]{:S(2)}, u32[]{:S(2)}) collective-permute-start(bf16[8,64,512]{2,1,0:T(8,128)(2,1)} %get-tuple-element.17), channel_id=1, source_target_pairs={{0,32},{32,64},{64,96},{96,128},{128,160},{160,192},{192,224},{224... | collective-permute-start | bytes 1572872 | tf_op jit(solution)/shard_map/ppermute | solution.py:436
  53.3 1.6 collective-permute-start.5
  54.9 2.6 %collective-permute-start.6 = (bf16[8,56,512]{2,1,0:T(8,128)(2,1)}, bf16[8,56,512]{2,1,0:T(8,128)(2,1)}, u32[]{:S(2)}, u32[]{:S(2)}) collective-permute-start(bf16[8,56,512]{2,1,0:T(8,128)(2,1)} %get-tuple-element.16), channel_id=1, source_target_pairs={{0,192},{32,224},{64,0},{96,32},{128,64},{160,96},{192,128},{224,1... | collective-permute-start | bytes 1376264 | tf_op jit(solution)/shard_map/ppermute | solution.py:436
  57.5 9.3 %collective-permute-done.7.refs_0_ = bf16[8,64,512]{2,1,0:T(8,128)(2,1)S(1)} collective-permute-done((bf16[8,64,512]{2,1,0:T(8,128)(2,1)}, bf16[8,64,512]{2,1,0:T(8,128)(2,1)S(1)}, u32[]{:S(2)}, u32[]{:S(2)}) %collective-permute-start.7) | collective-permute-done | bytes 524320 | tf_op jit(solution)/shard_map/ppermute | solution.py:436
  66.8 1.7 collective-permute-done.8.refs_1_
  69.3 2.2 %fill.2.refs_2_ = bf16[8,240,512]{2,1,0:T(8,128)(2,1)} custom-call(bf16[8,64,512]{2,1,0:T(8,128)(2,1)} %copy-done.3, bf16[8,64,512]{2,1,0:T(8,128)(2,1)} %copy-done.4), custom_call_target="tpu_custom_call" | custom-call | bytes 2097152 | tf_op jit(solution)/shard_map/fill/pallas_call | solution.py:422
  71.5 14.4 %collective-permute-done.5.refs_0_ = bf16[8,56,512]{2,1,0:T(8,128)(2,1)} collective-permute-done((bf16[8,56,512]{2,1,0:T(8,128)(2,1)}, bf16[8,56,512]{2,1,0:T(8,128)(2,1)}, u32[]{:S(2)}, u32[]{:S(2)}) %collective-permute-start.5) | collective-permute-done | bytes 458784 | tf_op jit(solution)/shard_map/ppermute | solution.py:436
  86.8 2.1 %fill.3 = bf16[8,240,512]{2,1,0:T(8,128)(2,1)} custom-call(bf16[8,56,512]{2,1,0:T(8,128)(2,1)} %collective-permute-done.5.refs_0_, bf16[8,56,512]{2,1,0:T(8,128)(2,1)} %collective-permute-done.6.refs_1_, bf16[8,240,512]{2,1,0:T(8,128)(2,1)} %fill.2.refs_2_), custom_call_target="tpu_custom_call", output_to_operand_aliasing={{}: (2, {})} | custom-call | bytes 2097152 | tf_op jit(solution)/shard_map/fill/pallas_call | solution.py:422
  88.9 4.5 %all-to-all-start.2 = ((bf16[8,240,512]{2,1,0:T(8,128)(2,1)}), bf16[8,240,512]{2,1,0:T(8,128)(2,1)}, u32[]{:S(2)}, u32[]{:S(2)}) async-start(bf16[8,240,512]{2,1,0:T(8,128)(2,1)} %fill.3), calls=%async_computation.2 | async-start | bytes 3932160 | tf_op jit(solution)/shard_map/all_to_all | solution.py:440
  95.4 2.1 %collective-permute-start.2 = (bf16[1024,512]{1,0:T(8,128)(2,1)}, bf16[1024,512]{1,0:T(8,128)(2,1)}, u32[]{:S(2)}, u32[]{:S(2)}) collective-permute-start(bf16[1024,512]{1,0:T(8,128)(2,1)} %own_ref.1), channel_id=1, source_target_pairs={{0,2},{1,3},{2,0},{3,1},{4,6},{5,7},{6,4},{7,5},{8,10},{9,11},{10,... | collective-permute-start | bytes 3145736 | tf_op jit(solution)/shard_map/ppermute | solution.py:436
  97.7 5.0 %collective-permute-start.10 = (bf16[8,40,512]{2,1,0:T(8,128)(2,1)S(1)}, bf16[8,40,512]{2,1,0:T(8,128)(2,1)S(1)}, u32[]{:S(2)}, u32[]{:S(2)}) collective-permute-start(bf16[8,40,512]{2,1,0:T(8,128)(2,1)S(1)} %get-tuple-element.19), channel_id=1, source_target_pairs={{0,160},{32,192},{64,224},{96,0},{128,32},{160,64},{192,96},{224,1... | collective-permute-start | bytes 983048 | tf_op jit(solution)/shard_map/ppermute | solution.py:436
  102.7 17.0 %collective-permute-done.left_ref = bf16[1024,512]{1,0:T(8,128)(2,1)} collective-permute-done((bf16[1024,512]{1,0:T(8,128)(2,1)}, bf16[1024,512]{1,0:T(8,128)(2,1)}, u32[]{:S(2)}, u32[]{:S(2)}) %collective-permute-start) | collective-permute-done | bytes 1048608 | tf_op jit(solution)/shard_map/ppermute | solution.py:436
  120.6 23.0 %collective-permute-done.2.far_ref = bf16[1024,512]{1,0:T(8,128)(2,1)} collective-permute-done((bf16[1024,512]{1,0:T(8,128)(2,1)}, bf16[1024,512]{1,0:T(8,128)(2,1)}, u32[]{:S(2)}, u32[]{:S(2)}) %collective-permute-start.2) | collective-permute-done | bytes 1048608 | tf_op jit(solution)/shard_map/ppermute | solution.py:436
  143.6 15.3 %token_path.1 = (f32[1024,512]{1,0:T(8,128)}, f32[2,2,4,128]{3,2,1,0:T(4,128)}) custom-call(s32[1]{0:T(128)} %bitcast.1.me_ref, bf16[1024,512]{1,0:T(8,128)(2,1)} %own_ref.1, bf16[1024,512]{1,0:T(8,128)(2,1)} %collective-permute-done.left_ref, bf16[1024,512]{1,0:T(8,128)(2,1)} %collective-permute-done.1.right_ref, ...), custom_call_target="tpu_custom_call" | custom-call | flops 4294967296 | bytes 10485760 | tf_op jit(solution)/shard_map/token_path/pallas_call | solution.py:160
  159.6 9.3 %psum.7.stats_ref = f32[2,8,128]{2,1,0:T(8,128)} all-reduce(f32[2,8,128]{2,1,0:T(8,128)S(1)} %bitcast.20), channel_id=1, replica_groups=mesh['z'=8,'y'=4,'c'=2,'tp'=4] {'tp'}, use_global_device_ids=true, to_apply=%region_0.1 | all-reduce | flops 2048 | bytes 16384 | tf_op jit(solution)/shard_map/psum | solution.py:503
  168.8 2.8 %finish.1.conv_ref = f32[1024,512]{1,0:T(8,128)} custom-call(f32[1024,512]{1,0:T(8,128)} %get-tuple-element.12.conv_ref, f32[2,8,128]{2,1,0:T(8,128)} %psum.7.stats_ref, f32[1,512]{1,0:T(1,128)} %bitcast.24), custom_call_target="tpu_custom_call" | custom-call | flops 4194304 | bytes 4194304 | tf_op jit(solution)/shard_map/finish/pallas_call | solution.py:204
  172.5 5.6 %attend.1 = bf16[1024,512]{1,0:T(8,128)(2,1)} custom-call(s32[1]{0:T(128)} %bitcast.plane_ref, s32[32]{0:T(128)} %copy-done.8, f32[1024,512]{1,0:T(8,128)} %finish.1.conv_ref, f32[1,512]{1,0:T(1,128)} %bitcast.25, bf16[8,272,512]{2,1,0:T(8,128)(2,1)} %copy-done, bf16[8,240,512]{2,1,0:T(8,128)(2,1)} %all-to-all-done.2.refs_1_, bf16[8,40,512]{2,1,0:T(8,128)(2,1)} %copy-done.5, ...), custom_call_target="tpu_custom_call" | custom-call | flops 268435456 | bytes 5242880 | tf_op jit(solution)/shard_map/attend/pallas_call | solution.py:334
  (44 shorter events, 9.4 us)
Async XLA Ops:
  0.0 12.7 %copy-start.9 = (s32[16,2]{0,1:T(2,128)S(1)}, s32[16,2]{0,1:T(2,128)}, u32[]{:S(2)}) copy-start(s32[16,2]{0,1:T(2,128)} %param.24) | copy-start | bytes 388
  0.0 12.9 %copy-start.10 = (s32[16,2]{0,1:T(2,128)S(1)}, s32[16,2]{0,1:T(2,128)}, u32[]{:S(2)}) copy-start(s32[16,2]{0,1:T(2,128)} %param.25) | copy-start | bytes 388
  6.8 34.3 %collective-permute-start.3 = (bf16[16,64,512]{2,1,0:T(8,128)(2,1)}, bf16[16,64,512]{2,1,0:T(8,128)(2,1)S(1)}, u32[]{:S(2)}, u32[]{:S(2)}) collective-permute-start(bf16[16,64,512]{2,1,0:T(8,128)(2,1)} %bitcast.16), channel_id=1, source_target_pairs={{0,32},{32,64},{64,96},{96,128},{128,160},{160,192},{192,224},{224... | collective-permute-start | bytes 3145736 | tf_op jit(solution)/shard_map/ppermute | solution.py:436
  8.8 32.4 %collective-permute-start.4 = (bf16[16,64,512]{2,1,0:T(8,128)(2,1)}, bf16[16,64,512]{2,1,0:T(8,128)(2,1)S(1)}, u32[]{:S(2)}, u32[]{:S(2)}) collective-permute-start(bf16[16,64,512]{2,1,0:T(8,128)(2,1)} %bitcast.17), channel_id=1, source_target_pairs={{0,224},{32,0},{64,32},{96,64},{128,96},{160,128},{192,160},{224,1... | collective-permute-start | bytes 3145736 | tf_op jit(solution)/shard_map/ppermute | solution.py:436
  12.9 33.5 %copy-start.8 = (s32[32]{0:T(128)}, s32[32]{0:T(128)S(1)}, u32[]{:S(2)}) copy-start(s32[32]{0:T(128)S(1)} %reshape.46.where_ref) | copy-start | bytes 388
  13.9 27.2 %all-to-all-start = ((s32[64,1,8]{2,1,0:T(1,128)}), s32[64,1,8]{2,1,0:T(1,128)S(1)}, u32[]{:S(2)}, u32[]{:S(2)}) async-start(s32[64,1,8]{2,1,0:T(1,128)} %bitcast.11), calls=%async_computation | async-start | bytes 65536 | tf_op jit(solution)/shard_map/all_to_all | solution.py:440
  41.1 1.0 copy-start.1
  41.1 1.3 copy-start.2
  46.4 42.5 %all-to-all-start.1 = ((bf16[8,272,512]{2,1,0:T(8,128)(2,1)}), bf16[8,272,512]{2,1,0:T(8,128)(2,1)S(1)}, u32[]{:S(2)}, u32[]{:S(2)}) async-start(bf16[8,272,512]{2,1,0:T(8,128)(2,1)} %get-tuple-element.14), calls=%async_computation.1 | async-start | bytes 4456448 | tf_op jit(solution)/shard_map/all_to_all | solution.py:440
  50.0 16.8 %collective-permute-start.7 = (bf16[8,64,512]{2,1,0:T(8,128)(2,1)}, bf16[8,64,512]{2,1,0:T(8,128)(2,1)S(1)}, u32[]{:S(2)}, u32[]{:S(2)}) collective-permute-start(bf16[8,64,512]{2,1,0:T(8,128)(2,1)} %get-tuple-element.17), channel_id=1, source_target_pairs={{0,32},{32,64},{64,96},{96,128},{128,160},{160,192},{192,224},{224... | collective-permute-start | bytes 1572872 | tf_op jit(solution)/shard_map/ppermute | solution.py:436
  52.8 15.7 %collective-permute-start.8 = (bf16[8,64,512]{2,1,0:T(8,128)(2,1)}, bf16[8,64,512]{2,1,0:T(8,128)(2,1)S(1)}, u32[]{:S(2)}, u32[]{:S(2)}) collective-permute-start(bf16[8,64,512]{2,1,0:T(8,128)(2,1)} %get-tuple-element.18), channel_id=1, source_target_pairs={{0,224},{32,0},{64,32},{96,64},{128,96},{160,128},{192,160},{224,1... | collective-permute-start | bytes 1572872 | tf_op jit(solution)/shard_map/ppermute | solution.py:436
  53.3 32.5 %collective-permute-start.5 = (bf16[8,56,512]{2,1,0:T(8,128)(2,1)}, bf16[8,56,512]{2,1,0:T(8,128)(2,1)}, u32[]{:S(2)}, u32[]{:S(2)}) collective-permute-start(bf16[8,56,512]{2,1,0:T(8,128)(2,1)} %get-tuple-element.15), channel_id=1, source_target_pairs={{0,64},{32,96},{64,128},{96,160},{128,192},{160,224},{192,0},{224,... | collective-permute-start | bytes 1376264 | tf_op jit(solution)/shard_map/ppermute | solution.py:436
  54.9 31.8 %collective-permute-start.6 = (bf16[8,56,512]{2,1,0:T(8,128)(2,1)}, bf16[8,56,512]{2,1,0:T(8,128)(2,1)}, u32[]{:S(2)}, u32[]{:S(2)}) collective-permute-start(bf16[8,56,512]{2,1,0:T(8,128)(2,1)} %get-tuple-element.16), channel_id=1, source_target_pairs={{0,192},{32,224},{64,0},{96,32},{128,64},{160,96},{192,128},{224,1... | collective-permute-start | bytes 1376264 | tf_op jit(solution)/shard_map/ppermute | solution.py:436
  66.8 1.7 copy-start.3
  68.5 0.8 copy-start.4
  88.9 8.7 %copy-start = (bf16[8,272,512]{2,1,0:T(8,128)(2,1)}, bf16[8,272,512]{2,1,0:T(8,128)(2,1)S(1)}, u32[]{:S(2)}) copy-start(bf16[8,272,512]{2,1,0:T(8,128)(2,1)S(1)} %all-to-all-done.1.refs_0_) | copy-start | bytes 6684676
  88.9 82.8 %all-to-all-start.2 = ((bf16[8,240,512]{2,1,0:T(8,128)(2,1)}), bf16[8,240,512]{2,1,0:T(8,128)(2,1)}, u32[]{:S(2)}, u32[]{:S(2)}) async-start(bf16[8,240,512]{2,1,0:T(8,128)(2,1)} %fill.3), calls=%async_computation.2 | async-start | bytes 3932160 | tf_op jit(solution)/shard_map/all_to_all | solution.py:440
  93.4 26.4 %collective-permute-start = (bf16[1024,512]{1,0:T(8,128)(2,1)}, bf16[1024,512]{1,0:T(8,128)(2,1)}, u32[]{:S(2)}, u32[]{:S(2)}) collective-permute-start(bf16[1024,512]{1,0:T(8,128)(2,1)} %own_ref.1), channel_id=1, source_target_pairs={{0,1},{1,2},{2,3},{3,0},{4,5},{5,6},{6,7},{7,4},{8,9},{9,10},{10,1... | collective-permute-start | bytes 3145736 | tf_op jit(solution)/shard_map/ppermute | solution.py:436
  94.9 25.7 %collective-permute-start.1 = (bf16[1024,512]{1,0:T(8,128)(2,1)}, bf16[1024,512]{1,0:T(8,128)(2,1)}, u32[]{:S(2)}, u32[]{:S(2)}) collective-permute-start(bf16[1024,512]{1,0:T(8,128)(2,1)} %own_ref.1), channel_id=1, source_target_pairs={{0,3},{1,0},{2,1},{3,2},{4,7},{5,4},{6,5},{7,6},{8,11},{9,8},{10,9... | collective-permute-start | bytes 3145736 | tf_op jit(solution)/shard_map/ppermute | solution.py:436
  95.4 48.1 %collective-permute-start.2 = (bf16[1024,512]{1,0:T(8,128)(2,1)}, bf16[1024,512]{1,0:T(8,128)(2,1)}, u32[]{:S(2)}, u32[]{:S(2)}) collective-permute-start(bf16[1024,512]{1,0:T(8,128)(2,1)} %own_ref.1), channel_id=1, source_target_pairs={{0,2},{1,3},{2,0},{3,1},{4,6},{5,7},{6,4},{7,5},{8,10},{9,11},{10,... | collective-permute-start | bytes 3145736 | tf_op jit(solution)/shard_map/ppermute | solution.py:436
  97.6 74.1 %collective-permute-start.9 = (bf16[8,40,512]{2,1,0:T(8,128)(2,1)S(1)}, bf16[8,40,512]{2,1,0:T(8,128)(2,1)S(1)}, u32[]{:S(2)}, u32[]{:S(2)}) collective-permute-start(bf16[8,40,512]{2,1,0:T(8,128)(2,1)S(1)} %get-tuple-element.20), channel_id=1, source_target_pairs={{0,96},{32,128},{64,160},{96,192},{128,224},{160,0},{192,32},{224,... | collective-permute-start | bytes 983048 | tf_op jit(solution)/shard_map/ppermute | solution.py:436
  97.7 74.0 %collective-permute-start.10 = (bf16[8,40,512]{2,1,0:T(8,128)(2,1)S(1)}, bf16[8,40,512]{2,1,0:T(8,128)(2,1)S(1)}, u32[]{:S(2)}, u32[]{:S(2)}) collective-permute-start(bf16[8,40,512]{2,1,0:T(8,128)(2,1)S(1)} %get-tuple-element.19), channel_id=1, source_target_pairs={{0,160},{32,192},{64,224},{96,0},{128,32},{160,64},{192,96},{224,1... | collective-permute-start | bytes 983048 | tf_op jit(solution)/shard_map/ppermute | solution.py:436
  171.7 0.7 copy-start.5
  171.7 0.8 copy-start.6
  (1 other events, 0.6 us)

commit v7 on v6

--- a/solution.py
+++ b/solution.py
@@ -30,6 +30,14 @@
     return [(i, (i + step) % size) for i in range(size)]
 
 
+def in_vmem(*values):
+    return [pltpu.with_memory_space_constraint(value, pltpu.VMEM) for value in values]
+
+
+def in_hbm(*values):
+    return [pltpu.with_memory_space_constraint(value, pltpu.HBM) for value in values]
+
+
 def whole(shape):
     return pl.BlockSpec(shape, lambda *_: (0,) * len(shape))
 
@@ -64,8 +72,9 @@
         cost_estimate=pl.CostEstimate(
             flops=4 * count * D * HEAD, transcendentals=0, bytes_accessed=7 << 20
         ),
+        compiler_params=pltpu.CompilerParams(vmem_limit_bytes=16 << 20),
         name="project_passages",
-    )(rows, gain.reshape(1, D), keys_weight, values_weight)
+    )(*in_hbm(rows), gain.reshape(1, D), *in_hbm(keys_weight, values_weight))
 
 
 def token_kernel(
@@ -161,23 +170,26 @@
         token_kernel,
         grid_spec=grid_spec,
         out_shape=[
-            jax.ShapeDtypeStruct((rows, width), jnp.float32),
+            pltpu.HBM((rows, width), jnp.float32),
             jax.ShapeDtypeStruct((rows // LENGTH, 2, LENGTH // 128, 128), jnp.float32),
         ],
         cost_estimate=pl.CostEstimate(
             flops=4 * rows * D * width, transcendentals=rows * width, bytes_accessed=10 << 20
         ),
+        compiler_params=pltpu.CompilerParams(vmem_limit_bytes=40 << 20),
         name="token_path",
     )(
         me,
-        own,
-        left,
-        right,
-        far,
-        gain.reshape(4, 1, width),
-        inner_weight.reshape(4, width, width),
-        gating_weight.reshape(4, width, width),
-        taps,
+        *in_hbm(
+            own,
+            left,
+            right,
+            far,
+            gain.reshape(4, 1, width),
+            inner_weight.reshape(4, width, width),
+            gating_weight.reshape(4, width, width),
+            taps,
+        ),
     )
 
 
@@ -210,12 +222,13 @@
             whole((1, width)),
         ],
         out_specs=pl.BlockSpec((tile, width), lambda i: (i, 0)),
-        out_shape=jax.ShapeDtypeStruct((rows, width), jnp.float32),
+        out_shape=pltpu.HBM((rows, width), jnp.float32),
         cost_estimate=pl.CostEstimate(
             flops=8 * rows * width, transcendentals=rows * width, bytes_accessed=4 << 20
         ),
+        compiler_params=pltpu.CompilerParams(vmem_limit_bytes=14 << 20),
         name="finish",
-    )(convolved, stats, channel_gain.reshape(1, width))
+    )(*in_hbm(convolved), stats, channel_gain.reshape(1, width))
 
 
 def attend_kernel(plane_ref, where_ref, conv_ref, gate_ref, *refs):
@@ -340,8 +353,9 @@
             transcendentals=rows * 2 * PB * PROWS,
             bytes_accessed=5 << 20,
         ),
+        compiler_params=pltpu.CompilerParams(vmem_limit_bytes=16 << 20),
         name="attend",
-    )(plane, where, conv_out, retrieval_gate.reshape(1, width), *groups)
+    )(plane, where, *in_hbm(conv_out), retrieval_gate.reshape(1, width), *in_vmem(*groups))
 
 
 def pick_kernel(plane_ref, table_ref, own_ref, below_ref, above_ref, *refs):
@@ -393,15 +407,16 @@
     return pl.pallas_call(
         pick_kernel,
         in_specs=[pl.BlockSpec(memory_space=pltpu.SMEM)] * 2
-        + [pl.BlockSpec(memory_space=pltpu.VMEM)] * 3,
+        + [pl.BlockSpec(memory_space=pl.ANY)] * 3,
         out_specs=[pl.BlockSpec(memory_space=pl.ANY)] * len(shapes),
         scratch_shapes=[pltpu.SemaphoreType.DMA((len(shapes),))],
         out_shape=[
-            jax.ShapeDtypeStruct((*shape, 2 * HEAD), jnp.bfloat16) for shape in shapes
+            pltpu.HBM((*shape, 2 * HEAD), jnp.bfloat16) for shape in shapes
         ],
         cost_estimate=pl.CostEstimate(flops=0, transcendentals=0, bytes_accessed=8 << 20),
+        compiler_params=pltpu.CompilerParams(vmem_limit_bytes=2 << 20),
         name="pick",
-    )(plane, table, own, below, above)
+    )(plane, table, *in_vmem(own, below, above))
 
 
 def fill_kernel(*refs, at):
@@ -421,15 +436,15 @@
     held = [] if into is None else [into]
     return pl.pallas_call(
         functools.partial(fill_kernel, at=at),
-        in_specs=[pl.BlockSpec(memory_space=pltpu.VMEM)] * 2
-        + [pl.BlockSpec(memory_space=pl.ANY)] * len(held),
+        in_specs=[pl.BlockSpec(memory_space=pl.ANY)] * (2 + len(held)),
         out_specs=pl.BlockSpec(memory_space=pl.ANY),
         scratch_shapes=[pltpu.SemaphoreType.DMA((2,))],
-        out_shape=jax.ShapeDtypeStruct((8, AWAY_ROWS, 2 * HEAD), jnp.bfloat16),
+        out_shape=pltpu.HBM((8, AWAY_ROWS, 2 * HEAD), jnp.bfloat16),
         input_output_aliases={2: 0} if held else {},
         cost_estimate=pl.CostEstimate(flops=0, transcendentals=0, bytes_accessed=2 << 20),
+        compiler_params=pltpu.CompilerParams(vmem_limit_bytes=2 << 20),
         name="fill",
-    )(first, second, *held)
+    )(*in_vmem(first, second), *in_hbm(*held))
 
 
 def shift(value, axis, step):

time: 180 us -> 176 us (0.978)
  Pallas kernels: 38.9 us -> 36 us
  local copies, waits for them, and re-layouts: 4.8 us -> 2.62 us
    pallas_call x2, Pallas kernels: 4.33 us -> 1.97 us  [fill(): pl.pallas_call(functools.partial(fill_kernel, at=at), in_specs=[pl.BlockS...]
    unnamed x24 -> x16, local copies, waits for them, and re-layouts: 3.12 us -> 0.89 us
  transfers between devices with their start and end apart: 14 -> 14, of which waited for: 8 -> 8; matrix products, arithmetic and copies ran while one was open for 1% -> 1% of each run, Pallas kernels for 13% -> 12%
where the time goes in v7:
time: 176 us; the launch traced here: 174 us
  waiting for transfers between devices  85.7 us (49%)
  starting transfers between devices  40.3 us (23%)
  Pallas kernels  36 us (20%)
  blocking collectives  8.71 us (5%)
  local copies, waits for them, and re-layouts  2.62 us (1%)
    ppermute x11, waiting for transfers between devices, shift(): return lax.ppermute(value, axis, ring(lax.axis_size(axis), step))  68.2 us
    ppermute x11, starting transfers between devices, shift(): return lax.ppermute(value, axis, ring(lax.axis_size(axis), step))  22.7 us
    all_to_all x3, starting transfers between devices, exchange(): return lax.all_to_all(value, axes, split_axis=0, concat_axis=0, tiled=True)  17.6 us
    all_to_all x3, waiting for transfers between devices, exchange(): return lax.all_to_all(value, axes, split_axis=0, concat_axis=0, tiled=True)  17.5 us
    pallas_call x1, Pallas kernels, token_path(): pl.pallas_call(token_kernel, grid_spec=grid_spec, out_shape=[pltpu.HBM((r...  15.4 us
    psum x1, blocking collectives, layer(): stats = lax.psum(stats, 'tp')  8.71 us
    pallas_call x1, Pallas kernels, attend(): pl.pallas_call(attend_kernel, grid_spec=grid_spec, out_shape=jax.ShapeDty...  6.71 us
    pallas_call x1, Pallas kernels, project_passages(): pl.pallas_call(project_kernel, grid=(count // tile,), in_specs=[pl.BlockS...  6.01 us
  transfers between devices with their start and end apart: 14, of which 8 were waited for; matrix products, arithmetic and copies ran while one was open for 1% of the time, Pallas kernels for 12%

profile of v7, /device:TPU:2, one launch (start us, length us, event | category | flops | bytes accessed | tf_op | source)
XLA Modules:
  0.0 173.7 jit_solution(10175501746297032106)
XLA Ops:
  0.7 6.0 %project_passages.1 = bf16[1024,512]{1,0:T(8,128)(2,1)S(1)} custom-call(bf16[1024,2048]{1,0:T(8,128)(2,1)} %bitcast.27, f32[1,2048]{1,0:T(1,128)S(1)} %bitcast.23, bf16[2048,256]{1,0:T(8,128)(2,1)} %keys_ref.1, bf16[2048,256]{1,0:T(8,128)(2,1)} %values_ref.1), custom_call_target="tpu_custom_call" | custom-call | flops 2147483648 | bytes 7340032 | tf_op jit(solution)/shard_map/project_passages/pallas_call | solution.py:61
  6.7 2.0 %collective-permute-start.3 = (bf16[16,64,512]{2,1,0:T(8,128)(2,1)S(1)}, bf16[16,64,512]{2,1,0:T(8,128)(2,1)S(1)}, u32[]{:S(2)}, u32[]{:S(2)}) collective-permute-start(bf16[16,64,512]{2,1,0:T(8,128)(2,1)S(1)} %bitcast.16), channel_id=1, source_target_pairs={{0,32},{32,64},{64,96},{96,128},{128,160},{160,192},{192,224},{224... | collective-permute-start | bytes 3145736 | tf_op jit(solution)/shard_map/ppermute | solution.py:451
  8.7 4.0 %collective-permute-start.4 = (bf16[16,64,512]{2,1,0:T(8,128)(2,1)S(1)}, bf16[16,64,512]{2,1,0:T(8,128)(2,1)S(1)}, u32[]{:S(2)}, u32[]{:S(2)}) collective-permute-start(bf16[16,64,512]{2,1,0:T(8,128)(2,1)S(1)} %bitcast.17), channel_id=1, source_target_pairs={{0,224},{32,0},{64,32},{96,64},{128,96},{160,128},{192,160},{224,1... | collective-permute-start | bytes 3145736 | tf_op jit(solution)/shard_map/ppermute | solution.py:451
  14.0 9.4 %all-to-all-start = ((s32[64,1,8]{2,1,0:T(1,128)}), s32[64,1,8]{2,1,0:T(1,128)S(1)}, u32[]{:S(2)}, u32[]{:S(2)}) async-start(s32[64,1,8]{2,1,0:T(1,128)} %bitcast.11), calls=%async_computation | async-start | bytes 65536 | tf_op jit(solution)/shard_map/all_to_all | solution.py:455
  23.4 17.5 %all-to-all-done = s32[64,1,8]{2,1,0:T(1,128)S(1)} async-done(((s32[64,1,8]{2,1,0:T(1,128)}), s32[64,1,8]{2,1,0:T(1,128)S(1)}, u32[]{:S(2)}, u32[]{:S(2)}) %all-to-all-start) | async-done | bytes 2080 | tf_op jit(solution)/shard_map/all_to_all | solution.py:455
  40.9 3.1 %pick.1 = (bf16[8,272,512]{2,1,0:T(8,128)(2,1)}, bf16[8,64,512]{2,1,0:T(8,128)(2,1)}, bf16[8,64,512]{2,1,0:T(8,128)(2,1)}, bf16[8,56,512]{2,1,0:T(8,128)(2,1)}, bf16[8,56,512]{2,1,0:T(8,128)(2,1)}) custom-call(s32[1]{0:T(128)} %bitcast.plane_ref, s32[64,8]{1,0:T(8,128)S(1)} %bitcast.19, bf16[16,64,512]{2,1,0:T(8,128)(2,1)S(1)} %bitcast.18, ...), custom_call_target="tpu_custom_call" | custom-call | bytes 8388608 | tf_op jit(solution)/shard_map/pick/pallas_call | solution.py:407
  44.0 3.8 %all-to-all-start.1 = ((bf16[8,272,512]{2,1,0:T(8,128)(2,1)}), bf16[8,272,512]{2,1,0:T(8,128)(2,1)S(1)}, u32[]{:S(2)}, u32[]{:S(2)}) async-start(bf16[8,272,512]{2,1,0:T(8,128)(2,1)} %get-tuple-element.14), calls=%async_computation.1 | async-start | bytes 4456448 | tf_op jit(solution)/shard_map/all_to_all | solution.py:455
  47.8 2.8 %collective-permute-start.7 = (bf16[8,64,512]{2,1,0:T(8,128)(2,1)S(1)}, bf16[8,64,512]{2,1,0:T(8,128)(2,1)S(1)}, u32[]{:S(2)}, u32[]{:S(2)}) collective-permute-start(bf16[8,64,512]{2,1,0:T(8,128)(2,1)S(1)} %copy-done.6), channel_id=1, source_target_pairs={{0,32},{32,64},{64,96},{96,128},{128,160},{160,192},{192,224},{224... | collective-permute-start | bytes 1572872 | tf_op jit(solution)/shard_map/ppermute | solution.py:451
  51.1 1.6 collective-permute-start.5
  52.7 2.5 %collective-permute-start.6 = (bf16[8,56,512]{2,1,0:T(8,128)(2,1)}, bf16[8,56,512]{2,1,0:T(8,128)(2,1)S(1)}, u32[]{:S(2)}, u32[]{:S(2)}) collective-permute-start(bf16[8,56,512]{2,1,0:T(8,128)(2,1)} %get-tuple-element.16), channel_id=1, source_target_pairs={{0,192},{32,224},{64,0},{96,32},{128,64},{160,96},{192,128},{224,1... | collective-permute-start | bytes 1376264 | tf_op jit(solution)/shard_map/ppermute | solution.py:451
  55.2 9.1 %collective-permute-done.7.refs_0_ = bf16[8,64,512]{2,1,0:T(8,128)(2,1)S(1)} collective-permute-done((bf16[8,64,512]{2,1,0:T(8,128)(2,1)S(1)}, bf16[8,64,512]{2,1,0:T(8,128)(2,1)S(1)}, u32[]{:S(2)}, u32[]{:S(2)}) %collective-permute-start.7) | collective-permute-done | bytes 524320 | tf_op jit(solution)/shard_map/ppermute | solution.py:451
  64.3 1.7 collective-permute-done.8.refs_1_
  66.0 1.0 fill.2.refs_2_
  67.0 16.2 %collective-permute-done.5.refs_0_ = bf16[8,56,512]{2,1,0:T(8,128)(2,1)S(1)} collective-permute-done((bf16[8,56,512]{2,1,0:T(8,128)(2,1)}, bf16[8,56,512]{2,1,0:T(8,128)(2,1)S(1)}, u32[]{:S(2)}, u32[]{:S(2)}) %collective-permute-start.5) | collective-permute-done | bytes 458784 | tf_op jit(solution)/shard_map/ppermute | solution.py:451
  85.2 4.5 %all-to-all-start.2 = ((bf16[8,240,512]{2,1,0:T(8,128)(2,1)}), bf16[8,240,512]{2,1,0:T(8,128)(2,1)}, u32[]{:S(2)}, u32[]{:S(2)}) async-start(bf16[8,240,512]{2,1,0:T(8,128)(2,1)} %fill.3), calls=%async_computation.2 | async-start | bytes 3932160 | tf_op jit(solution)/shard_map/all_to_all | solution.py:455
  89.6 1.5 collective-permute-start
  91.7 2.1 %collective-permute-start.2 = (bf16[1024,512]{1,0:T(8,128)(2,1)}, bf16[1024,512]{1,0:T(8,128)(2,1)}, u32[]{:S(2)}, u32[]{:S(2)}) collective-permute-start(bf16[1024,512]{1,0:T(8,128)(2,1)} %own_ref.1), channel_id=1, source_target_pairs={{0,2},{1,3},{2,0},{3,1},{4,6},{5,7},{6,4},{7,5},{8,10},{9,11},{10,... | collective-permute-start | bytes 3145736 | tf_op jit(solution)/shard_map/ppermute | solution.py:451
  94.6 5.0 %collective-permute-start.10 = (bf16[8,40,512]{2,1,0:T(8,128)(2,1)S(1)}, bf16[8,40,512]{2,1,0:T(8,128)(2,1)S(1)}, u32[]{:S(2)}, u32[]{:S(2)}) collective-permute-start(bf16[8,40,512]{2,1,0:T(8,128)(2,1)S(1)} %get-tuple-element.19), channel_id=1, source_target_pairs={{0,160},{32,192},{64,224},{96,0},{128,32},{160,64},{192,96},{224,1... | collective-permute-start | bytes 983048 | tf_op jit(solution)/shard_map/ppermute | solution.py:451
  99.6 16.4 %collective-permute-done.left_ref = bf16[1024,512]{1,0:T(8,128)(2,1)} collective-permute-done((bf16[1024,512]{1,0:T(8,128)(2,1)}, bf16[1024,512]{1,0:T(8,128)(2,1)}, u32[]{:S(2)}, u32[]{:S(2)}) %collective-permute-start) | collective-permute-done | bytes 1048608 | tf_op jit(solution)/shard_map/ppermute | solution.py:451
  116.9 22.9 %collective-permute-done.2.far_ref = bf16[1024,512]{1,0:T(8,128)(2,1)} collective-permute-done((bf16[1024,512]{1,0:T(8,128)(2,1)}, bf16[1024,512]{1,0:T(8,128)(2,1)}, u32[]{:S(2)}, u32[]{:S(2)}) %collective-permute-start.2) | collective-permute-done | bytes 1048608 | tf_op jit(solution)/shard_map/ppermute | solution.py:451
  139.8 15.4 %token_path.1 = (f32[1024,512]{1,0:T(8,128)}, f32[2,2,4,128]{3,2,1,0:T(4,128)S(1)}) custom-call(s32[1]{0:T(128)} %bitcast.1.me_ref, bf16[1024,512]{1,0:T(8,128)(2,1)} %own_ref.1, bf16[1024,512]{1,0:T(8,128)(2,1)} %collective-permute-done.left_ref, bf16[1024,512]{1,0:T(8,128)(2,1)} %collective-permute-done.1.right_ref, ...), custom_call_target="tpu_custom_call" | custom-call | flops 4294967296 | bytes 10485760 | tf_op jit(solution)/shard_map/token_path/pallas_call | solution.py:169
  155.2 8.7 %psum.7.stats_ref = f32[2,8,128]{2,1,0:T(8,128)S(1)} all-reduce(f32[2,8,128]{2,1,0:T(8,128)S(1)} %bitcast.24), channel_id=1, replica_groups=mesh['z'=8,'y'=4,'c'=2,'tp'=4] {'tp'}, use_global_device_ids=true, to_apply=%region_0.1 | all-reduce | flops 2048 | bytes 16384 | tf_op jit(solution)/shard_map/psum | solution.py:518
  164.0 2.8 %finish.1.conv_ref = f32[1024,512]{1,0:T(8,128)} custom-call(f32[1024,512]{1,0:T(8,128)} %get-tuple-element.12.conv_ref, f32[2,8,128]{2,1,0:T(8,128)S(1)} %psum.7.stats_ref, f32[1,512]{1,0:T(1,128)S(1)} %bitcast.21), custom_call_target="tpu_custom_call" | custom-call | flops 4194304 | bytes 4194304 | tf_op jit(solution)/shard_map/finish/pallas_call | solution.py:216
  166.8 6.7 %attend.1 = bf16[1024,512]{1,0:T(8,128)(2,1)} custom-call(s32[1]{0:T(128)} %bitcast.plane_ref, s32[32]{0:T(128)S(1)} %reshape.46.where_ref, f32[1024,512]{1,0:T(8,128)} %finish.1.conv_ref, f32[1,512]{1,0:T(1,128)S(1)} %bitcast.22, bf16[8,272,512]{2,1,0:T(8,128)(2,1)S(1)} %all-to-all-done.1.refs_0_, bf16[8,240,512]{2,1,0:T(8,128)(2,1)} %all-to-all-done.2.refs_1_, ...), custom_call_target="tpu_custom_call" | custom-call | flops 268435456 | bytes 5242880 | tf_op jit(solution)/shard_map/attend/pallas_call | solution.py:347
  (36 shorter events, 6.6 us)
Async XLA Ops:
  0.0 0.7 copy-start.2
  0.7 12.0 %copy-start.3 = (s32[16,2]{0,1:T(2,128)S(1)}, s32[16,2]{0,1:T(2,128)}, u32[]{:S(2)}) copy-start(s32[16,2]{0,1:T(2,128)} %param.24) | copy-start | bytes 388
  0.7 12.2 %copy-start.4 = (s32[16,2]{0,1:T(2,128)S(1)}, s32[16,2]{0,1:T(2,128)}, u32[]{:S(2)}) copy-start(s32[16,2]{0,1:T(2,128)} %param.25) | copy-start | bytes 388
  6.7 34.2 %collective-permute-start.3 = (bf16[16,64,512]{2,1,0:T(8,128)(2,1)S(1)}, bf16[16,64,512]{2,1,0:T(8,128)(2,1)S(1)}, u32[]{:S(2)}, u32[]{:S(2)}) collective-permute-start(bf16[16,64,512]{2,1,0:T(8,128)(2,1)S(1)} %bitcast.16), channel_id=1, source_target_pairs={{0,32},{32,64},{64,96},{96,128},{128,160},{160,192},{192,224},{224... | collective-permute-start | bytes 3145736 | tf_op jit(solution)/shard_map/ppermute | solution.py:451
  8.7 32.2 %collective-permute-start.4 = (bf16[16,64,512]{2,1,0:T(8,128)(2,1)S(1)}, bf16[16,64,512]{2,1,0:T(8,128)(2,1)S(1)}, u32[]{:S(2)}, u32[]{:S(2)}) collective-permute-start(bf16[16,64,512]{2,1,0:T(8,128)(2,1)S(1)} %bitcast.17), channel_id=1, source_target_pairs={{0,224},{32,0},{64,32},{96,64},{128,96},{160,128},{192,160},{224,1... | collective-permute-start | bytes 3145736 | tf_op jit(solution)/shard_map/ppermute | solution.py:451
  14.0 26.9 %all-to-all-start = ((s32[64,1,8]{2,1,0:T(1,128)}), s32[64,1,8]{2,1,0:T(1,128)S(1)}, u32[]{:S(2)}, u32[]{:S(2)}) async-start(s32[64,1,8]{2,1,0:T(1,128)} %bitcast.11), calls=%async_computation | async-start | bytes 65536 | tf_op jit(solution)/shard_map/all_to_all | solution.py:455
  44.0 3.8 %copy-start.6 = (bf16[8,64,512]{2,1,0:T(8,128)(2,1)S(1)}, bf16[8,64,512]{2,1,0:T(8,128)(2,1)}, u32[]{:S(2)}) copy-start(bf16[8,64,512]{2,1,0:T(8,128)(2,1)} %get-tuple-element.17) | copy-start | bytes 1572868
  44.0 6.6 %copy-start.5 = (bf16[8,64,512]{2,1,0:T(8,128)(2,1)S(1)}, bf16[8,64,512]{2,1,0:T(8,128)(2,1)}, u32[]{:S(2)}) copy-start(bf16[8,64,512]{2,1,0:T(8,128)(2,1)} %get-tuple-element.18) | copy-start | bytes 1572868
  44.0 41.2 %all-to-all-start.1 = ((bf16[8,272,512]{2,1,0:T(8,128)(2,1)}), bf16[8,272,512]{2,1,0:T(8,128)(2,1)S(1)}, u32[]{:S(2)}, u32[]{:S(2)}) async-start(bf16[8,272,512]{2,1,0:T(8,128)(2,1)} %get-tuple-element.14), calls=%async_computation.1 | async-start | bytes 4456448 | tf_op jit(solution)/shard_map/all_to_all | solution.py:455
  47.8 16.6 %collective-permute-start.7 = (bf16[8,64,512]{2,1,0:T(8,128)(2,1)S(1)}, bf16[8,64,512]{2,1,0:T(8,128)(2,1)S(1)}, u32[]{:S(2)}, u32[]{:S(2)}) collective-permute-start(bf16[8,64,512]{2,1,0:T(8,128)(2,1)S(1)} %copy-done.6), channel_id=1, source_target_pairs={{0,32},{32,64},{64,96},{96,128},{128,160},{160,192},{192,224},{224... | collective-permute-start | bytes 1572872 | tf_op jit(solution)/shard_map/ppermute | solution.py:451
  50.5 15.5 %collective-permute-start.8 = (bf16[8,64,512]{2,1,0:T(8,128)(2,1)S(1)}, bf16[8,64,512]{2,1,0:T(8,128)(2,1)S(1)}, u32[]{:S(2)}, u32[]{:S(2)}) collective-permute-start(bf16[8,64,512]{2,1,0:T(8,128)(2,1)S(1)} %copy-done.5), channel_id=1, source_target_pairs={{0,224},{32,0},{64,32},{96,64},{128,96},{160,128},{192,160},{224,1... | collective-permute-start | bytes 1572872 | tf_op jit(solution)/shard_map/ppermute | solution.py:451
  51.1 32.2 %collective-permute-start.5 = (bf16[8,56,512]{2,1,0:T(8,128)(2,1)}, bf16[8,56,512]{2,1,0:T(8,128)(2,1)S(1)}, u32[]{:S(2)}, u32[]{:S(2)}) collective-permute-start(bf16[8,56,512]{2,1,0:T(8,128)(2,1)} %get-tuple-element.15), channel_id=1, source_target_pairs={{0,64},{32,96},{64,128},{96,160},{128,192},{160,224},{192,0},{224,... | collective-permute-start | bytes 1376264 | tf_op jit(solution)/shard_map/ppermute | solution.py:451
  52.7 31.5 %collective-permute-start.6 = (bf16[8,56,512]{2,1,0:T(8,128)(2,1)}, bf16[8,56,512]{2,1,0:T(8,128)(2,1)S(1)}, u32[]{:S(2)}, u32[]{:S(2)}) collective-permute-start(bf16[8,56,512]{2,1,0:T(8,128)(2,1)} %get-tuple-element.16), channel_id=1, source_target_pairs={{0,192},{32,224},{64,0},{96,32},{128,64},{160,96},{192,128},{224,1... | collective-permute-start | bytes 1376264 | tf_op jit(solution)/shard_map/ppermute | solution.py:451
  85.2 81.6 %all-to-all-start.2 = ((bf16[8,240,512]{2,1,0:T(8,128)(2,1)}), bf16[8,240,512]{2,1,0:T(8,128)(2,1)}, u32[]{:S(2)}, u32[]{:S(2)}) async-start(bf16[8,240,512]{2,1,0:T(8,128)(2,1)} %fill.3), calls=%async_computation.2 | async-start | bytes 3932160 | tf_op jit(solution)/shard_map/all_to_all | solution.py:455
  89.6 26.4 %collective-permute-start = (bf16[1024,512]{1,0:T(8,128)(2,1)}, bf16[1024,512]{1,0:T(8,128)(2,1)}, u32[]{:S(2)}, u32[]{:S(2)}) collective-permute-start(bf16[1024,512]{1,0:T(8,128)(2,1)} %own_ref.1), channel_id=1, source_target_pairs={{0,1},{1,2},{2,3},{3,0},{4,5},{5,6},{6,7},{7,4},{8,9},{9,10},{10,1... | collective-permute-start | bytes 3145736 | tf_op jit(solution)/shard_map/ppermute | solution.py:451
  91.1 25.7 %collective-permute-start.1 = (bf16[1024,512]{1,0:T(8,128)(2,1)}, bf16[1024,512]{1,0:T(8,128)(2,1)}, u32[]{:S(2)}, u32[]{:S(2)}) collective-permute-start(bf16[1024,512]{1,0:T(8,128)(2,1)} %own_ref.1), channel_id=1, source_target_pairs={{0,3},{1,0},{2,1},{3,2},{4,7},{5,4},{6,5},{7,6},{8,11},{9,8},{10,9... | collective-permute-start | bytes 3145736 | tf_op jit(solution)/shard_map/ppermute | solution.py:451
  91.7 48.1 %collective-permute-start.2 = (bf16[1024,512]{1,0:T(8,128)(2,1)}, bf16[1024,512]{1,0:T(8,128)(2,1)}, u32[]{:S(2)}, u32[]{:S(2)}) collective-permute-start(bf16[1024,512]{1,0:T(8,128)(2,1)} %own_ref.1), channel_id=1, source_target_pairs={{0,2},{1,3},{2,0},{3,1},{4,6},{5,7},{6,4},{7,5},{8,10},{9,11},{10,... | collective-permute-start | bytes 3145736 | tf_op jit(solution)/shard_map/ppermute | solution.py:451
  94.6 72.2 %collective-permute-start.9 = (bf16[8,40,512]{2,1,0:T(8,128)(2,1)}, bf16[8,40,512]{2,1,0:T(8,128)(2,1)S(1)}, u32[]{:S(2)}, u32[]{:S(2)}) collective-permute-start(bf16[8,40,512]{2,1,0:T(8,128)(2,1)} %get-tuple-element.20), channel_id=1, source_target_pairs={{0,96},{32,128},{64,160},{96,192},{128,224},{160,0},{192,32},{224,... | collective-permute-start | bytes 983048 | tf_op jit(solution)/shard_map/ppermute | solution.py:451
  94.6 72.2 %collective-permute-start.10 = (bf16[8,40,512]{2,1,0:T(8,128)(2,1)S(1)}, bf16[8,40,512]{2,1,0:T(8,128)(2,1)S(1)}, u32[]{:S(2)}, u32[]{:S(2)}) collective-permute-start(bf16[8,40,512]{2,1,0:T(8,128)(2,1)S(1)} %get-tuple-element.19), channel_id=1, source_target_pairs={{0,160},{32,192},{64,224},{96,0},{128,32},{160,64},{192,96},{224,1... | collective-permute-start | bytes 983048 | tf_op jit(solution)/shard_map/ppermute | solution.py:451
  139.8 24.1 %copy-start = (f32[512]{0:T(512)S(1)}, f32[512]{0:T(512)}, u32[]{:S(2)}) copy-start(f32[512]{0:T(512)} %param.18) | copy-start | bytes 6148
  164.0 2.9 %copy-start.1 = (f32[512]{0:T(512)S(1)}, f32[512]{0:T(512)}, u32[]{:S(2)}) copy-start(f32[512]{0:T(512)} %param.19) | copy-start | bytes 6148

commit v8 on v7

--- a/solution.py
+++ b/solution.py
@@ -54,15 +54,16 @@
     ).astype(jnp.bfloat16)
 
 
-def project_passages(store, gain, keys_weight, values_weight):
+def project_passages(store, gain, keys_weight, values_weight, part):
     rows = store.reshape(-1, D)
-    count = rows.shape[0]
+    count = rows.shape[0] // 2
     tile = 256
+    first = part * (count // tile)
     return pl.pallas_call(
         project_kernel,
         grid=(count // tile,),
         in_specs=[
-            pl.BlockSpec((tile, D), lambda i: (i, 0)),
+            pl.BlockSpec((tile, D), lambda i: (i + first, 0)),
             whole((1, D)),
             whole((D, HEAD)),
             whole((D, HEAD)),
@@ -70,7 +71,7 @@
         out_specs=pl.BlockSpec((tile, 2 * HEAD), lambda i: (i, 0)),
         out_shape=jax.ShapeDtypeStruct((count, 2 * HEAD), jnp.bfloat16),
         cost_estimate=pl.CostEstimate(
-            flops=4 * count * D * HEAD, transcendentals=0, bytes_accessed=7 << 20
+            flops=4 * count * D * HEAD, transcendentals=0, bytes_accessed=4 << 20
         ),
         compiler_params=pltpu.CompilerParams(vmem_limit_bytes=16 << 20),
         name="project_passages",
@@ -355,10 +356,11 @@
         ),
         compiler_params=pltpu.CompilerParams(vmem_limit_bytes=16 << 20),
         name="attend",
-    )(plane, where, *in_hbm(conv_out), retrieval_gate.reshape(1, width), *in_vmem(*groups))
-
-
-def pick_kernel(plane_ref, table_ref, own_ref, below_ref, above_ref, *refs):
+    )(plane, where, *in_hbm(conv_out), retrieval_gate.reshape(1, width), *in_hbm(*groups))
+
+
+def pick_kernel(plane_ref, table_ref, *refs):
+    (own, below, above), refs = (refs[0:2], refs[2:4], refs[4:6]), refs[6:]
     outs, sems = refs[:-1], refs[-1]
     here = plane_ref[0]
     half = PROWS // 2
@@ -367,63 +369,66 @@
         at = lax.rem(here + reader_plane + 8, 8) * 8 + reader
         return table_ref[at, lax.rem(here + owner_plane + 8, 8)]
 
+    def send(sources, taken, first, rows, target, n):
+        size = sources[0].shape[0]
+        for part, source in enumerate(sources):
+
+            @pl.when((taken < size) if part == 0 else (taken >= size))
+            def _():
+                pltpu.make_async_copy(
+                    source.at[taken - part * size, pl.ds(first, rows)], target, sems.at[n]
+                ).start()
+
+    for reader in range(8):
+        for n, (source, side, steps, rows) in enumerate(
+            (
+                (below, 1, 1, PROWS),
+                (above, -1, 1, PROWS),
+                (below, 1, 2, KEPT),
+                (above, -1, 2, KEPT),
+            )
+        ):
+            taken = slot(side * steps, reader, -side)
+            send(source, taken, 0, rows, outs[1 + n].at[reader], 1 + n)
     for reader in range(8):
         at = 0
         for source, reader_plane, owner_plane, first, rows in (
-            (own_ref, 0, 0, 0, PROWS),
-            (below_ref, 0, -1, 0, PROWS),
-            (above_ref, 0, 1, 0, PROWS),
-            (below_ref, 3, -1, 0, half),
-            (own_ref, 3, 0, KEPT, PROWS - KEPT),
-            (above_ref, -3, 1, half, half),
-            (own_ref, -3, 0, KEPT, PROWS - KEPT),
+            (own, 0, 0, 0, PROWS),
+            (below, 0, -1, 0, PROWS),
+            (above, 0, 1, 0, PROWS),
+            (below, 3, -1, 0, half),
+            (own, 3, 0, KEPT, PROWS - KEPT),
+            (above, -3, 1, half, half),
+            (own, -3, 0, KEPT, PROWS - KEPT),
         ):
-            pltpu.make_async_copy(
-                source.at[slot(reader_plane, reader, owner_plane), pl.ds(first, rows)],
-                outs[0].at[reader, pl.ds(at, rows)],
-                sems.at[0],
-            ).start()
+            taken = slot(reader_plane, reader, owner_plane)
+            send(source, taken, first, rows, outs[0].at[reader, pl.ds(at, rows)], 0)
             at += rows
-    for reader in range(8):
-        for n, (source, side, steps, rows) in enumerate(
-            (
-                (below_ref, 1, 1, PROWS),
-                (above_ref, -1, 1, PROWS),
-                (below_ref, 1, 2, KEPT),
-                (above_ref, -1, 2, KEPT),
-            )
-        ):
-            pltpu.make_async_copy(
-                source.at[slot(side * steps, reader, -side), pl.ds(0, rows)],
-                outs[1 + n].at[reader],
-                sems.at[1 + n],
-            ).start()
     for n, out in enumerate(outs):
         pltpu.make_async_copy(out, out, sems.at[n]).wait()
 
 
-def pick(plane, table, own, below, above):
+def pick(plane, table, *sources):
     shapes = [(8, NEAR_ROWS), (8, PROWS), (8, PROWS), (8, KEPT), (8, KEPT)]
     return pl.pallas_call(
         pick_kernel,
         in_specs=[pl.BlockSpec(memory_space=pltpu.SMEM)] * 2
-        + [pl.BlockSpec(memory_space=pl.ANY)] * 3,
+        + [pl.BlockSpec(memory_space=pl.ANY)] * len(sources),
         out_specs=[pl.BlockSpec(memory_space=pl.ANY)] * len(shapes),
         scratch_shapes=[pltpu.SemaphoreType.DMA((len(shapes),))],
-        out_shape=[
-            pltpu.HBM((*shape, 2 * HEAD), jnp.bfloat16) for shape in shapes
-        ],
+        out_shape=[pltpu.HBM((*shape, 2 * HEAD), jnp.bfloat16) for shape in shapes],
         cost_estimate=pl.CostEstimate(flops=0, transcendentals=0, bytes_accessed=8 << 20),
         compiler_params=pltpu.CompilerParams(vmem_limit_bytes=2 << 20),
         name="pick",
-    )(plane, table, *in_vmem(own, below, above))
+    )(plane, table, *in_vmem(*sources))
 
 
 def fill_kernel(*refs, at):
-    first_ref, second_ref, out_ref, sems = refs[0], refs[1], refs[-2], refs[-1]
+    first_ref, second_ref = refs[:2]
+    out_ref, stores = refs[-2:]
     rows = first_ref.shape[1]
     copies = [
-        pltpu.make_async_copy(ref, out_ref.at[:, pl.ds(at + n * rows, rows)], sems.at[n])
+        pltpu.make_async_copy(ref, out_ref.at[:, pl.ds(at + n * rows, rows)], stores.at[n])
         for n, ref in enumerate((first_ref, second_ref))
     ]
     for copy in copies:
@@ -432,19 +437,50 @@
         copy.wait()
 
 
+def staged_fill_kernel(first_ref, second_ref, into_ref, out_ref, held_ref, loads, stores, *, at):
+    del into_ref
+    size, rows, _ = first_ref.shape
+    count = size // 2
+    parts = [(n, h) for h in range(2) for n in range(2)]
+
+    def load(n, h):
+        source = (first_ref, second_ref)[n].at[pl.ds(h * count, count)]
+        return pltpu.make_async_copy(source, held_ref.at[n, h], loads.at[n, h])
+
+    def store(n, h):
+        target = out_ref.at[pl.ds(h * count, count), pl.ds(at + n * rows, rows)]
+        return pltpu.make_async_copy(held_ref.at[n, h], target, stores.at[n, h])
+
+    for part in parts:
+        load(*part).start()
+    for part in parts:
+        load(*part).wait()
+        store(*part).start()
+    for part in parts:
+        store(*part).wait()
+
+
 def fill(first, second, at, into=None):
-    held = [] if into is None else [into]
+    size, rows, width = first.shape
+    if into is None:
+        kernel, held = fill_kernel, in_vmem(first, second)
+        scratch = [pltpu.SemaphoreType.DMA((2,))]
+    else:
+        kernel, held = staged_fill_kernel, in_hbm(first, second, into)
+        scratch = [pltpu.VMEM((2, 2, size // 2, rows, width), first.dtype)] + [
+            pltpu.SemaphoreType.DMA((2, 2))
+        ] * 2
     return pl.pallas_call(
-        functools.partial(fill_kernel, at=at),
-        in_specs=[pl.BlockSpec(memory_space=pl.ANY)] * (2 + len(held)),
+        functools.partial(kernel, at=at),
+        in_specs=[pl.BlockSpec(memory_space=pl.ANY)] * len(held),
         out_specs=pl.BlockSpec(memory_space=pl.ANY),
-        scratch_shapes=[pltpu.SemaphoreType.DMA((2,))],
-        out_shape=pltpu.HBM((8, AWAY_ROWS, 2 * HEAD), jnp.bfloat16),
-        input_output_aliases={2: 0} if held else {},
+        scratch_shapes=scratch,
+        out_shape=pltpu.HBM((size, AWAY_ROWS, width), first.dtype),
+        input_output_aliases={} if into is None else {2: 0},
         cost_estimate=pl.CostEstimate(flops=0, transcendentals=0, bytes_accessed=2 << 20),
-        compiler_params=pltpu.CompilerParams(vmem_limit_bytes=2 << 20),
+        compiler_params=pltpu.CompilerParams(vmem_limit_bytes=4 << 20),
         name="fill",
-    )(*in_vmem(first, second), *in_hbm(*held))
+    )(*held)
 
 
 def shift(value, axis, step):
@@ -476,10 +512,15 @@
     right = shift(tokens, "tp", -1)
     far = shift(tokens, "tp", 2)
 
-    own = project_passages(passage_store, passage_gain, keys_weight, values_weight)
-    own = own.reshape(-1, PROWS, 2 * HEAD)
-    below = shift(own, "z", 1)
-    above = shift(own, "z", -1)
+    sources = [[], [], []]
+    for part in range(2):
+        own = project_passages(
+            passage_store, passage_gain, keys_weight, values_weight, part
+        )
+        own = own.reshape(-1, PROWS, 2 * HEAD)
+        sources[0].append(own)
+        sources[1].append(shift(own, "z", 1))
+        sources[2].append(shift(own, "z", -1))
 
     asked = owners.reshape(-1)
     slots = local_slots.reshape(-1)
@@ -490,7 +531,7 @@
     wanted = jnp.broadcast_to(wanted.reshape(1, 8, 8).transpose(0, 2, 1), (8, 8, 8))
     table = exchange(wanted.reshape(64, 8), ST)
 
-    near, up1, down1, up2, down2 = pick(plane, table, own, below, above)
+    near, up1, down1, up2, down2 = pick(plane, table, *sum(sources, []))
     side = ("y", "c")
     near = exchange(near, side)
     up1 = shift(up1, "z", 1)

time: 176 us -> 180 us (1.023)
  starting transfers between devices: 40.3 us -> 42.6 us
    unnamed x16 -> x26, local copies, waits for them, and re-layouts: 0.89 us -> 3.23 us
    ppermute x11 -> x13, starting transfers between devices: 22.7 us -> 25 us  [shift(): return lax.ppermute(value, axis, ring(lax.axis_size(axis), step))]
    pallas_call x1 -> x2, Pallas kernels: 6.01 us -> 7.5 us  [project_passages(): pl.pallas_call(project_kernel, grid=(count // tile,), in_specs=[pl.BlockS...]
    ppermute x11 -> x13, waiting for transfers between devices: 68.2 us -> 68.3 us  [shift(): return lax.ppermute(value, axis, ring(lax.axis_size(axis), step))]
  transfers between devices with their start and end apart: 14 -> 16, of which waited for: 8 -> 8; matrix products, arithmetic and copies ran while one was open for 1% -> 1% of each run, Pallas kernels for 12% -> 14%
where the time goes in v8:
time: 180 us; the launch traced here: 178 us
  waiting for transfers between devices  84.8 us (47%)
  starting transfers between devices  42.6 us (24%)
  Pallas kernels  37.3 us (21%)
  blocking collectives  8.71 us (5%)
  local copies, waits for them, and re-layouts  4.23 us (2%)
    ppermute x13, waiting for transfers between devices, shift(): return lax.ppermute(value, axis, ring(lax.axis_size(axis), step))  68.3 us
    ppermute x13, starting transfers between devices, shift(): return lax.ppermute(value, axis, ring(lax.axis_size(axis), step))  25 us
    all_to_all x3, starting transfers between devices, exchange(): return lax.all_to_all(value, axes, split_axis=0, concat_axis=0, tiled=True)  17.6 us
    all_to_all x3, waiting for transfers between devices, exchange(): return lax.all_to_all(value, axes, split_axis=0, concat_axis=0, tiled=True)  16.5 us
    pallas_call x1, Pallas kernels, token_path(): pl.pallas_call(token_kernel, grid_spec=grid_spec, out_shape=[pltpu.HBM((r...  15.3 us
    psum x1, blocking collectives, layer(): stats = lax.psum(stats, 'tp')  8.71 us
    pallas_call x2, Pallas kernels, project_passages(): pl.pallas_call(project_kernel, grid=(count // tile,), in_specs=[pl.BlockS...  7.5 us
    pallas_call x1, Pallas kernels, attend(): pl.pallas_call(attend_kernel, grid_spec=grid_spec, out_shape=jax.ShapeDty...  5.51 us
  transfers between devices with their start and end apart: 16, of which 8 were waited for; matrix products, arithmetic and copies ran while one was open for 1% of the time, Pallas kernels for 14%

profile of v8, /device:TPU:2, one launch (start us, length us, event | category | flops | bytes accessed | tf_op | source)
XLA Modules:
  0.0 178.2 jit_solution(17859379180360831)
XLA Ops:
  0.7 3.8 %project_passages.2 = bf16[512,512]{1,0:T(8,128)(2,1)S(1)} custom-call(bf16[1024,2048]{1,0:T(8,128)(2,1)} %bitcast.29, f32[1,2048]{1,0:T(1,128)S(1)} %bitcast.24, bf16[2048,256]{1,0:T(8,128)(2,1)} %keys_ref.3, bf16[2048,256]{1,0:T(8,128)(2,1)} %values_ref.3), custom_call_target="tpu_custom_call" | custom-call | flops 1073741824 | bytes 4194304 | tf_op jit(solution)/shard_map/project_passages/pallas_call | solution.py:62
  4.5 2.0 %collective-permute-start.3 = (bf16[8,64,512]{2,1,0:T(8,128)(2,1)S(1)}, bf16[8,64,512]{2,1,0:T(8,128)(2,1)S(1)}, u32[]{:S(2)}, u32[]{:S(2)}) collective-permute-start(bf16[8,64,512]{2,1,0:T(8,128)(2,1)S(1)} %bitcast.17), channel_id=1, source_target_pairs={{0,32},{32,64},{64,96},{96,128},{128,160},{160,192},{192,224},{224... | collective-permute-start | bytes 1572872 | tf_op jit(solution)/shard_map/ppermute | solution.py:487
  6.5 3.8 %project_passages.3 = bf16[512,512]{1,0:T(8,128)(2,1)S(1)} custom-call(bf16[1024,2048]{1,0:T(8,128)(2,1)} %bitcast.30, f32[1,2048]{1,0:T(1,128)S(1)} %bitcast.25, bf16[2048,256]{1,0:T(8,128)(2,1)} %keys_ref.3, bf16[2048,256]{1,0:T(8,128)(2,1)} %values_ref.3), custom_call_target="tpu_custom_call" | custom-call | flops 1073741824 | bytes 4194304 | tf_op jit(solution)/shard_map/project_passages/pallas_call | solution.py:62
  10.2 2.0 %collective-permute-start.4 = (bf16[8,64,512]{2,1,0:T(8,128)(2,1)S(1)}, bf16[8,64,512]{2,1,0:T(8,128)(2,1)S(1)}, u32[]{:S(2)}, u32[]{:S(2)}) collective-permute-start(bf16[8,64,512]{2,1,0:T(8,128)(2,1)S(1)} %bitcast.20), channel_id=1, source_target_pairs={{0,32},{32,64},{64,96},{96,128},{128,160},{160,192},{192,224},{224... | collective-permute-start | bytes 1572872 | tf_op jit(solution)/shard_map/ppermute | solution.py:487
  12.2 2.1 %collective-permute-start.5 = (bf16[8,64,512]{2,1,0:T(8,128)(2,1)S(1)}, bf16[8,64,512]{2,1,0:T(8,128)(2,1)S(1)}, u32[]{:S(2)}, u32[]{:S(2)}) collective-permute-start(bf16[8,64,512]{2,1,0:T(8,128)(2,1)S(1)} %bitcast.18), channel_id=1, source_target_pairs={{0,224},{32,0},{64,32},{96,64},{128,96},{160,128},{192,160},{224,1... | collective-permute-start | bytes 1572872 | tf_op jit(solution)/shard_map/ppermute | solution.py:487
  14.4 2.0 %collective-permute-start.6 = (bf16[8,64,512]{2,1,0:T(8,128)(2,1)S(1)}, bf16[8,64,512]{2,1,0:T(8,128)(2,1)S(1)}, u32[]{:S(2)}, u32[]{:S(2)}) collective-permute-start(bf16[8,64,512]{2,1,0:T(8,128)(2,1)S(1)} %bitcast.21), channel_id=1, source_target_pairs={{0,224},{32,0},{64,32},{96,64},{128,96},{160,128},{192,160},{224,1... | collective-permute-start | bytes 1572872 | tf_op jit(solution)/shard_map/ppermute | solution.py:487
  17.6 9.4 %all-to-all-start = ((s32[64,1,8]{2,1,0:T(1,128)}), s32[64,1,8]{2,1,0:T(1,128)S(1)}, u32[]{:S(2)}, u32[]{:S(2)}) async-start(s32[64,1,8]{2,1,0:T(1,128)} %bitcast.11), calls=%async_computation | async-start | bytes 65536 | tf_op jit(solution)/shard_map/all_to_all | solution.py:491
  27.0 16.5 %all-to-all-done = s32[64,1,8]{2,1,0:T(1,128)S(1)} async-done(((s32[64,1,8]{2,1,0:T(1,128)}), s32[64,1,8]{2,1,0:T(1,128)S(1)}, u32[]{:S(2)}, u32[]{:S(2)}) %all-to-all-start) | async-done | bytes 2080 | tf_op jit(solution)/shard_map/all_to_all | solution.py:491
  43.6 3.1 %pick.1 = (bf16[8,272,512]{2,1,0:T(8,128)(2,1)}, bf16[8,64,512]{2,1,0:T(8,128)(2,1)}, bf16[8,64,512]{2,1,0:T(8,128)(2,1)}, bf16[8,56,512]{2,1,0:T(8,128)(2,1)}, bf16[8,56,512]{2,1,0:T(8,128)(2,1)}) custom-call(s32[1]{0:T(128)} %bitcast.plane_ref, s32[64,8]{1,0:T(8,128)S(1)} %bitcast.23, bf16[8,64,512]{2,1,0:T(8,128)(2,1)S(1)} %bitcast.19, ...), custom_call_target="tpu_custom_call" | custom-call | bytes 8388608 | tf_op jit(solution)/shard_map/pick/pallas_call | solution.py:413
  46.7 3.8 %all-to-all-start.1 = ((bf16[8,272,512]{2,1,0:T(8,128)(2,1)}), bf16[8,272,512]{2,1,0:T(8,128)(2,1)S(1)}, u32[]{:S(2)}, u32[]{:S(2)}) async-start(bf16[8,272,512]{2,1,0:T(8,128)(2,1)} %get-tuple-element.14), calls=%async_computation.1 | async-start | bytes 4456448 | tf_op jit(solution)/shard_map/all_to_all | solution.py:491
  50.5 2.5 %collective-permute-start.9 = (bf16[8,64,512]{2,1,0:T(8,128)(2,1)S(1)}, bf16[8,64,512]{2,1,0:T(8,128)(2,1)S(1)}, u32[]{:S(2)}, u32[]{:S(2)}) collective-permute-start(bf16[8,64,512]{2,1,0:T(8,128)(2,1)S(1)} %copy-done.11), channel_id=1, source_target_pairs={{0,32},{32,64},{64,96},{96,128},{128,160},{160,192},{192,224},{224... | collective-permute-start | bytes 1572872 | tf_op jit(solution)/shard_map/ppermute | solution.py:487
  55.1 2.8 %collective-permute-start.8 = (bf16[8,56,512]{2,1,0:T(8,128)(2,1)}, bf16[8,56,512]{2,1,0:T(8,128)(2,1)S(1)}, u32[]{:S(2)}, u32[]{:S(2)}) collective-permute-start(bf16[8,56,512]{2,1,0:T(8,128)(2,1)} %get-tuple-element.16), channel_id=1, source_target_pairs={{0,192},{32,224},{64,0},{96,32},{128,64},{160,96},{192,128},{224,1... | collective-permute-start | bytes 1376264 | tf_op jit(solution)/shard_map/ppermute | solution.py:487
  57.9 8.6 %collective-permute-done.9.refs_0_ = bf16[8,64,512]{2,1,0:T(8,128)(2,1)S(1)} collective-permute-done((bf16[8,64,512]{2,1,0:T(8,128)(2,1)S(1)}, bf16[8,64,512]{2,1,0:T(8,128)(2,1)S(1)}, u32[]{:S(2)}, u32[]{:S(2)}) %collective-permute-start.9) | collective-permute-done | bytes 524320 | tf_op jit(solution)/shard_map/ppermute | solution.py:487
  69.3 17.3 %collective-permute-done.7.first_ref = bf16[8,56,512]{2,1,0:T(8,128)(2,1)S(1)} collective-permute-done((bf16[8,56,512]{2,1,0:T(8,128)(2,1)}, bf16[8,56,512]{2,1,0:T(8,128)(2,1)S(1)}, u32[]{:S(2)}, u32[]{:S(2)}) %collective-permute-start.7) | collective-permute-done | bytes 458784 | tf_op jit(solution)/shard_map/ppermute | solution.py:487
  88.1 2.0 %fill.3 = bf16[8,240,512]{2,1,0:T(8,128)(2,1)} custom-call(bf16[8,56,512]{2,1,0:T(8,128)(2,1)} %copy-done.4, bf16[8,56,512]{2,1,0:T(8,128)(2,1)} %copy-done.5, bf16[8,240,512]{2,1,0:T(8,128)(2,1)} %fill.2.into_ref), custom_call_target="tpu_custom_call", output_to_operand_aliasing={{}: (2, {})} | custom-call | bytes 2097152 | tf_op jit(solution)/shard_map/fill/pallas_call | solution.py:473
  90.1 4.5 %all-to-all-start.2 = ((bf16[8,240,512]{2,1,0:T(8,128)(2,1)}), bf16[8,240,512]{2,1,0:T(8,128)(2,1)}, u32[]{:S(2)}, u32[]{:S(2)}) async-start(bf16[8,240,512]{2,1,0:T(8,128)(2,1)} %fill.3), calls=%async_computation.2 | async-start | bytes 3932160 | tf_op jit(solution)/shard_map/all_to_all | solution.py:491
  96.7 2.1 %collective-permute-start.2 = (bf16[1024,512]{1,0:T(8,128)(2,1)}, bf16[1024,512]{1,0:T(8,128)(2,1)}, u32[]{:S(2)}, u32[]{:S(2)}) collective-permute-start(bf16[1024,512]{1,0:T(8,128)(2,1)} %own_ref.1), channel_id=1, source_target_pairs={{0,2},{1,3},{2,0},{3,1},{4,6},{5,7},{6,4},{7,5},{8,10},{9,11},{10,... | collective-permute-start | bytes 3145736 | tf_op jit(solution)/shard_map/ppermute | solution.py:487
  99.1 5.0 %collective-permute-start.12 = (bf16[8,40,512]{2,1,0:T(8,128)(2,1)S(1)}, bf16[8,40,512]{2,1,0:T(8,128)(2,1)S(1)}, u32[]{:S(2)}, u32[]{:S(2)}) collective-permute-start(bf16[8,40,512]{2,1,0:T(8,128)(2,1)S(1)} %get-tuple-element.19), channel_id=1, source_target_pairs={{0,160},{32,192},{64,224},{96,0},{128,32},{160,64},{192,96},{224,1... | collective-permute-start | bytes 983048 | tf_op jit(solution)/shard_map/ppermute | solution.py:487
  104.1 16.9 %collective-permute-done.left_ref = bf16[1024,512]{1,0:T(8,128)(2,1)} collective-permute-done((bf16[1024,512]{1,0:T(8,128)(2,1)}, bf16[1024,512]{1,0:T(8,128)(2,1)}, u32[]{:S(2)}, u32[]{:S(2)}) %collective-permute-start) | collective-permute-done | bytes 1048608 | tf_op jit(solution)/shard_map/ppermute | solution.py:487
  121.8 23.0 %collective-permute-done.2.far_ref = bf16[1024,512]{1,0:T(8,128)(2,1)} collective-permute-done((bf16[1024,512]{1,0:T(8,128)(2,1)}, bf16[1024,512]{1,0:T(8,128)(2,1)}, u32[]{:S(2)}, u32[]{:S(2)}) %collective-permute-start.2) | collective-permute-done | bytes 1048608 | tf_op jit(solution)/shard_map/ppermute | solution.py:487
  144.8 15.3 %token_path.1 = (f32[1024,512]{1,0:T(8,128)}, f32[2,2,4,128]{3,2,1,0:T(4,128)S(1)}) custom-call(s32[1]{0:T(128)} %bitcast.1.me_ref, bf16[1024,512]{1,0:T(8,128)(2,1)} %own_ref.1, bf16[1024,512]{1,0:T(8,128)(2,1)} %collective-permute-done.left_ref, bf16[1024,512]{1,0:T(8,128)(2,1)} %collective-permute-done.1.right_ref, ...), custom_call_target="tpu_custom_call" | custom-call | flops 4294967296 | bytes 10485760 | tf_op jit(solution)/shard_map/token_path/pallas_call | solution.py:170
  160.1 8.7 %psum.7.stats_ref = f32[2,8,128]{2,1,0:T(8,128)S(1)} all-reduce(f32[2,8,128]{2,1,0:T(8,128)S(1)} %bitcast.31), channel_id=1, replica_groups=mesh['z'=8,'y'=4,'c'=2,'tp'=4] {'tp'}, use_global_device_ids=true, to_apply=%region_0.1 | all-reduce | flops 2048 | bytes 16384 | tf_op jit(solution)/shard_map/psum | solution.py:559
  168.8 2.8 %finish.1.conv_ref = f32[1024,512]{1,0:T(8,128)} custom-call(f32[1024,512]{1,0:T(8,128)} %get-tuple-element.12.conv_ref, f32[2,8,128]{2,1,0:T(8,128)S(1)} %psum.7.stats_ref, f32[1,512]{1,0:T(1,128)S(1)} %bitcast.27), custom_call_target="tpu_custom_call" | custom-call | flops 4194304 | bytes 4194304 | tf_op jit(solution)/shard_map/finish/pallas_call | solution.py:217
  172.5 5.5 %attend.1 = bf16[1024,512]{1,0:T(8,128)(2,1)} custom-call(s32[1]{0:T(128)} %bitcast.plane_ref, s32[32]{0:T(128)S(1)} %reshape.51.where_ref, f32[1024,512]{1,0:T(8,128)} %finish.1.conv_ref, f32[1,512]{1,0:T(1,128)S(1)} %bitcast.28, bf16[8,272,512]{2,1,0:T(8,128)(2,1)} %copy-done.3, bf16[8,240,512]{2,1,0:T(8,128)(2,1)} %all-to-all-done.2.refs_1_, ...), custom_call_target="tpu_custom_call" | custom-call | flops 268435456 | bytes 5242880 | tf_op jit(solution)/shard_map/attend/pallas_call | solution.py:348
  (51 shorter events, 12.4 us)
Async XLA Ops:
  4.5 11.9 %copy-start.8 = (s32[16,2]{0,1:T(2,128)S(1)}, s32[16,2]{0,1:T(2,128)}, u32[]{:S(2)}) copy-start(s32[16,2]{0,1:T(2,128)} %param.24) | copy-start | bytes 388
  4.5 12.1 %copy-start.9 = (s32[16,2]{0,1:T(2,128)S(1)}, s32[16,2]{0,1:T(2,128)}, u32[]{:S(2)}) copy-start(s32[16,2]{0,1:T(2,128)} %param.25) | copy-start | bytes 388
  4.5 39.1 %collective-permute-start.3 = (bf16[8,64,512]{2,1,0:T(8,128)(2,1)S(1)}, bf16[8,64,512]{2,1,0:T(8,128)(2,1)S(1)}, u32[]{:S(2)}, u32[]{:S(2)}) collective-permute-start(bf16[8,64,512]{2,1,0:T(8,128)(2,1)S(1)} %bitcast.17), channel_id=1, source_target_pairs={{0,32},{32,64},{64,96},{96,128},{128,160},{160,192},{192,224},{224... | collective-permute-start | bytes 1572872 | tf_op jit(solution)/shard_map/ppermute | solution.py:487
  10.2 33.3 %collective-permute-start.4 = (bf16[8,64,512]{2,1,0:T(8,128)(2,1)S(1)}, bf16[8,64,512]{2,1,0:T(8,128)(2,1)S(1)}, u32[]{:S(2)}, u32[]{:S(2)}) collective-permute-start(bf16[8,64,512]{2,1,0:T(8,128)(2,1)S(1)} %bitcast.20), channel_id=1, source_target_pairs={{0,32},{32,64},{64,96},{96,128},{128,160},{160,192},{192,224},{224... | collective-permute-start | bytes 1572872 | tf_op jit(solution)/shard_map/ppermute | solution.py:487
  12.2 31.3 %collective-permute-start.5 = (bf16[8,64,512]{2,1,0:T(8,128)(2,1)S(1)}, bf16[8,64,512]{2,1,0:T(8,128)(2,1)S(1)}, u32[]{:S(2)}, u32[]{:S(2)}) collective-permute-start(bf16[8,64,512]{2,1,0:T(8,128)(2,1)S(1)} %bitcast.18), channel_id=1, source_target_pairs={{0,224},{32,0},{64,32},{96,64},{128,96},{160,128},{192,160},{224,1... | collective-permute-start | bytes 1572872 | tf_op jit(solution)/shard_map/ppermute | solution.py:487
  14.4 29.2 %collective-permute-start.6 = (bf16[8,64,512]{2,1,0:T(8,128)(2,1)S(1)}, bf16[8,64,512]{2,1,0:T(8,128)(2,1)S(1)}, u32[]{:S(2)}, u32[]{:S(2)}) collective-permute-start(bf16[8,64,512]{2,1,0:T(8,128)(2,1)S(1)} %bitcast.21), channel_id=1, source_target_pairs={{0,224},{32,0},{64,32},{96,64},{128,96},{160,128},{192,160},{224,1... | collective-permute-start | bytes 1572872 | tf_op jit(solution)/shard_map/ppermute | solution.py:487
  17.6 25.9 %all-to-all-start = ((s32[64,1,8]{2,1,0:T(1,128)}), s32[64,1,8]{2,1,0:T(1,128)S(1)}, u32[]{:S(2)}, u32[]{:S(2)}) async-start(s32[64,1,8]{2,1,0:T(1,128)} %bitcast.11), calls=%async_computation | async-start | bytes 65536 | tf_op jit(solution)/shard_map/all_to_all | solution.py:491
  46.7 3.8 %copy-start.11 = (bf16[8,64,512]{2,1,0:T(8,128)(2,1)S(1)}, bf16[8,64,512]{2,1,0:T(8,128)(2,1)}, u32[]{:S(2)}) copy-start(bf16[8,64,512]{2,1,0:T(8,128)(2,1)} %get-tuple-element.17) | copy-start | bytes 1572868
  46.7 6.3 %copy-start.10 = (bf16[8,64,512]{2,1,0:T(8,128)(2,1)S(1)}, bf16[8,64,512]{2,1,0:T(8,128)(2,1)}, u32[]{:S(2)}) copy-start(bf16[8,64,512]{2,1,0:T(8,128)(2,1)} %get-tuple-element.18) | copy-start | bytes 1572868
  46.7 43.4 %all-to-all-start.1 = ((bf16[8,272,512]{2,1,0:T(8,128)(2,1)}), bf16[8,272,512]{2,1,0:T(8,128)(2,1)S(1)}, u32[]{:S(2)}, u32[]{:S(2)}) async-start(bf16[8,272,512]{2,1,0:T(8,128)(2,1)} %get-tuple-element.14), calls=%async_computation.1 | async-start | bytes 4456448 | tf_op jit(solution)/shard_map/all_to_all | solution.py:491
  50.5 16.1 %collective-permute-start.9 = (bf16[8,64,512]{2,1,0:T(8,128)(2,1)S(1)}, bf16[8,64,512]{2,1,0:T(8,128)(2,1)S(1)}, u32[]{:S(2)}, u32[]{:S(2)}) collective-permute-start(bf16[8,64,512]{2,1,0:T(8,128)(2,1)S(1)} %copy-done.11), channel_id=1, source_target_pairs={{0,32},{32,64},{64,96},{96,128},{128,160},{160,192},{192,224},{224... | collective-permute-start | bytes 1572872 | tf_op jit(solution)/shard_map/ppermute | solution.py:487
  53.0 15.3 %collective-permute-start.10 = (bf16[8,64,512]{2,1,0:T(8,128)(2,1)S(1)}, bf16[8,64,512]{2,1,0:T(8,128)(2,1)S(1)}, u32[]{:S(2)}, u32[]{:S(2)}) collective-permute-start(bf16[8,64,512]{2,1,0:T(8,128)(2,1)S(1)} %copy-done.10), channel_id=1, source_target_pairs={{0,224},{32,0},{64,32},{96,64},{128,96},{160,128},{192,160},{224,1... | collective-permute-start | bytes 1572872 | tf_op jit(solution)/shard_map/ppermute | solution.py:487
  53.8 32.7 %collective-permute-start.7 = (bf16[8,56,512]{2,1,0:T(8,128)(2,1)}, bf16[8,56,512]{2,1,0:T(8,128)(2,1)S(1)}, u32[]{:S(2)}, u32[]{:S(2)}) collective-permute-start(bf16[8,56,512]{2,1,0:T(8,128)(2,1)} %get-tuple-element.15), channel_id=1, source_target_pairs={{0,64},{32,96},{64,128},{96,160},{128,192},{160,224},{192,0},{224,... | collective-permute-start | bytes 1376264 | tf_op jit(solution)/shard_map/ppermute | solution.py:487
  55.1 31.5 %collective-permute-start.8 = (bf16[8,56,512]{2,1,0:T(8,128)(2,1)}, bf16[8,56,512]{2,1,0:T(8,128)(2,1)S(1)}, u32[]{:S(2)}, u32[]{:S(2)}) collective-permute-start(bf16[8,56,512]{2,1,0:T(8,128)(2,1)} %get-tuple-element.16), channel_id=1, source_target_pairs={{0,192},{32,224},{64,0},{96,32},{128,64},{160,96},{192,128},{224,1... | collective-permute-start | bytes 1376264 | tf_op jit(solution)/shard_map/ppermute | solution.py:487
  90.1 8.7 %copy-start.3 = (bf16[8,272,512]{2,1,0:T(8,128)(2,1)}, bf16[8,272,512]{2,1,0:T(8,128)(2,1)S(1)}, u32[]{:S(2)}) copy-start(bf16[8,272,512]{2,1,0:T(8,128)(2,1)S(1)} %all-to-all-done.1.refs_0_) | copy-start | bytes 6684676
  90.1 81.5 %all-to-all-start.2 = ((bf16[8,240,512]{2,1,0:T(8,128)(2,1)}), bf16[8,240,512]{2,1,0:T(8,128)(2,1)}, u32[]{:S(2)}, u32[]{:S(2)}) async-start(bf16[8,240,512]{2,1,0:T(8,128)(2,1)} %fill.3), calls=%async_computation.2 | async-start | bytes 3932160 | tf_op jit(solution)/shard_map/all_to_all | solution.py:491
  94.6 26.4 %collective-permute-start = (bf16[1024,512]{1,0:T(8,128)(2,1)}, bf16[1024,512]{1,0:T(8,128)(2,1)}, u32[]{:S(2)}, u32[]{:S(2)}) collective-permute-start(bf16[1024,512]{1,0:T(8,128)(2,1)} %own_ref.1), channel_id=1, source_target_pairs={{0,1},{1,2},{2,3},{3,0},{4,5},{5,6},{6,7},{7,4},{8,9},{9,10},{10,1... | collective-permute-start | bytes 3145736 | tf_op jit(solution)/shard_map/ppermute | solution.py:487
  96.1 25.7 %collective-permute-start.1 = (bf16[1024,512]{1,0:T(8,128)(2,1)}, bf16[1024,512]{1,0:T(8,128)(2,1)}, u32[]{:S(2)}, u32[]{:S(2)}) collective-permute-start(bf16[1024,512]{1,0:T(8,128)(2,1)} %own_ref.1), channel_id=1, source_target_pairs={{0,3},{1,0},{2,1},{3,2},{4,7},{5,4},{6,5},{7,6},{8,11},{9,8},{10,9... | collective-permute-start | bytes 3145736 | tf_op jit(solution)/shard_map/ppermute | solution.py:487
  96.7 48.1 %collective-permute-start.2 = (bf16[1024,512]{1,0:T(8,128)(2,1)}, bf16[1024,512]{1,0:T(8,128)(2,1)}, u32[]{:S(2)}, u32[]{:S(2)}) collective-permute-start(bf16[1024,512]{1,0:T(8,128)(2,1)} %own_ref.1), channel_id=1, source_target_pairs={{0,2},{1,3},{2,0},{3,1},{4,6},{5,7},{6,4},{7,5},{8,10},{9,11},{10,... | collective-permute-start | bytes 3145736 | tf_op jit(solution)/shard_map/ppermute | solution.py:487
  98.8 72.9 %collective-permute-start.11 = (bf16[8,40,512]{2,1,0:T(8,128)(2,1)S(1)}, bf16[8,40,512]{2,1,0:T(8,128)(2,1)S(1)}, u32[]{:S(2)}, u32[]{:S(2)}) collective-permute-start(bf16[8,40,512]{2,1,0:T(8,128)(2,1)S(1)} %get-tuple-element.20), channel_id=1, source_target_pairs={{0,96},{32,128},{64,160},{96,192},{128,224},{160,0},{192,32},{224,... | collective-permute-start | bytes 983048 | tf_op jit(solution)/shard_map/ppermute | solution.py:487
  99.1 72.6 %collective-permute-start.12 = (bf16[8,40,512]{2,1,0:T(8,128)(2,1)S(1)}, bf16[8,40,512]{2,1,0:T(8,128)(2,1)S(1)}, u32[]{:S(2)}, u32[]{:S(2)}) collective-permute-start(bf16[8,40,512]{2,1,0:T(8,128)(2,1)S(1)} %get-tuple-element.19), channel_id=1, source_target_pairs={{0,160},{32,192},{64,224},{96,0},{128,32},{160,64},{192,96},{224,1... | collective-permute-start | bytes 983048 | tf_op jit(solution)/shard_map/ppermute | solution.py:487
  144.8 24.1 %copy-start.1 = (f32[512]{0:T(512)S(1)}, f32[512]{0:T(512)}, u32[]{:S(2)}) copy-start(f32[512]{0:T(512)} %param.18) | copy-start | bytes 6148
  168.8 3.7 %copy-start.2 = (f32[512]{0:T(512)S(1)}, f32[512]{0:T(512)}, u32[]{:S(2)}) copy-start(f32[512]{0:T(512)} %param.19) | copy-start | bytes 6148
  171.7 0.8 copy-start.7
  (4 other events, 3.0 us)

commit v9 on v8

--- a/solution.py
+++ b/solution.py
@@ -91,8 +91,24 @@
     out_ref,
     stats_ref,
     padded_ref,
+    inner_held,
+    gating_held,
+    sems,
 ):
     me = me_ref[0]
+    begin = pl.program_id(0) == 0
+
+    def load(n, offset):
+        at = lax.rem(me + offset, 4)
+        source, target = ((inner_ref, inner_held), (gating_ref, gating_held))[n]
+        return pltpu.make_async_copy(source.at[at], target.at[offset], sems.at[n, offset])
+
+    @pl.when(begin)
+    def _():
+        for offset in range(4):
+            for n in range(2):
+                load(n, offset).start()
+
     width = own_ref.shape[1]
     squares = jnp.zeros((LENGTH, 1), jnp.float32)
     inner = jnp.zeros((LENGTH, width), jnp.float32)
@@ -109,8 +125,14 @@
             piece = far_ref[...].astype(jnp.float32)
         squares = squares + jnp.sum(piece * piece, axis=1, keepdims=True)
         scaled = (piece * gain_ref[at]).astype(jnp.bfloat16)
-        inner = inner + jnp.dot(scaled, inner_ref[at], preferred_element_type=jnp.float32)
-        gating = gating + jnp.dot(scaled, gating_ref[at], preferred_element_type=jnp.float32)
+
+        @pl.when(begin)
+        def _():
+            for n in range(2):
+                load(n, offset).wait()
+
+        inner = inner + jnp.dot(scaled, inner_held[offset], preferred_element_type=jnp.float32)
+        gating = gating + jnp.dot(scaled, gating_held[offset], preferred_element_type=jnp.float32)
     inverse = lax.rsqrt(squares / D + EPSILON)
     gated = (inner * inverse * jax.nn.sigmoid(gating * inverse)).astype(jnp.bfloat16)
     padded_ref[:LEAD, :] = jnp.zeros((LEAD, width), jnp.float32)
@@ -157,15 +179,20 @@
         in_specs=[pl.BlockSpec((LENGTH, width), lambda i, m: (i, 0))] * 4
         + [
             whole((4, 1, width)),
-            whole((4, width, width)),
-            whole((4, width, width)),
+            pl.BlockSpec(memory_space=pl.ANY),
+            pl.BlockSpec(memory_space=pl.ANY),
             whole((CONV, width)),
         ],
         out_specs=[
             pl.BlockSpec((LENGTH, width), lambda i, m: (i, 0)),
             pl.BlockSpec((None, 2, LENGTH // 128, 128), lambda i, m: (i, 0, 0, 0)),
         ],
-        scratch_shapes=[pltpu.VMEM((LEAD + LENGTH, width), jnp.float32)],
+        scratch_shapes=[
+            pltpu.VMEM((LEAD + LENGTH, width), jnp.float32),
+            pltpu.VMEM((4, width, width), jnp.bfloat16),
+            pltpu.VMEM((4, width, width), jnp.bfloat16),
+            pltpu.SemaphoreType.DMA((2, 4)),
+        ],
     )
     return pl.pallas_call(
         token_kernel,
@@ -366,8 +393,9 @@
     half = PROWS // 2
 
     def slot(reader_plane, reader, owner_plane):
-        at = lax.rem(here + reader_plane + 8, 8) * 8 + reader
-        return table_ref[at, lax.rem(here + owner_plane + 8, 8)]
+        return table_ref[
+            lax.rem(here + reader_plane + 8, 8), reader * 8 + lax.rem(here + owner_plane + 8, 8)
+        ]
 
     def send(sources, taken, first, rows, target, n):
         size = sources[0].shape[0]
@@ -528,8 +556,8 @@
         jnp.where(asked[:, None] == jnp.arange(64, dtype=jnp.int32)[None, :], slots[:, None], 0),
         axis=0,
     )
-    wanted = jnp.broadcast_to(wanted.reshape(1, 8, 8).transpose(0, 2, 1), (8, 8, 8))
-    table = exchange(wanted.reshape(64, 8), ST)
+    wanted = exchange(wanted.reshape(8, 8).T, ("y", "c"))
+    table = exchange(jnp.broadcast_to(wanted.reshape(1, 64), (8, 64)), "z")
 
     near, up1, down1, up2, down2 = pick(plane, table, *sum(sources, []))
     side = ("y", "c")

time: 180 us -> 179 us (level)
  blocking collectives: 8.71 us -> 18.3 us
  waiting for transfers between devices: 84.8 us -> 75.8 us
  starting transfers between devices: 42.6 us -> 38.8 us
    all_to_all x0 -> x1, blocking collectives: none -> 9.54 us  [exchange(): return lax.all_to_all(value, axes, split_axis=0, concat_axis=0, tiled=True)]
    all_to_all x3, waiting for transfers between devices: 16.5 us -> 7.64 us  [exchange(): return lax.all_to_all(value, axes, split_axis=0, concat_axis=0, tiled=True)]
    all_to_all x3, starting transfers between devices: 17.6 us -> 13.9 us  [exchange(): return lax.all_to_all(value, axes, split_axis=0, concat_axis=0, tiled=True)]
  transfers between devices with their start and end apart: 16 -> 16, of which waited for: 8 -> 7; matrix products, arithmetic and copies ran while one was open for 1% -> 1% of each run, Pallas kernels for 14% -> 15%
where the time goes in v9:
time: 179 us; the launch traced here: 177 us
  waiting for transfers between devices  75.8 us (42%)
  starting transfers between devices  38.8 us (22%)
  Pallas kernels  38 us (21%)
  blocking collectives  18.3 us (10%)
  local copies, waits for them, and re-layouts  4.83 us (3%)
    ppermute x13, waiting for transfers between devices, shift(): return lax.ppermute(value, axis, ring(lax.axis_size(axis), step))  68.1 us
    ppermute x13, starting transfers between devices, shift(): return lax.ppermute(value, axis, ring(lax.axis_size(axis), step))  24.9 us
    pallas_call x1, Pallas kernels, token_path(): pl.pallas_call(token_kernel, grid_spec=grid_spec, out_shape=[pltpu.HBM((r...  16.4 us
    all_to_all x3, starting transfers between devices, exchange(): return lax.all_to_all(value, axes, split_axis=0, concat_axis=0, tiled=True)  13.9 us
    all_to_all x1, blocking collectives, exchange(): return lax.all_to_all(value, axes, split_axis=0, concat_axis=0, tiled=True)  9.54 us
    psum x1, blocking collectives, layer(): stats = lax.psum(stats, 'tp')  8.72 us
    all_to_all x3, waiting for transfers between devices, exchange(): return lax.all_to_all(value, axes, split_axis=0, concat_axis=0, tiled=True)  7.64 us
    pallas_call x2, Pallas kernels, project_passages(): pl.pallas_call(project_kernel, grid=(count // tile,), in_specs=[pl.BlockS...  7.5 us
  transfers between devices with their start and end apart: 16, of which 7 were waited for; matrix products, arithmetic and copies ran while one was open for 1% of the time, Pallas kernels for 15%

profile of v9, /device:TPU:2, one launch (start us, length us, event | category | flops | bytes accessed | tf_op | source)
XLA Modules:
  0.0 176.8 jit_solution(16144081807574485028)
XLA Ops:
  0.7 3.7 %project_passages.2 = bf16[512,512]{1,0:T(8,128)(2,1)S(1)} custom-call(bf16[1024,2048]{1,0:T(8,128)(2,1)} %bitcast.29, f32[1,2048]{1,0:T(1,128)S(1)} %bitcast.23, bf16[2048,256]{1,0:T(8,128)(2,1)} %keys_ref.3, bf16[2048,256]{1,0:T(8,128)(2,1)} %values_ref.3), custom_call_target="tpu_custom_call" | custom-call | flops 1073741824 | bytes 4194304 | tf_op jit(solution)/shard_map/project_passages/pallas_call | solution.py:62
  4.5 2.0 %collective-permute-start.3 = (bf16[8,64,512]{2,1,0:T(8,128)(2,1)S(1)}, bf16[8,64,512]{2,1,0:T(8,128)(2,1)S(1)}, u32[]{:S(2)}, u32[]{:S(2)}) collective-permute-start(bf16[8,64,512]{2,1,0:T(8,128)(2,1)S(1)} %bitcast.17), channel_id=1, source_target_pairs={{0,32},{32,64},{64,96},{96,128},{128,160},{160,192},{192,224},{224... | collective-permute-start | bytes 1572872 | tf_op jit(solution)/shard_map/ppermute | solution.py:515
  6.5 3.8 %project_passages.3 = bf16[512,512]{1,0:T(8,128)(2,1)S(1)} custom-call(bf16[1024,2048]{1,0:T(8,128)(2,1)} %bitcast.30, f32[1,2048]{1,0:T(1,128)S(1)} %bitcast.24, bf16[2048,256]{1,0:T(8,128)(2,1)} %keys_ref.3, bf16[2048,256]{1,0:T(8,128)(2,1)} %values_ref.3), custom_call_target="tpu_custom_call" | custom-call | flops 1073741824 | bytes 4194304 | tf_op jit(solution)/shard_map/project_passages/pallas_call | solution.py:62
  10.2 2.0 %collective-permute-start.4 = (bf16[8,64,512]{2,1,0:T(8,128)(2,1)S(1)}, bf16[8,64,512]{2,1,0:T(8,128)(2,1)S(1)}, u32[]{:S(2)}, u32[]{:S(2)}) collective-permute-start(bf16[8,64,512]{2,1,0:T(8,128)(2,1)S(1)} %bitcast.20), channel_id=1, source_target_pairs={{0,32},{32,64},{64,96},{96,128},{128,160},{160,192},{192,224},{224... | collective-permute-start | bytes 1572872 | tf_op jit(solution)/shard_map/ppermute | solution.py:515
  12.2 2.1 %collective-permute-start.5 = (bf16[8,64,512]{2,1,0:T(8,128)(2,1)S(1)}, bf16[8,64,512]{2,1,0:T(8,128)(2,1)S(1)}, u32[]{:S(2)}, u32[]{:S(2)}) collective-permute-start(bf16[8,64,512]{2,1,0:T(8,128)(2,1)S(1)} %bitcast.18), channel_id=1, source_target_pairs={{0,224},{32,0},{64,32},{96,64},{128,96},{160,128},{192,160},{224,1... | collective-permute-start | bytes 1572872 | tf_op jit(solution)/shard_map/ppermute | solution.py:515
  14.4 2.0 %collective-permute-start.6 = (bf16[8,64,512]{2,1,0:T(8,128)(2,1)S(1)}, bf16[8,64,512]{2,1,0:T(8,128)(2,1)S(1)}, u32[]{:S(2)}, u32[]{:S(2)}) collective-permute-start(bf16[8,64,512]{2,1,0:T(8,128)(2,1)S(1)} %bitcast.21), channel_id=1, source_target_pairs={{0,224},{32,0},{64,32},{96,64},{128,96},{160,128},{192,160},{224,1... | collective-permute-start | bytes 1572872 | tf_op jit(solution)/shard_map/ppermute | solution.py:515
  17.0 9.5 %all_to_all.27 = s32[8,1,8]{2,1,0:T(1,128)S(1)} all-to-all(s32[8,1,8]{2,1,0:T(1,128)S(1)} %copy.32), channel_id=1, replica_groups=mesh['z'=8,'y'=4,'c'=2,'tp'=4] {'y','c'}, dimensions={0} | all-to-all | bytes 512 | tf_op jit(solution)/shard_map/all_to_all | solution.py:519
  28.4 5.8 %all-to-all-start.1 = ((s32[8,1,64]{2,1,0:T(1,128)}), s32[8,1,64]{2,1,0:T(1,128)S(1)}, u32[]{:S(2)}, u32[]{:S(2)}) async-start(s32[8,1,64]{2,1,0:T(1,128)} %broadcast_in_dim.26), calls=%async_computation.1 | async-start | bytes 8192 | tf_op jit(solution)/shard_map/all_to_all | solution.py:519
  34.1 7.6 %all-to-all-done.1 = s32[8,1,64]{2,1,0:T(1,128)S(1)} async-done(((s32[8,1,64]{2,1,0:T(1,128)}), s32[8,1,64]{2,1,0:T(1,128)S(1)}, u32[]{:S(2)}, u32[]{:S(2)}) %all-to-all-start.1) | async-done | bytes 2080 | tf_op jit(solution)/shard_map/all_to_all | solution.py:519
  41.8 2.6 %pick.1 = (bf16[8,272,512]{2,1,0:T(8,128)(2,1)}, bf16[8,64,512]{2,1,0:T(8,128)(2,1)}, bf16[8,64,512]{2,1,0:T(8,128)(2,1)}, bf16[8,56,512]{2,1,0:T(8,128)(2,1)}, bf16[8,56,512]{2,1,0:T(8,128)(2,1)}) custom-call(s32[1]{0:T(128)} %bitcast.plane_ref, s32[8,64]{1,0:T(8,128)S(1)} %bitcast.25, bf16[8,64,512]{2,1,0:T(8,128)(2,1)S(1)} %bitcast.19, ...), custom_call_target="tpu_custom_call" | custom-call | bytes 8388608 | tf_op jit(solution)/shard_map/pick/pallas_call | solution.py:441
  44.5 3.8 %all-to-all-start.2 = ((bf16[8,272,512]{2,1,0:T(8,128)(2,1)}), bf16[8,272,512]{2,1,0:T(8,128)(2,1)S(1)}, u32[]{:S(2)}, u32[]{:S(2)}) async-start(bf16[8,272,512]{2,1,0:T(8,128)(2,1)} %get-tuple-element.14), calls=%async_computation.2 | async-start | bytes 4456448 | tf_op jit(solution)/shard_map/all_to_all | solution.py:519
  52.2 3.5 %collective-permute-start.8 = (bf16[8,56,512]{2,1,0:T(8,128)(2,1)}, bf16[8,56,512]{2,1,0:T(8,128)(2,1)S(1)}, u32[]{:S(2)}, u32[]{:S(2)}) collective-permute-start(bf16[8,56,512]{2,1,0:T(8,128)(2,1)} %get-tuple-element.16), channel_id=1, source_target_pairs={{0,192},{32,224},{64,0},{96,32},{128,64},{160,96},{192,128},{224,1... | collective-permute-start | bytes 1376264 | tf_op jit(solution)/shard_map/ppermute | solution.py:515
  55.7 8.6 %collective-permute-done.9.refs_0_ = bf16[8,64,512]{2,1,0:T(8,128)(2,1)S(1)} collective-permute-done((bf16[8,64,512]{2,1,0:T(8,128)(2,1)S(1)}, bf16[8,64,512]{2,1,0:T(8,128)(2,1)S(1)}, u32[]{:S(2)}, u32[]{:S(2)}) %collective-permute-start.9) | collective-permute-done | bytes 524320 | tf_op jit(solution)/shard_map/ppermute | solution.py:515
  66.5 17.5 %collective-permute-done.7.first_ref = bf16[8,56,512]{2,1,0:T(8,128)(2,1)S(1)} collective-permute-done((bf16[8,56,512]{2,1,0:T(8,128)(2,1)}, bf16[8,56,512]{2,1,0:T(8,128)(2,1)S(1)}, u32[]{:S(2)}, u32[]{:S(2)}) %collective-permute-start.7) | collective-permute-done | bytes 458784 | tf_op jit(solution)/shard_map/ppermute | solution.py:515
  85.5 2.0 %fill.3 = bf16[8,240,512]{2,1,0:T(8,128)(2,1)} custom-call(bf16[8,56,512]{2,1,0:T(8,128)(2,1)} %copy-done.4, bf16[8,56,512]{2,1,0:T(8,128)(2,1)} %copy-done.5, bf16[8,240,512]{2,1,0:T(8,128)(2,1)} %fill.2.into_ref), custom_call_target="tpu_custom_call", output_to_operand_aliasing={{}: (2, {})} | custom-call | bytes 2097152 | tf_op jit(solution)/shard_map/fill/pallas_call | solution.py:501
  87.6 4.4 %all-to-all-start.3 = ((bf16[8,240,512]{2,1,0:T(8,128)(2,1)}), bf16[8,240,512]{2,1,0:T(8,128)(2,1)}, u32[]{:S(2)}, u32[]{:S(2)}) async-start(bf16[8,240,512]{2,1,0:T(8,128)(2,1)} %fill.3), calls=%async_computation.3 | async-start | bytes 3932160 | tf_op jit(solution)/shard_map/all_to_all | solution.py:519
  94.1 2.1 %collective-permute-start.2 = (bf16[1024,512]{1,0:T(8,128)(2,1)}, bf16[1024,512]{1,0:T(8,128)(2,1)}, u32[]{:S(2)}, u32[]{:S(2)}) collective-permute-start(bf16[1024,512]{1,0:T(8,128)(2,1)} %own_ref.1), channel_id=1, source_target_pairs={{0,2},{1,3},{2,0},{3,1},{4,6},{5,7},{6,4},{7,5},{8,10},{9,11},{10,... | collective-permute-start | bytes 3145736 | tf_op jit(solution)/shard_map/ppermute | solution.py:515
  96.3 5.0 %collective-permute-start.12 = (bf16[8,40,512]{2,1,0:T(8,128)(2,1)S(1)}, bf16[8,40,512]{2,1,0:T(8,128)(2,1)S(1)}, u32[]{:S(2)}, u32[]{:S(2)}) collective-permute-start(bf16[8,40,512]{2,1,0:T(8,128)(2,1)S(1)} %get-tuple-element.19), channel_id=1, source_target_pairs={{0,160},{32,192},{64,224},{96,0},{128,32},{160,64},{192,96},{224,1... | collective-permute-start | bytes 983048 | tf_op jit(solution)/shard_map/ppermute | solution.py:515
  101.4 17.0 %collective-permute-done.left_ref = bf16[1024,512]{1,0:T(8,128)(2,1)} collective-permute-done((bf16[1024,512]{1,0:T(8,128)(2,1)}, bf16[1024,512]{1,0:T(8,128)(2,1)}, u32[]{:S(2)}, u32[]{:S(2)}) %collective-permute-start) | collective-permute-done | bytes 1048608 | tf_op jit(solution)/shard_map/ppermute | solution.py:515
  119.3 22.9 %collective-permute-done.2.far_ref = bf16[1024,512]{1,0:T(8,128)(2,1)} collective-permute-done((bf16[1024,512]{1,0:T(8,128)(2,1)}, bf16[1024,512]{1,0:T(8,128)(2,1)}, u32[]{:S(2)}, u32[]{:S(2)}) %collective-permute-start.2) | collective-permute-done | bytes 1048608 | tf_op jit(solution)/shard_map/ppermute | solution.py:515
  142.2 16.4 %token_path.1 = (f32[1024,512]{1,0:T(8,128)}, f32[2,2,4,128]{3,2,1,0:T(4,128)S(1)}) custom-call(s32[1]{0:T(128)} %bitcast.1.me_ref, bf16[1024,512]{1,0:T(8,128)(2,1)} %own_ref.1, bf16[1024,512]{1,0:T(8,128)(2,1)} %collective-permute-done.left_ref, bf16[1024,512]{1,0:T(8,128)(2,1)} %collective-permute-done.1.right_ref, ...), custom_call_target="tpu_custom_call" | custom-call | flops 4294967296 | bytes 10485760 | tf_op jit(solution)/shard_map/token_path/pallas_call | solution.py:197
  158.6 8.7 %psum.7.stats_ref = f32[2,8,128]{2,1,0:T(8,128)S(1)} all-reduce(f32[2,8,128]{2,1,0:T(8,128)S(1)} %bitcast.31), channel_id=1, replica_groups=mesh['z'=8,'y'=4,'c'=2,'tp'=4] {'tp'}, use_global_device_ids=true, to_apply=%region_0.1 | all-reduce | flops 2048 | bytes 16384 | tf_op jit(solution)/shard_map/psum | solution.py:587
  167.4 2.8 %finish.1.conv_ref = f32[1024,512]{1,0:T(8,128)} custom-call(f32[1024,512]{1,0:T(8,128)} %get-tuple-element.12.conv_ref, f32[2,8,128]{2,1,0:T(8,128)S(1)} %psum.7.stats_ref, f32[1,512]{1,0:T(1,128)S(1)} %bitcast.27), custom_call_target="tpu_custom_call" | custom-call | flops 4194304 | bytes 4194304 | tf_op jit(solution)/shard_map/finish/pallas_call | solution.py:244
  171.1 5.5 %attend.1 = bf16[1024,512]{1,0:T(8,128)(2,1)} custom-call(s32[1]{0:T(128)} %bitcast.plane_ref, s32[32]{0:T(128)S(1)} %reshape.59.where_ref, f32[1024,512]{1,0:T(8,128)} %finish.1.conv_ref, f32[1,512]{1,0:T(1,128)S(1)} %bitcast.28, bf16[8,272,512]{2,1,0:T(8,128)(2,1)} %copy-done.3, bf16[8,240,512]{2,1,0:T(8,128)(2,1)} %all-to-all-done.3.refs_1_, ...), custom_call_target="tpu_custom_call" | custom-call | flops 268435456 | bytes 5242880 | tf_op jit(solution)/shard_map/attend/pallas_call | solution.py:375
  (55 shorter events, 14.8 us)
Async XLA Ops:
  4.4 11.9 %copy-start.8 = (s32[16,2]{0,1:T(2,128)S(1)}, s32[16,2]{0,1:T(2,128)}, u32[]{:S(2)}) copy-start(s32[16,2]{0,1:T(2,128)} %param.24) | copy-start | bytes 388
  4.5 12.1 %copy-start.9 = (s32[16,2]{0,1:T(2,128)S(1)}, s32[16,2]{0,1:T(2,128)}, u32[]{:S(2)}) copy-start(s32[16,2]{0,1:T(2,128)} %param.25) | copy-start | bytes 388
  4.5 37.3 %collective-permute-start.3 = (bf16[8,64,512]{2,1,0:T(8,128)(2,1)S(1)}, bf16[8,64,512]{2,1,0:T(8,128)(2,1)S(1)}, u32[]{:S(2)}, u32[]{:S(2)}) collective-permute-start(bf16[8,64,512]{2,1,0:T(8,128)(2,1)S(1)} %bitcast.17), channel_id=1, source_target_pairs={{0,32},{32,64},{64,96},{96,128},{128,160},{160,192},{192,224},{224... | collective-permute-start | bytes 1572872 | tf_op jit(solution)/shard_map/ppermute | solution.py:515
  10.2 31.5 %collective-permute-start.4 = (bf16[8,64,512]{2,1,0:T(8,128)(2,1)S(1)}, bf16[8,64,512]{2,1,0:T(8,128)(2,1)S(1)}, u32[]{:S(2)}, u32[]{:S(2)}) collective-permute-start(bf16[8,64,512]{2,1,0:T(8,128)(2,1)S(1)} %bitcast.20), channel_id=1, source_target_pairs={{0,32},{32,64},{64,96},{96,128},{128,160},{160,192},{192,224},{224... | collective-permute-start | bytes 1572872 | tf_op jit(solution)/shard_map/ppermute | solution.py:515
  12.2 29.6 %collective-permute-start.5 = (bf16[8,64,512]{2,1,0:T(8,128)(2,1)S(1)}, bf16[8,64,512]{2,1,0:T(8,128)(2,1)S(1)}, u32[]{:S(2)}, u32[]{:S(2)}) collective-permute-start(bf16[8,64,512]{2,1,0:T(8,128)(2,1)S(1)} %bitcast.18), channel_id=1, source_target_pairs={{0,224},{32,0},{64,32},{96,64},{128,96},{160,128},{192,160},{224,1... | collective-permute-start | bytes 1572872 | tf_op jit(solution)/shard_map/ppermute | solution.py:515
  14.4 27.4 %collective-permute-start.6 = (bf16[8,64,512]{2,1,0:T(8,128)(2,1)S(1)}, bf16[8,64,512]{2,1,0:T(8,128)(2,1)S(1)}, u32[]{:S(2)}, u32[]{:S(2)}) collective-permute-start(bf16[8,64,512]{2,1,0:T(8,128)(2,1)S(1)} %bitcast.21), channel_id=1, source_target_pairs={{0,224},{32,0},{64,32},{96,64},{128,96},{160,128},{192,160},{224,1... | collective-permute-start | bytes 1572872 | tf_op jit(solution)/shard_map/ppermute | solution.py:515
  28.4 13.4 %all-to-all-start.1 = ((s32[8,1,64]{2,1,0:T(1,128)}), s32[8,1,64]{2,1,0:T(1,128)S(1)}, u32[]{:S(2)}, u32[]{:S(2)}) async-start(s32[8,1,64]{2,1,0:T(1,128)} %broadcast_in_dim.26), calls=%async_computation.1 | async-start | bytes 8192 | tf_op jit(solution)/shard_map/all_to_all | solution.py:519
  44.4 3.8 %copy-start.11 = (bf16[8,64,512]{2,1,0:T(8,128)(2,1)S(1)}, bf16[8,64,512]{2,1,0:T(8,128)(2,1)}, u32[]{:S(2)}) copy-start(bf16[8,64,512]{2,1,0:T(8,128)(2,1)} %get-tuple-element.17) | copy-start | bytes 1572868
  44.5 5.7 %copy-start.10 = (bf16[8,64,512]{2,1,0:T(8,128)(2,1)S(1)}, bf16[8,64,512]{2,1,0:T(8,128)(2,1)}, u32[]{:S(2)}) copy-start(bf16[8,64,512]{2,1,0:T(8,128)(2,1)} %get-tuple-element.18) | copy-start | bytes 1572868
  44.5 43.1 %all-to-all-start.2 = ((bf16[8,272,512]{2,1,0:T(8,128)(2,1)}), bf16[8,272,512]{2,1,0:T(8,128)(2,1)S(1)}, u32[]{:S(2)}, u32[]{:S(2)}) async-start(bf16[8,272,512]{2,1,0:T(8,128)(2,1)} %get-tuple-element.14), calls=%async_computation.2 | async-start | bytes 4456448 | tf_op jit(solution)/shard_map/all_to_all | solution.py:519
  48.2 16.1 %collective-permute-start.9 = (bf16[8,64,512]{2,1,0:T(8,128)(2,1)S(1)}, bf16[8,64,512]{2,1,0:T(8,128)(2,1)S(1)}, u32[]{:S(2)}, u32[]{:S(2)}) collective-permute-start(bf16[8,64,512]{2,1,0:T(8,128)(2,1)S(1)} %copy-done.11), channel_id=1, source_target_pairs={{0,32},{32,64},{64,96},{96,128},{128,160},{160,192},{192,224},{224... | collective-permute-start | bytes 1572872 | tf_op jit(solution)/shard_map/ppermute | solution.py:515
  50.2 15.3 %collective-permute-start.10 = (bf16[8,64,512]{2,1,0:T(8,128)(2,1)S(1)}, bf16[8,64,512]{2,1,0:T(8,128)(2,1)S(1)}, u32[]{:S(2)}, u32[]{:S(2)}) collective-permute-start(bf16[8,64,512]{2,1,0:T(8,128)(2,1)S(1)} %copy-done.10), channel_id=1, source_target_pairs={{0,224},{32,0},{64,32},{96,64},{128,96},{160,128},{192,160},{224,1... | collective-permute-start | bytes 1572872 | tf_op jit(solution)/shard_map/ppermute | solution.py:515
  51.5 32.4 %collective-permute-start.7 = (bf16[8,56,512]{2,1,0:T(8,128)(2,1)}, bf16[8,56,512]{2,1,0:T(8,128)(2,1)S(1)}, u32[]{:S(2)}, u32[]{:S(2)}) collective-permute-start(bf16[8,56,512]{2,1,0:T(8,128)(2,1)} %get-tuple-element.15), channel_id=1, source_target_pairs={{0,64},{32,96},{64,128},{96,160},{128,192},{160,224},{192,0},{224,... | collective-permute-start | bytes 1376264 | tf_op jit(solution)/shard_map/ppermute | solution.py:515
  52.2 31.8 %collective-permute-start.8 = (bf16[8,56,512]{2,1,0:T(8,128)(2,1)}, bf16[8,56,512]{2,1,0:T(8,128)(2,1)S(1)}, u32[]{:S(2)}, u32[]{:S(2)}) collective-permute-start(bf16[8,56,512]{2,1,0:T(8,128)(2,1)} %get-tuple-element.16), channel_id=1, source_target_pairs={{0,192},{32,224},{64,0},{96,32},{128,64},{160,96},{192,128},{224,1... | collective-permute-start | bytes 1376264 | tf_op jit(solution)/shard_map/ppermute | solution.py:515
  87.6 8.7 %copy-start.3 = (bf16[8,272,512]{2,1,0:T(8,128)(2,1)}, bf16[8,272,512]{2,1,0:T(8,128)(2,1)S(1)}, u32[]{:S(2)}) copy-start(bf16[8,272,512]{2,1,0:T(8,128)(2,1)S(1)} %all-to-all-done.2.refs_0_) | copy-start | bytes 6684676
  87.6 82.7 %all-to-all-start.3 = ((bf16[8,240,512]{2,1,0:T(8,128)(2,1)}), bf16[8,240,512]{2,1,0:T(8,128)(2,1)}, u32[]{:S(2)}, u32[]{:S(2)}) async-start(bf16[8,240,512]{2,1,0:T(8,128)(2,1)} %fill.3), calls=%async_computation.3 | async-start | bytes 3932160 | tf_op jit(solution)/shard_map/all_to_all | solution.py:519
  92.0 26.4 %collective-permute-start = (bf16[1024,512]{1,0:T(8,128)(2,1)}, bf16[1024,512]{1,0:T(8,128)(2,1)}, u32[]{:S(2)}, u32[]{:S(2)}) collective-permute-start(bf16[1024,512]{1,0:T(8,128)(2,1)} %own_ref.1), channel_id=1, source_target_pairs={{0,1},{1,2},{2,3},{3,0},{4,5},{5,6},{6,7},{7,4},{8,9},{9,10},{10,1... | collective-permute-start | bytes 3145736 | tf_op jit(solution)/shard_map/ppermute | solution.py:515
  93.6 25.7 %collective-permute-start.1 = (bf16[1024,512]{1,0:T(8,128)(2,1)}, bf16[1024,512]{1,0:T(8,128)(2,1)}, u32[]{:S(2)}, u32[]{:S(2)}) collective-permute-start(bf16[1024,512]{1,0:T(8,128)(2,1)} %own_ref.1), channel_id=1, source_target_pairs={{0,3},{1,0},{2,1},{3,2},{4,7},{5,4},{6,5},{7,6},{8,11},{9,8},{10,9... | collective-permute-start | bytes 3145736 | tf_op jit(solution)/shard_map/ppermute | solution.py:515
  94.1 48.1 %collective-permute-start.2 = (bf16[1024,512]{1,0:T(8,128)(2,1)}, bf16[1024,512]{1,0:T(8,128)(2,1)}, u32[]{:S(2)}, u32[]{:S(2)}) collective-permute-start(bf16[1024,512]{1,0:T(8,128)(2,1)} %own_ref.1), channel_id=1, source_target_pairs={{0,2},{1,3},{2,0},{3,1},{4,6},{5,7},{6,4},{7,5},{8,10},{9,11},{10,... | collective-permute-start | bytes 3145736 | tf_op jit(solution)/shard_map/ppermute | solution.py:515
  96.3 74.0 %collective-permute-start.11 = (bf16[8,40,512]{2,1,0:T(8,128)(2,1)S(1)}, bf16[8,40,512]{2,1,0:T(8,128)(2,1)S(1)}, u32[]{:S(2)}, u32[]{:S(2)}) collective-permute-start(bf16[8,40,512]{2,1,0:T(8,128)(2,1)S(1)} %get-tuple-element.20), channel_id=1, source_target_pairs={{0,96},{32,128},{64,160},{96,192},{128,224},{160,0},{192,32},{224,... | collective-permute-start | bytes 983048 | tf_op jit(solution)/shard_map/ppermute | solution.py:515
  96.3 73.9 %collective-permute-start.12 = (bf16[8,40,512]{2,1,0:T(8,128)(2,1)S(1)}, bf16[8,40,512]{2,1,0:T(8,128)(2,1)S(1)}, u32[]{:S(2)}, u32[]{:S(2)}) collective-permute-start(bf16[8,40,512]{2,1,0:T(8,128)(2,1)S(1)} %get-tuple-element.19), channel_id=1, source_target_pairs={{0,160},{32,192},{64,224},{96,0},{128,32},{160,64},{192,96},{224,1... | collective-permute-start | bytes 983048 | tf_op jit(solution)/shard_map/ppermute | solution.py:515
  142.2 25.2 %copy-start.1 = (f32[512]{0:T(512)S(1)}, f32[512]{0:T(512)}, u32[]{:S(2)}) copy-start(f32[512]{0:T(512)} %param.18) | copy-start | bytes 6148
  167.4 3.7 %copy-start.2 = (f32[512]{0:T(512)S(1)}, f32[512]{0:T(512)}, u32[]{:S(2)}) copy-start(f32[512]{0:T(512)} %param.19) | copy-start | bytes 6148
  170.3 0.8 copy-start.7
  (4 other events, 3.0 us)

commit v10 on v8

--- a/solution.py
+++ b/solution.py
@@ -75,7 +75,7 @@
         ),
         compiler_params=pltpu.CompilerParams(vmem_limit_bytes=16 << 20),
         name="project_passages",
-    )(*in_hbm(rows), gain.reshape(1, D), *in_hbm(keys_weight, values_weight))
+    )(*in_hbm(rows, gain.reshape(1, D), keys_weight, values_weight))
 
 
 def token_kernel(
@@ -223,7 +223,7 @@
             whole((1, width)),
         ],
         out_specs=pl.BlockSpec((tile, width), lambda i: (i, 0)),
-        out_shape=pltpu.HBM((rows, width), jnp.float32),
+        out_shape=pltpu.VMEM((rows, width), jnp.float32),
         cost_estimate=pl.CostEstimate(
             flops=8 * rows * width, transcendentals=rows * width, bytes_accessed=4 << 20
         ),
@@ -330,7 +330,7 @@
 def attend(plane, where, conv_out, retrieval_gate, groups):
     rows, width = conv_out.shape
     count = where.shape[0]
-    tile = 512
+    tile = rows
     grid_spec = pltpu.PrefetchScalarGridSpec(
         num_scalar_prefetch=2,
         grid=(rows // tile,),
@@ -356,7 +356,7 @@
         ),
         compiler_params=pltpu.CompilerParams(vmem_limit_bytes=16 << 20),
         name="attend",
-    )(plane, where, *in_hbm(conv_out), retrieval_gate.reshape(1, width), *in_hbm(*groups))
+    )(plane, where, *in_vmem(conv_out), retrieval_gate.reshape(1, width), *in_hbm(*groups[:2]), *in_vmem(*groups[2:]))
 
 
 def pick_kernel(plane_ref, table_ref, *refs):

time: 180 us -> 177 us (0.983)
  no operation moved by 1% of the time
where the time goes in v10:
time: 177 us; the launch traced here: 175 us
  waiting for transfers between devices  84.8 us (48%)
  starting transfers between devices  42.6 us (24%)
  Pallas kernels  35.9 us (20%)
  blocking collectives  8.71 us (5%)
  local copies, waits for them, and re-layouts  2.68 us (2%)
    ppermute x13, waiting for transfers between devices, shift(): return lax.ppermute(value, axis, ring(lax.axis_size(axis), step))  68.3 us
    ppermute x13, starting transfers between devices, shift(): return lax.ppermute(value, axis, ring(lax.axis_size(axis), step))  25 us
    all_to_all x3, starting transfers between devices, exchange(): return lax.all_to_all(value, axes, split_axis=0, concat_axis=0, tiled=True)  17.6 us
    all_to_all x3, waiting for transfers between devices, exchange(): return lax.all_to_all(value, axes, split_axis=0, concat_axis=0, tiled=True)  16.5 us
    pallas_call x1, Pallas kernels, token_path(): pl.pallas_call(token_kernel, grid_spec=grid_spec, out_shape=[pltpu.HBM((r...  15.3 us
    psum x1, blocking collectives, layer(): stats = lax.psum(stats, 'tp')  8.71 us
    pallas_call x2, Pallas kernels, project_passages(): pl.pallas_call(project_kernel, grid=(count // tile,), in_specs=[pl.BlockS...  7.52 us
    pallas_call x1, Pallas kernels, attend(): pl.pallas_call(attend_kernel, grid_spec=grid_spec, out_shape=jax.ShapeDty...  5.07 us
  transfers between devices with their start and end apart: 16, of which 8 were waited for; matrix products, arithmetic and copies ran while one was open for 1% of the time, Pallas kernels for 14%

profile of v10, /device:TPU:2, one launch (start us, length us, event | category | flops | bytes accessed | tf_op | source)
XLA Modules:
  0.0 175.3 jit_solution(4404634009948554415)
XLA Ops:
  0.0 3.8 %project_passages.2 = bf16[512,512]{1,0:T(8,128)(2,1)S(1)} custom-call(bf16[1024,2048]{1,0:T(8,128)(2,1)} %bitcast.27, f32[1,2048]{1,0:T(1,128)} %bitcast.29, bf16[2048,256]{1,0:T(8,128)(2,1)} %keys_ref.3, bf16[2048,256]{1,0:T(8,128)(2,1)} %values_ref.3), custom_call_target="tpu_custom_call" | custom-call | flops 1073741824 | bytes 4194304 | tf_op jit(solution)/shard_map/project_passages/pallas_call | solution.py:62
  3.8 2.0 %collective-permute-start.3 = (bf16[8,64,512]{2,1,0:T(8,128)(2,1)S(1)}, bf16[8,64,512]{2,1,0:T(8,128)(2,1)S(1)}, u32[]{:S(2)}, u32[]{:S(2)}) collective-permute-start(bf16[8,64,512]{2,1,0:T(8,128)(2,1)S(1)} %bitcast.17), channel_id=1, source_target_pairs={{0,32},{32,64},{64,96},{96,128},{128,160},{160,192},{192,224},{224... | collective-permute-start | bytes 1572872 | tf_op jit(solution)/shard_map/ppermute | solution.py:487
  5.8 3.8 %project_passages.3 = bf16[512,512]{1,0:T(8,128)(2,1)S(1)} custom-call(bf16[1024,2048]{1,0:T(8,128)(2,1)} %bitcast.28, f32[1,2048]{1,0:T(1,128)} %bitcast.30, bf16[2048,256]{1,0:T(8,128)(2,1)} %keys_ref.3, bf16[2048,256]{1,0:T(8,128)(2,1)} %values_ref.3), custom_call_target="tpu_custom_call" | custom-call | flops 1073741824 | bytes 4194304 | tf_op jit(solution)/shard_map/project_passages/pallas_call | solution.py:62
  9.6 2.0 %collective-permute-start.4 = (bf16[8,64,512]{2,1,0:T(8,128)(2,1)S(1)}, bf16[8,64,512]{2,1,0:T(8,128)(2,1)S(1)}, u32[]{:S(2)}, u32[]{:S(2)}) collective-permute-start(bf16[8,64,512]{2,1,0:T(8,128)(2,1)S(1)} %bitcast.20), channel_id=1, source_target_pairs={{0,32},{32,64},{64,96},{96,128},{128,160},{160,192},{192,224},{224... | collective-permute-start | bytes 1572872 | tf_op jit(solution)/shard_map/ppermute | solution.py:487
  11.6 2.1 %collective-permute-start.5 = (bf16[8,64,512]{2,1,0:T(8,128)(2,1)S(1)}, bf16[8,64,512]{2,1,0:T(8,128)(2,1)S(1)}, u32[]{:S(2)}, u32[]{:S(2)}) collective-permute-start(bf16[8,64,512]{2,1,0:T(8,128)(2,1)S(1)} %bitcast.18), channel_id=1, source_target_pairs={{0,224},{32,0},{64,32},{96,64},{128,96},{160,128},{192,160},{224,1... | collective-permute-start | bytes 1572872 | tf_op jit(solution)/shard_map/ppermute | solution.py:487
  13.7 2.0 %collective-permute-start.6 = (bf16[8,64,512]{2,1,0:T(8,128)(2,1)S(1)}, bf16[8,64,512]{2,1,0:T(8,128)(2,1)S(1)}, u32[]{:S(2)}, u32[]{:S(2)}) collective-permute-start(bf16[8,64,512]{2,1,0:T(8,128)(2,1)S(1)} %bitcast.21), channel_id=1, source_target_pairs={{0,224},{32,0},{64,32},{96,64},{128,96},{160,128},{192,160},{224,1... | collective-permute-start | bytes 1572872 | tf_op jit(solution)/shard_map/ppermute | solution.py:487
  16.9 9.4 %all-to-all-start = ((s32[64,1,8]{2,1,0:T(1,128)}), s32[64,1,8]{2,1,0:T(1,128)S(1)}, u32[]{:S(2)}, u32[]{:S(2)}) async-start(s32[64,1,8]{2,1,0:T(1,128)} %bitcast.11), calls=%async_computation | async-start | bytes 65536 | tf_op jit(solution)/shard_map/all_to_all | solution.py:491
  26.3 16.5 %all-to-all-done = s32[64,1,8]{2,1,0:T(1,128)S(1)} async-done(((s32[64,1,8]{2,1,0:T(1,128)}), s32[64,1,8]{2,1,0:T(1,128)S(1)}, u32[]{:S(2)}, u32[]{:S(2)}) %all-to-all-start) | async-done | bytes 2080 | tf_op jit(solution)/shard_map/all_to_all | solution.py:491
  42.9 3.1 %pick.1 = (bf16[8,272,512]{2,1,0:T(8,128)(2,1)}, bf16[8,64,512]{2,1,0:T(8,128)(2,1)}, bf16[8,64,512]{2,1,0:T(8,128)(2,1)}, bf16[8,56,512]{2,1,0:T(8,128)(2,1)}, bf16[8,56,512]{2,1,0:T(8,128)(2,1)}) custom-call(s32[1]{0:T(128)} %bitcast.plane_ref, s32[64,8]{1,0:T(8,128)S(1)} %bitcast.23, bf16[8,64,512]{2,1,0:T(8,128)(2,1)S(1)} %bitcast.19, ...), custom_call_target="tpu_custom_call" | custom-call | bytes 8388608 | tf_op jit(solution)/shard_map/pick/pallas_call | solution.py:413
  46.0 3.8 %all-to-all-start.1 = ((bf16[8,272,512]{2,1,0:T(8,128)(2,1)}), bf16[8,272,512]{2,1,0:T(8,128)(2,1)S(1)}, u32[]{:S(2)}, u32[]{:S(2)}) async-start(bf16[8,272,512]{2,1,0:T(8,128)(2,1)} %get-tuple-element.14), calls=%async_computation.1 | async-start | bytes 4456448 | tf_op jit(solution)/shard_map/all_to_all | solution.py:491
  49.8 2.5 %collective-permute-start.9 = (bf16[8,64,512]{2,1,0:T(8,128)(2,1)S(1)}, bf16[8,64,512]{2,1,0:T(8,128)(2,1)S(1)}, u32[]{:S(2)}, u32[]{:S(2)}) collective-permute-start(bf16[8,64,512]{2,1,0:T(8,128)(2,1)S(1)} %copy-done.8), channel_id=1, source_target_pairs={{0,32},{32,64},{64,96},{96,128},{128,160},{160,192},{192,224},{224... | collective-permute-start | bytes 1572872 | tf_op jit(solution)/shard_map/ppermute | solution.py:487
  54.4 2.8 %collective-permute-start.8 = (bf16[8,56,512]{2,1,0:T(8,128)(2,1)}, bf16[8,56,512]{2,1,0:T(8,128)(2,1)S(1)}, u32[]{:S(2)}, u32[]{:S(2)}) collective-permute-start(bf16[8,56,512]{2,1,0:T(8,128)(2,1)} %get-tuple-element.16), channel_id=1, source_target_pairs={{0,192},{32,224},{64,0},{96,32},{128,64},{160,96},{192,128},{224,1... | collective-permute-start | bytes 1376264 | tf_op jit(solution)/shard_map/ppermute | solution.py:487
  57.2 8.6 %collective-permute-done.9.refs_0_ = bf16[8,64,512]{2,1,0:T(8,128)(2,1)S(1)} collective-permute-done((bf16[8,64,512]{2,1,0:T(8,128)(2,1)S(1)}, bf16[8,64,512]{2,1,0:T(8,128)(2,1)S(1)}, u32[]{:S(2)}, u32[]{:S(2)}) %collective-permute-start.9) | collective-permute-done | bytes 524320 | tf_op jit(solution)/shard_map/ppermute | solution.py:487
  68.6 17.2 %collective-permute-done.7.first_ref = bf16[8,56,512]{2,1,0:T(8,128)(2,1)S(1)} collective-permute-done((bf16[8,56,512]{2,1,0:T(8,128)(2,1)}, bf16[8,56,512]{2,1,0:T(8,128)(2,1)S(1)}, u32[]{:S(2)}, u32[]{:S(2)}) %collective-permute-start.7) | collective-permute-done | bytes 458784 | tf_op jit(solution)/shard_map/ppermute | solution.py:487
  87.4 2.0 %fill.3 = bf16[8,240,512]{2,1,0:T(8,128)(2,1)} custom-call(bf16[8,56,512]{2,1,0:T(8,128)(2,1)} %copy-done.3, bf16[8,56,512]{2,1,0:T(8,128)(2,1)} %copy-done.4, bf16[8,240,512]{2,1,0:T(8,128)(2,1)} %fill.2.into_ref), custom_call_target="tpu_custom_call", output_to_operand_aliasing={{}: (2, {})} | custom-call | bytes 2097152 | tf_op jit(solution)/shard_map/fill/pallas_call | solution.py:473
  89.5 4.5 %all-to-all-start.2 = ((bf16[8,240,512]{2,1,0:T(8,128)(2,1)}), bf16[8,240,512]{2,1,0:T(8,128)(2,1)}, u32[]{:S(2)}, u32[]{:S(2)}) async-start(bf16[8,240,512]{2,1,0:T(8,128)(2,1)} %fill.3), calls=%async_computation.2 | async-start | bytes 3932160 | tf_op jit(solution)/shard_map/all_to_all | solution.py:491
  96.0 2.1 %collective-permute-start.2 = (bf16[1024,512]{1,0:T(8,128)(2,1)}, bf16[1024,512]{1,0:T(8,128)(2,1)}, u32[]{:S(2)}, u32[]{:S(2)}) collective-permute-start(bf16[1024,512]{1,0:T(8,128)(2,1)} %own_ref.1), channel_id=1, source_target_pairs={{0,2},{1,3},{2,0},{3,1},{4,6},{5,7},{6,4},{7,5},{8,10},{9,11},{10,... | collective-permute-start | bytes 3145736 | tf_op jit(solution)/shard_map/ppermute | solution.py:487
  98.4 5.0 %collective-permute-start.12 = (bf16[8,40,512]{2,1,0:T(8,128)(2,1)S(1)}, bf16[8,40,512]{2,1,0:T(8,128)(2,1)S(1)}, u32[]{:S(2)}, u32[]{:S(2)}) collective-permute-start(bf16[8,40,512]{2,1,0:T(8,128)(2,1)S(1)} %get-tuple-element.19), channel_id=1, source_target_pairs={{0,160},{32,192},{64,224},{96,0},{128,32},{160,64},{192,96},{224,1... | collective-permute-start | bytes 983048 | tf_op jit(solution)/shard_map/ppermute | solution.py:487
  103.4 16.8 %collective-permute-done.left_ref = bf16[1024,512]{1,0:T(8,128)(2,1)} collective-permute-done((bf16[1024,512]{1,0:T(8,128)(2,1)}, bf16[1024,512]{1,0:T(8,128)(2,1)}, u32[]{:S(2)}, u32[]{:S(2)}) %collective-permute-start) | collective-permute-done | bytes 1048608 | tf_op jit(solution)/shard_map/ppermute | solution.py:487
  121.2 22.9 %collective-permute-done.2.far_ref = bf16[1024,512]{1,0:T(8,128)(2,1)} collective-permute-done((bf16[1024,512]{1,0:T(8,128)(2,1)}, bf16[1024,512]{1,0:T(8,128)(2,1)}, u32[]{:S(2)}, u32[]{:S(2)}) %collective-permute-start.2) | collective-permute-done | bytes 1048608 | tf_op jit(solution)/shard_map/ppermute | solution.py:487
  144.1 15.3 %token_path.1 = (f32[1024,512]{1,0:T(8,128)}, f32[2,2,4,128]{3,2,1,0:T(4,128)S(1)}) custom-call(s32[1]{0:T(128)} %bitcast.1.me_ref, bf16[1024,512]{1,0:T(8,128)(2,1)} %own_ref.1, bf16[1024,512]{1,0:T(8,128)(2,1)} %collective-permute-done.left_ref, bf16[1024,512]{1,0:T(8,128)(2,1)} %collective-permute-done.1.right_ref, ...), custom_call_target="tpu_custom_call" | custom-call | flops 4294967296 | bytes 10485760 | tf_op jit(solution)/shard_map/token_path/pallas_call | solution.py:170
  159.4 8.7 %psum.7.stats_ref = f32[2,8,128]{2,1,0:T(8,128)S(1)} all-reduce(f32[2,8,128]{2,1,0:T(8,128)S(1)} %bitcast.31), channel_id=1, replica_groups=mesh['z'=8,'y'=4,'c'=2,'tp'=4] {'tp'}, use_global_device_ids=true, to_apply=%region_0.1 | all-reduce | flops 2048 | bytes 16384 | tf_op jit(solution)/shard_map/psum | solution.py:559
  168.1 1.9 %finish.1.conv_ref = f32[1024,512]{1,0:T(8,128)S(1)} custom-call(f32[1024,512]{1,0:T(8,128)} %get-tuple-element.12.conv_ref, f32[2,8,128]{2,1,0:T(8,128)S(1)} %psum.7.stats_ref, f32[1,512]{1,0:T(1,128)S(1)} %bitcast.25), custom_call_target="tpu_custom_call" | custom-call | flops 4194304 | bytes 4194304 | tf_op jit(solution)/shard_map/finish/pallas_call | solution.py:217
  170.1 5.1 %attend.1 = bf16[1024,512]{1,0:T(8,128)(2,1)} custom-call(s32[1]{0:T(128)} %bitcast.plane_ref, s32[32]{0:T(128)S(1)} %reshape.51.where_ref, f32[1024,512]{1,0:T(8,128)S(1)} %finish.1.conv_ref, f32[1,512]{1,0:T(1,128)S(1)} %bitcast.26, bf16[8,272,512]{2,1,0:T(8,128)(2,1)} %copy-done.2, bf16[8,240,512]{2,1,0:T(8,128)(2,1)} %all-to-all-done.2.refs_1_, ...), custom_call_target="tpu_custom_call" | custom-call | flops 268435456 | bytes 5242880 | tf_op jit(solution)/shard_map/attend/pallas_call | solution.py:348
  (45 shorter events, 10.9 us)
Async XLA Ops:
  3.8 11.9 %copy-start.5 = (s32[16,2]{0,1:T(2,128)S(1)}, s32[16,2]{0,1:T(2,128)}, u32[]{:S(2)}) copy-start(s32[16,2]{0,1:T(2,128)} %param.24) | copy-start | bytes 388
  3.8 12.1 %copy-start.6 = (s32[16,2]{0,1:T(2,128)S(1)}, s32[16,2]{0,1:T(2,128)}, u32[]{:S(2)}) copy-start(s32[16,2]{0,1:T(2,128)} %param.25) | copy-start | bytes 388
  3.8 39.0 %collective-permute-start.3 = (bf16[8,64,512]{2,1,0:T(8,128)(2,1)S(1)}, bf16[8,64,512]{2,1,0:T(8,128)(2,1)S(1)}, u32[]{:S(2)}, u32[]{:S(2)}) collective-permute-start(bf16[8,64,512]{2,1,0:T(8,128)(2,1)S(1)} %bitcast.17), channel_id=1, source_target_pairs={{0,32},{32,64},{64,96},{96,128},{128,160},{160,192},{192,224},{224... | collective-permute-start | bytes 1572872 | tf_op jit(solution)/shard_map/ppermute | solution.py:487
  9.6 33.3 %collective-permute-start.4 = (bf16[8,64,512]{2,1,0:T(8,128)(2,1)S(1)}, bf16[8,64,512]{2,1,0:T(8,128)(2,1)S(1)}, u32[]{:S(2)}, u32[]{:S(2)}) collective-permute-start(bf16[8,64,512]{2,1,0:T(8,128)(2,1)S(1)} %bitcast.20), channel_id=1, source_target_pairs={{0,32},{32,64},{64,96},{96,128},{128,160},{160,192},{192,224},{224... | collective-permute-start | bytes 1572872 | tf_op jit(solution)/shard_map/ppermute | solution.py:487
  11.6 31.3 %collective-permute-start.5 = (bf16[8,64,512]{2,1,0:T(8,128)(2,1)S(1)}, bf16[8,64,512]{2,1,0:T(8,128)(2,1)S(1)}, u32[]{:S(2)}, u32[]{:S(2)}) collective-permute-start(bf16[8,64,512]{2,1,0:T(8,128)(2,1)S(1)} %bitcast.18), channel_id=1, source_target_pairs={{0,224},{32,0},{64,32},{96,64},{128,96},{160,128},{192,160},{224,1... | collective-permute-start | bytes 1572872 | tf_op jit(solution)/shard_map/ppermute | solution.py:487
  13.7 29.2 %collective-permute-start.6 = (bf16[8,64,512]{2,1,0:T(8,128)(2,1)S(1)}, bf16[8,64,512]{2,1,0:T(8,128)(2,1)S(1)}, u32[]{:S(2)}, u32[]{:S(2)}) collective-permute-start(bf16[8,64,512]{2,1,0:T(8,128)(2,1)S(1)} %bitcast.21), channel_id=1, source_target_pairs={{0,224},{32,0},{64,32},{96,64},{128,96},{160,128},{192,160},{224,1... | collective-permute-start | bytes 1572872 | tf_op jit(solution)/shard_map/ppermute | solution.py:487
  16.9 25.9 %all-to-all-start = ((s32[64,1,8]{2,1,0:T(1,128)}), s32[64,1,8]{2,1,0:T(1,128)S(1)}, u32[]{:S(2)}, u32[]{:S(2)}) async-start(s32[64,1,8]{2,1,0:T(1,128)} %bitcast.11), calls=%async_computation | async-start | bytes 65536 | tf_op jit(solution)/shard_map/all_to_all | solution.py:491
  46.0 3.8 %copy-start.8 = (bf16[8,64,512]{2,1,0:T(8,128)(2,1)S(1)}, bf16[8,64,512]{2,1,0:T(8,128)(2,1)}, u32[]{:S(2)}) copy-start(bf16[8,64,512]{2,1,0:T(8,128)(2,1)} %get-tuple-element.17) | copy-start | bytes 1572868
  46.0 6.3 %copy-start.7 = (bf16[8,64,512]{2,1,0:T(8,128)(2,1)S(1)}, bf16[8,64,512]{2,1,0:T(8,128)(2,1)}, u32[]{:S(2)}) copy-start(bf16[8,64,512]{2,1,0:T(8,128)(2,1)} %get-tuple-element.18) | copy-start | bytes 1572868
  46.0 43.4 %all-to-all-start.1 = ((bf16[8,272,512]{2,1,0:T(8,128)(2,1)}), bf16[8,272,512]{2,1,0:T(8,128)(2,1)S(1)}, u32[]{:S(2)}, u32[]{:S(2)}) async-start(bf16[8,272,512]{2,1,0:T(8,128)(2,1)} %get-tuple-element.14), calls=%async_computation.1 | async-start | bytes 4456448 | tf_op jit(solution)/shard_map/all_to_all | solution.py:491
  49.8 16.1 %collective-permute-start.9 = (bf16[8,64,512]{2,1,0:T(8,128)(2,1)S(1)}, bf16[8,64,512]{2,1,0:T(8,128)(2,1)S(1)}, u32[]{:S(2)}, u32[]{:S(2)}) collective-permute-start(bf16[8,64,512]{2,1,0:T(8,128)(2,1)S(1)} %copy-done.8), channel_id=1, source_target_pairs={{0,32},{32,64},{64,96},{96,128},{128,160},{160,192},{192,224},{224... | collective-permute-start | bytes 1572872 | tf_op jit(solution)/shard_map/ppermute | solution.py:487
  52.3 15.3 %collective-permute-start.10 = (bf16[8,64,512]{2,1,0:T(8,128)(2,1)S(1)}, bf16[8,64,512]{2,1,0:T(8,128)(2,1)S(1)}, u32[]{:S(2)}, u32[]{:S(2)}) collective-permute-start(bf16[8,64,512]{2,1,0:T(8,128)(2,1)S(1)} %copy-done.7), channel_id=1, source_target_pairs={{0,224},{32,0},{64,32},{96,64},{128,96},{160,128},{192,160},{224,1... | collective-permute-start | bytes 1572872 | tf_op jit(solution)/shard_map/ppermute | solution.py:487
  53.1 32.7 %collective-permute-start.7 = (bf16[8,56,512]{2,1,0:T(8,128)(2,1)}, bf16[8,56,512]{2,1,0:T(8,128)(2,1)S(1)}, u32[]{:S(2)}, u32[]{:S(2)}) collective-permute-start(bf16[8,56,512]{2,1,0:T(8,128)(2,1)} %get-tuple-element.15), channel_id=1, source_target_pairs={{0,64},{32,96},{64,128},{96,160},{128,192},{160,224},{192,0},{224,... | collective-permute-start | bytes 1376264 | tf_op jit(solution)/shard_map/ppermute | solution.py:487
  54.4 31.5 %collective-permute-start.8 = (bf16[8,56,512]{2,1,0:T(8,128)(2,1)}, bf16[8,56,512]{2,1,0:T(8,128)(2,1)S(1)}, u32[]{:S(2)}, u32[]{:S(2)}) collective-permute-start(bf16[8,56,512]{2,1,0:T(8,128)(2,1)} %get-tuple-element.16), channel_id=1, source_target_pairs={{0,192},{32,224},{64,0},{96,32},{128,64},{160,96},{192,128},{224,1... | collective-permute-start | bytes 1376264 | tf_op jit(solution)/shard_map/ppermute | solution.py:487
  86.6 0.8 copy-start.4
  89.5 8.7 %copy-start.2 = (bf16[8,272,512]{2,1,0:T(8,128)(2,1)}, bf16[8,272,512]{2,1,0:T(8,128)(2,1)S(1)}, u32[]{:S(2)}) copy-start(bf16[8,272,512]{2,1,0:T(8,128)(2,1)S(1)} %all-to-all-done.1.refs_0_) | copy-start | bytes 6684676
  89.5 80.6 %all-to-all-start.2 = ((bf16[8,240,512]{2,1,0:T(8,128)(2,1)}), bf16[8,240,512]{2,1,0:T(8,128)(2,1)}, u32[]{:S(2)}, u32[]{:S(2)}) async-start(bf16[8,240,512]{2,1,0:T(8,128)(2,1)} %fill.3), calls=%async_computation.2 | async-start | bytes 3932160 | tf_op jit(solution)/shard_map/all_to_all | solution.py:491
  93.9 26.4 %collective-permute-start = (bf16[1024,512]{1,0:T(8,128)(2,1)}, bf16[1024,512]{1,0:T(8,128)(2,1)}, u32[]{:S(2)}, u32[]{:S(2)}) collective-permute-start(bf16[1024,512]{1,0:T(8,128)(2,1)} %own_ref.1), channel_id=1, source_target_pairs={{0,1},{1,2},{2,3},{3,0},{4,5},{5,6},{6,7},{7,4},{8,9},{9,10},{10,1... | collective-permute-start | bytes 3145736 | tf_op jit(solution)/shard_map/ppermute | solution.py:487
  95.4 25.7 %collective-permute-start.1 = (bf16[1024,512]{1,0:T(8,128)(2,1)}, bf16[1024,512]{1,0:T(8,128)(2,1)}, u32[]{:S(2)}, u32[]{:S(2)}) collective-permute-start(bf16[1024,512]{1,0:T(8,128)(2,1)} %own_ref.1), channel_id=1, source_target_pairs={{0,3},{1,0},{2,1},{3,2},{4,7},{5,4},{6,5},{7,6},{8,11},{9,8},{10,9... | collective-permute-start | bytes 3145736 | tf_op jit(solution)/shard_map/ppermute | solution.py:487
  96.0 48.1 %collective-permute-start.2 = (bf16[1024,512]{1,0:T(8,128)(2,1)}, bf16[1024,512]{1,0:T(8,128)(2,1)}, u32[]{:S(2)}, u32[]{:S(2)}) collective-permute-start(bf16[1024,512]{1,0:T(8,128)(2,1)} %own_ref.1), channel_id=1, source_target_pairs={{0,2},{1,3},{2,0},{3,1},{4,6},{5,7},{6,4},{7,5},{8,10},{9,11},{10,... | collective-permute-start | bytes 3145736 | tf_op jit(solution)/shard_map/ppermute | solution.py:487
  98.1 71.9 %collective-permute-start.11 = (bf16[8,40,512]{2,1,0:T(8,128)(2,1)S(1)}, bf16[8,40,512]{2,1,0:T(8,128)(2,1)S(1)}, u32[]{:S(2)}, u32[]{:S(2)}) collective-permute-start(bf16[8,40,512]{2,1,0:T(8,128)(2,1)S(1)} %get-tuple-element.20), channel_id=1, source_target_pairs={{0,96},{32,128},{64,160},{96,192},{128,224},{160,0},{192,32},{224,... | collective-permute-start | bytes 983048 | tf_op jit(solution)/shard_map/ppermute | solution.py:487
  98.4 71.6 %collective-permute-start.12 = (bf16[8,40,512]{2,1,0:T(8,128)(2,1)S(1)}, bf16[8,40,512]{2,1,0:T(8,128)(2,1)S(1)}, u32[]{:S(2)}, u32[]{:S(2)}) collective-permute-start(bf16[8,40,512]{2,1,0:T(8,128)(2,1)S(1)} %get-tuple-element.19), channel_id=1, source_target_pairs={{0,160},{32,192},{64,224},{96,0},{128,32},{160,64},{192,96},{224,1... | collective-permute-start | bytes 983048 | tf_op jit(solution)/shard_map/ppermute | solution.py:487
  144.1 24.0 %copy-start = (f32[512]{0:T(512)S(1)}, f32[512]{0:T(512)}, u32[]{:S(2)}) copy-start(f32[512]{0:T(512)} %param.18) | copy-start | bytes 6148
  168.1 1.9 %copy-start.1 = (f32[512]{0:T(512)S(1)}, f32[512]{0:T(512)}, u32[]{:S(2)}) copy-start(f32[512]{0:T(512)} %param.19) | copy-start | bytes 6148
  (1 other events, 0.8 us)
